TPU v7x, 512 devices: a whole 4x8x8 slice. The times are simulated.
512 devices in a mesh: ep: 32 (over z, x), tp: 16 (over y, core).
Axes of the slice: x: 4, y: 8, z: 8, core: 2. Of those that a mesh axis runs over, the one named last changes fastest.
Arguments:
- queries: bfloat16 [8192, 1536], P('ep', 'tp'), may hold values from -600 to 600
- compressed_key_value: bfloat16 [8192, 512], P('ep'), may hold values from -6 to 6
- rope_key: bfloat16 [8192, 32], P('ep'), may hold values from -6 to 6
- latent_norm_gain: float32 [512], replicated, may hold values from 0.1 to 1.9
- latent_to_key_value: bfloat16 [512, 2048], P(None, 'tp'), may hold values from -0.25 to 0.25
- out_proj: bfloat16 [1024, 2048], P(None, 'tp'), may hold values from -1.5 to 1.5
- moe_input: bfloat16 [8192, 2048], P('ep'), may hold values from -6 to 6
- moe_gain: float32 [2048], replicated, may hold values from 0.1 to 1.9
- routes: int32 [8192, 2], P('ep'), may hold values from 0 to 31, all different within a row; in each aligned block of 256 rows (0 to 255, 256 to 511, ...) at most 24 rows name the same one
- route_weight: float32 [8192, 2], P('ep'), may hold values from 0.2 to 1
- gate_weight: bfloat16 [32, 2048, 4096], P('ep', None, 'tp'), may hold values from -0.125 to 0.125
- up_weight: bfloat16 [32, 2048, 4096], P('ep', None, 'tp'), may hold values from -0.125 to 0.125
- down_weight: bfloat16 [32, 4096, 2048], P('ep', 'tp'), may hold values from -0.09375 to 0.09375
Outputs:
- attention_out: bfloat16 [8192, 2048], P('ep', 'tp')
- expert_out: bfloat16 [8192, 2048], P('ep', 'tp')
Inputs may be any that keep to these rules, and one draw needn't show every extreme that they name: `routes`: each row names 2 different experts. In the rows of one device (aligned blocks of 256 rows) no expert is named by more than 24 rows, and in some blocks one expert is named by exactly 24 rows.
All inputs are finite; a program needn't handle non-finite values.
Results may differ from a plain program's by a relative error of at most 0.019.
The roundings to bfloat16 on the way count: a program that leaves them out, or rounds other values in their place, can miss the bound.
Values may be sent and summed in bfloat16 or wider, within the bound.
No kernel may reach another device: no remote copies, remote signals or barrier semaphores. Data moves between devices by JAX's collectives and lax.ppermute only.
A program may use at most 128 MiB of HBM per device.

v0:
```python
import math

import jax
import jax.numpy as jnp
from jax import lax
from jax.sharding import PartitionSpec as P

PLAIN_HEAD_DIM = 64
ROPE = 32
VALUE_HEAD_DIM = 64


EPSILON = 1e-06
ROPE_BASE_VALUE = 10000.0


def from_everyone(array, axis):
    length = lax.axis_size(axis)
    return lax.all_to_all(
        jnp.broadcast_to(array[None], (length, *array.shape)), axis, 0, 0, tiled=True
    )


def in_order(blocks, dim):
    blocks = jnp.moveaxis(blocks, 0, dim)
    lengths = blocks.shape
    return blocks.reshape(*lengths[:dim], lengths[dim] * lengths[dim + 1], *lengths[dim + 2 :])


def collect(array, axis, dim):
    blocks = from_everyone(array, axis)
    return in_order(blocks, dim)


def sent_together(arrays, axis, dim, along):
    widths = [a.shape[along] for a in arrays]
    both = jnp.concatenate(arrays, axis=along)
    result = collect(both, axis, dim)
    return tuple(jnp.split(result, [sum(widths[:k]) for k in range(1, len(widths))], axis=along))


def cut_along(array, dim, length):
    lengths = array.shape
    blocks = array.reshape(*lengths[:dim], length, lengths[dim] // length, *lengths[dim + 1 :])
    return jnp.moveaxis(blocks, dim, 0)


def sent_and_summed(array, axis, dim):
    length = lax.axis_size(axis)
    blocks = lax.all_to_all(cut_along(array, dim, length), axis, 0, 0, tiled=True)
    return jnp.sum(blocks.astype(jnp.float32), axis=0)


def rms_scale(values, gain_vector):
    floats = values.astype(jnp.float32)
    return (
        floats
        * lax.rsqrt(jnp.mean(floats * floats, axis=-1, keepdims=True) + EPSILON)
        * gain_vector
    )


def rotary(values, positions):
    full_width = values.shape[-1]
    half_dim = full_width // 2
    frequency = ROPE_BASE_VALUE ** (-jnp.arange(half_dim, dtype=jnp.float32) * 2.0 / full_width)
    angles = positions[..., None] * frequency
    cosine = jnp.cos(angles)
    sine_part = jnp.sin(angles)
    first_half = values[..., :half_dim]
    second_half = values[..., half_dim:]
    return jnp.concatenate(
        [
            first_half * cosine - second_half * sine_part,
            second_half * cosine + first_half * sine_part,
        ],
        axis=-1,
    )


def slot_table(block_routes, capacity, experts):
    flat_routes = block_routes.reshape(-1)
    onehot_table = (flat_routes[:, None] == jnp.arange(experts, dtype=jnp.int32)[None, :]).astype(
        jnp.int32
    )
    earlier = jnp.cumsum(onehot_table, axis=0) - onehot_table
    slot_index = jnp.sum(earlier * onehot_table, axis=1)
    destination = flat_routes * capacity + slot_index
    token_count = block_routes.shape[0]
    source_rows = jnp.arange(flat_routes.shape[0], dtype=jnp.int32) // block_routes.shape[1]
    source_table = (
        jnp.full((experts * capacity,), token_count, jnp.int32).at[destination].set(source_rows)
    )
    return (destination, source_table)


def local(
    queries,
    compressed_key_value,
    rope_key,
    latent_norm_gain,
    latent_to_key_value,
    out_proj,
    moe_input,
    moe_gain,
    routes,
    route_weight,
    gate_weight,
    up_weight,
    down_weight,
):
    row_count = queries.shape[0]
    head_count = latent_to_key_value.shape[1] // (PLAIN_HEAD_DIM + VALUE_HEAD_DIM)
    offset = lax.axis_index("ep") * row_count
    positions = (offset + jnp.arange(row_count, dtype=jnp.int32)).astype(jnp.float32)
    query_heads = queries.reshape(row_count, head_count, PLAIN_HEAD_DIM + ROPE)
    query_nope = query_heads[..., :PLAIN_HEAD_DIM]
    query_rope = rotary(
        query_heads[..., PLAIN_HEAD_DIM:].astype(jnp.float32), positions[:, None]
    ).astype(jnp.bfloat16)
    latent_normed = rms_scale(compressed_key_value, latent_norm_gain).astype(jnp.bfloat16)
    key_rope = rotary(rope_key.astype(jnp.float32), positions).astype(jnp.bfloat16)
    score_scale = (PLAIN_HEAD_DIM + ROPE) ** (-0.5)

    def attend_block(state_now, key_value, block_rope):
        run_max, run_total, run_values = state_now
        key_nope = key_value[..., :PLAIN_HEAD_DIM]
        block_values = key_value[..., PLAIN_HEAD_DIM:]
        scores = (
            jnp.einsum("qhd,khd->qhk", query_nope, key_nope, preferred_element_type=jnp.float32)
            + jnp.einsum("qhr,kr->qhk", query_rope, block_rope, preferred_element_type=jnp.float32)
        ) * score_scale
        new_max = jnp.maximum(run_max, jnp.max(scores, axis=-1))
        shrink = jnp.exp(run_max - new_max)
        weights = jnp.exp(scores - new_max[..., None])
        run_total = run_total * shrink + jnp.sum(weights, axis=-1)
        run_values = run_values * shrink[..., None] + jnp.einsum(
            "qhk,khd->qhd",
            weights.astype(jnp.bfloat16),
            block_values,
            preferred_element_type=jnp.float32,
        )
        return (new_max, run_total, run_values)

    initial = (
        jnp.full((row_count, head_count), -jnp.inf, jnp.float32),
        jnp.zeros((row_count, head_count), jnp.float32),
        jnp.zeros((row_count, head_count, VALUE_HEAD_DIM), jnp.float32),
    )

    def expand_heads(block_main):
        return block_main.reshape(block_main.shape[0], head_count, PLAIN_HEAD_DIM + VALUE_HEAD_DIM)

    own_keys = jnp.dot(
        latent_normed, latent_to_key_value, preferred_element_type=jnp.float32
    ).astype(jnp.bfloat16)
    piece_main, piece_rope = sent_together((own_keys, key_rope), "ep", 0, 1)
    piece_rows = piece_main.shape[0]
    group_rows = math.gcd(piece_rows, 2048)
    block_count = piece_rows // group_rows
    main_blocks = piece_main.reshape(block_count, group_rows, piece_main.shape[1])
    rope_blocks = piece_rope.reshape(block_count, group_rows, piece_rope.shape[1])

    def step_block(state_inner, block_data):
        block_main, block_rope = block_data
        return (attend_block(state_inner, expand_heads(block_main), block_rope), None)

    state_out, unused = lax.scan(step_block, initial, (main_blocks, rope_blocks))
    run_max, run_total, run_values = state_out
    attended = (
        (run_values / run_total[..., None])
        .astype(jnp.bfloat16)
        .reshape(row_count, head_count * VALUE_HEAD_DIM)
    )
    projected = jnp.dot(collect(attended, "tp", 1), out_proj, preferred_element_type=jnp.float32)
    attention_out = projected.astype(jnp.bfloat16)
    moe_rows = moe_input.shape[0]
    model_width = moe_input.shape[1]
    expert_local = gate_weight.shape[0]
    ep_count = lax.axis_size("ep")
    tp_count = lax.axis_size("tp")
    expert_total = ep_count * expert_local
    capacity = 3 * moe_rows // ep_count
    normed = rms_scale(moe_input, moe_gain).astype(jnp.bfloat16)
    destination, source_table = slot_table(routes, capacity, expert_total)
    padded = jnp.concatenate([normed, jnp.zeros((1, model_width), jnp.bfloat16)], axis=0)
    outgoing = padded[source_table].reshape(ep_count, expert_local, capacity, model_width)
    column_width = model_width // tp_count
    own_columns = lax.dynamic_slice_in_dim(
        outgoing, lax.axis_index("tp") * column_width, column_width, 3
    )
    arrived_whole = lax.all_gather(
        lax.all_to_all(own_columns, "ep", split_axis=0, concat_axis=0, tiled=True),
        "tp",
        axis=3,
        tiled=True,
    )
    gate_value = jnp.einsum(
        "sexd,edf->sexf", arrived_whole, gate_weight, preferred_element_type=jnp.float32
    )
    up_value = jnp.einsum(
        "sexd,edf->sexf", arrived_whole, up_weight, preferred_element_type=jnp.float32
    )
    hidden = (jax.nn.silu(gate_value) * up_value).astype(jnp.bfloat16)
    partial_out = jnp.einsum(
        "sexf,efd->sexd", hidden, down_weight, preferred_element_type=jnp.float32
    )
    summed = sent_and_summed(partial_out.astype(jnp.bfloat16), "tp", 3).astype(jnp.bfloat16)
    returned = lax.all_to_all(summed, "ep", split_axis=0, concat_axis=0, tiled=True)
    flat_back = returned.reshape(expert_total * capacity, returned.shape[3])
    picked = (
        flat_back[destination]
        .astype(jnp.float32)
        .reshape(moe_rows, routes.shape[1], returned.shape[3])
    )
    expert_out = jnp.sum(picked * route_weight[..., None], axis=1).astype(jnp.bfloat16)
    return (attention_out, expert_out)


def solution(mesh):
    return jax.shard_map(
        local,
        mesh=mesh,
        in_specs=(
            P("ep", "tp"),
            P("ep", None),
            P("ep", None),
            P(),
            P(None, "tp"),
            P(None, "tp"),
            P("ep", None),
            P(),
            P("ep", None),
            P("ep", None),
            P("ep", None, "tp"),
            P("ep", None, "tp"),
            P("ep", "tp", None),
        ),
        out_specs=(P("ep", "tp"), P("ep", "tp")),
        check_vma=False,
    )
```

profile of v0, /device:TPU:1, one launch (start us, length us, event | category | flops | bytes accessed | tf_op | source)
XLA Modules:
  0.0 267.2 jit_solution(14156987945600898278)
XLA Ops:
  11.0 2.4 scatter_custom_fusion
  13.5 1.5 fusion.20
  15.5 4.3 %gather_fusion = bf16[768,2048]{1,0:T(8,128)(2,1)} fusion(bf16[257,2048]{1,0:T(8,128)(2,1)S(1)} %concatenate.23, s32[1024]{0:T(1024)S(1)} %pad_clamp_fusion.1), kind=kCustom, calls=%fused_computation | custom fusion | bytes 6294528 | tf_op jit(solution)/shard_map/gather | solution.py:187
  19.7 1.6 constant_dynamic-slice_fusion
  21.4 13.7 %all-to-all-start.2 = ((bf16[32,1,24,128]{3,2,1,0:T(8,128)(2,1)}), bf16[32,1,24,128]{3,2,1,0:T(8,128)(2,1)S(1)}, u32[]{:S(2)}, u32[]{:S(2)}) async-start(bf16[32,1,24,128]{3,2,1,0:T(8,128)(2,1)} %constant_dynamic-slice_fusion), calls=%async_computation.2 | async-start | bytes 393216 | tf_op jit(solution)/shard_map/all_to_all | solution.py:193
  35.3 9.8 %all-to-all-done.2 = bf16[32,1,24,128]{3,2,1,0:T(8,128)(2,1)S(1)} async-done(((bf16[32,1,24,128]{3,2,1,0:T(8,128)(2,1)}), bf16[32,1,24,128]{3,2,1,0:T(8,128)(2,1)S(1)}, u32[]{:S(2)}, u32[]{:S(2)}) %all-to-all-start.2) | async-done | bytes 196640 | tf_op jit(solution)/shard_map/all_to_all | solution.py:193
  46.3 1.8 broadcast_in_dim.21
  48.1 4.9 %all-to-all-start = ((bf16[32,256,160]{1,2,0:T(8,128)(2,1)}), bf16[32,256,160]{1,2,0:T(8,128)(2,1)}, u32[]{:S(2)}, u32[]{:S(2)}) async-start(bf16[32,256,160]{1,2,0:T(8,128)(2,1)} %broadcast_in_dim.21), calls=%async_computation | async-start | bytes 5242880 | tf_op jit(solution)/shard_map/all_to_all | solution.py:19
  53.2 58.1 %all-to-all-done = bf16[32,256,160]{1,2,0:T(8,128)(2,1)} async-done(((bf16[32,256,160]{1,2,0:T(8,128)(2,1)}), bf16[32,256,160]{1,2,0:T(8,128)(2,1)}, u32[]{:S(2)}, u32[]{:S(2)}) %all-to-all-start) | async-done | bytes 2621472 | tf_op jit(solution)/shard_map/all_to_all | solution.py:19
  111.3 2.0 copy.47
  114.3 2.4 copy.44
  116.8 2.8 %copy.45 = bf16[8192,32]{1,0:T(8,128)(2,1)} copy(bf16[8192,32]{0,1:T(8,128)(2,1)} %split.9) | data formatting | bytes 1048576
  119.6 4.0 %fusion.24 = f32[32,1,24,256]{3,2,0,1:T(8,128)} fusion(bf16[32,1,24,2048]{3,2,0,1:T(8,128)(2,1)} %all-gather.2.cloned.1.call-done, bf16[1,2048,256]{2,1,0:T(8,128)(2,1)S(1)} %copy-done.11), kind=kOutput, calls=%fused_computation.41 | convolution fusion | flops 805306368 | bytes 4980736 | tf_op jit(solution)/shard_map/sexd,edf->sexf/dot_general | solution.py:198
  123.6 7.2 %fusion.23 = bf16[1,32,3,16,8,128]{5,4,3,2,1,0:T(8,128)(2,1)} fusion(bf16[1,256,2048]{2,1,0:T(8,128)(2,1)S(1)} %copy-done, bf16[32,1,24,2048]{3,2,0,1:T(8,128)(2,1)} %all-gather.2.cloned.1.call-done, bf16[1,2048,256]{2,1,0:T(8,128)(2,1)S(1)} %copy-done.12, f32[32,1,24,256]{3,2,0,1:T(8,128)} %fusion.24), kind=kOutput, calls=%fused_computation.40 | convolution fusion | flops 1613365248 | bytes 9175040 | tf_op jit(solution)/shard_map/sexf,efd->sexd/dot_general | solution.py:205
  130.7 4.4 %copy.51 = bf16[1,32,3,16,8,128]{5,4,2,1,0,3:T(8,128)(2,1)} copy(bf16[1,32,3,16,8,128]{5,4,3,2,1,0:T(8,128)(2,1)} %fusion.23) | data formatting | bytes 6291456 | tf_op jit(solution)/shard_map/reshape | solution.py:44
  135.1 11.7 %all-to-all-start.3 = ((bf16[16,32,1,24,128]{4,3,1,2,0:T(8,128)(2,1)}), bf16[16,32,1,24,128]{4,3,1,2,0:T(8,128)(2,1)}, u32[]{:S(2)}, u32[]{:S(2)}) async-start(bf16[16,32,1,24,128]{4,3,1,2,0:T(8,128)(2,1)} %bitcast.183), calls=%async_computation.3 | async-start | bytes 6291456 | tf_op jit(solution)/shard_map/all_to_all | solution.py:50
  146.8 20.3 %while.15 = (s32[]{:T(128)}, f32[256,1]{0,1:T(1,128)S(1)}, f32[256,1]{0,1:T(1,128)S(1)}, f32[256,1,64]{0,2,1:T(8,128)S(1)}, bf16[4,2048,128]{2,1,0:T(8,128)(2,1)...) while((s32[]{:T(128)}, f32[256,1]{0,1:T(1,128)S(1)}, ...), condition=%wide.region_4.5_spmd.clone, body=%wide.region_1.4_spmd.clone.sunk | while | flops 171492608 | bytes 17498796 | solution.py:168
  146.8 1.4 convolution_bitcast_fusion.4
  167.0 50.8 %all-to-all-done.3 = bf16[16,32,1,24,128]{4,3,1,2,0:T(8,128)(2,1)} async-done(((bf16[16,32,1,24,128]{4,3,1,2,0:T(8,128)(2,1)}), bf16[16,32,1,24,128]{4,3,1,2,0:T(8,128)(2,1)}, u32[]{:S(2)}, u32[]{:S(2)}) %all-to-all-start.3) | async-done | bytes 3145760 | tf_op jit(solution)/shard_map/all_to_all | solution.py:50
  218.7 5.5 %all-to-all-start.1 = ((bf16[16,256,64]{1,2,0:T(8,128)(2,1)}), bf16[16,256,64]{1,2,0:T(8,128)(2,1)S(1)}, u32[]{:S(2)}, u32[]{:S(2)}) async-start(bf16[16,256,64]{1,2,0:T(8,128)(2,1)} %broadcast_in_dim.23), calls=%async_computation.1 | async-start | bytes 1048576 | tf_op jit(solution)/shard_map/all_to_all | solution.py:19
  224.1 3.1 %reduce_sum.67 = bf16[32,24,128]{2,1,0:T(8,128)(2,1)} reduce(bf16[16,32,1,24,128]{4,3,1,2,0:T(8,128)(2,1)} %all-to-all-done.3, bf16[]{:T(256)} %constant.78.clone.1), dimensions={0,2}, to_apply=%region_10.11 | reduce | flops 1474560 | bytes 3342338 | tf_op jit(solution)/shard_map/reduce_sum | solution.py:51
  227.2 14.1 %all-to-all-done.1 = bf16[16,256,64]{1,2,0:T(8,128)(2,1)S(1)} async-done(((bf16[16,256,64]{1,2,0:T(8,128)(2,1)}), bf16[16,256,64]{1,2,0:T(8,128)(2,1)S(1)}, u32[]{:S(2)}, u32[]{:S(2)}) %all-to-all-start.1) | async-done | bytes 524320 | tf_op jit(solution)/shard_map/all_to_all | solution.py:19
  241.3 5.0 %all-to-all-start.4 = ((bf16[32,1,24,128]{3,2,1,0:T(8,128)(2,1)}), bf16[32,1,24,128]{3,2,1,0:T(8,128)(2,1)S(1)}, u32[]{:S(2)}, u32[]{:S(2)}) async-start(bf16[32,1,24,128]{3,2,1,0:T(8,128)(2,1)} %bitcast.33), calls=%async_computation.4 | async-start | bytes 393216 | tf_op jit(solution)/shard_map/all_to_all | solution.py:209
  247.4 10.5 %all-to-all-done.4 = bf16[32,1,24,128]{3,2,1,0:T(8,128)(2,1)S(1)} async-done(((bf16[32,1,24,128]{3,2,1,0:T(8,128)(2,1)}), bf16[32,1,24,128]{3,2,1,0:T(8,128)(2,1)S(1)}, u32[]{:S(2)}, u32[]{:S(2)}) %all-to-all-start.4) | async-done | bytes 196640 | tf_op jit(solution)/shard_map/all_to_all | solution.py:209
  (119 shorter events, 29.7 us)
Async XLA Ops:
  7.2 116.4 %copy-start = (bf16[1,256,2048]{2,1,0:T(8,128)(2,1)S(1)}, bf16[1,256,2048]{2,1,0:T(8,128)(2,1)}, u32[]{:S(2)}) copy-start(bf16[1,256,2048]{2,1,0:T(8,128)(2,1)} %param.27) | copy-start | bytes 3145732
  7.2 7.8 %copy-start.3 = (bf16[256,2048]{1,0:T(8,128)(2,1)S(1)}, bf16[256,2048]{1,0:T(8,128)(2,1)}, u32[]{:S(2)}) copy-start(bf16[256,2048]{1,0:T(8,128)(2,1)} %param.21) | copy-start | bytes 3145732
  7.2 7.8 %copy-start.9 = (f32[2048]{0:T(1024)S(1)}, f32[2048]{0:T(1024)}, u32[]{:S(2)}) copy-start(f32[2048]{0:T(1024)} %param.22) | copy-start | bytes 24580
  15.4 19.7 %copy-start.5 = (bf16[256,512]{1,0:T(8,128)(2,1)S(1)}, bf16[256,512]{1,0:T(8,128)(2,1)}, u32[]{:S(2)}) copy-start(bf16[256,512]{1,0:T(8,128)(2,1)} %param.16) | copy-start | bytes 786436
  15.4 30.3 %copy-start.8 = (bf16[256,32]{0,1:T(8,128)(2,1)S(1)}, bf16[256,32]{0,1:T(8,128)(2,1)}, u32[]{:S(2)}) copy-start(bf16[256,32]{0,1:T(8,128)(2,1)} %param.17) | copy-start | bytes 49156
  15.4 30.5 %copy-start.13 = (bf16[512,128]{1,0:T(8,128)(2,1)S(1)}, bf16[512,128]{1,0:T(8,128)(2,1)}, u32[]{:S(2)}) copy-start(bf16[512,128]{1,0:T(8,128)(2,1)} %param.19) | copy-start | bytes 393220
  15.5 30.5 %copy-start.14 = (f32[512]{0:T(512)S(1)}, f32[512]{0:T(512)}, u32[]{:S(2)}) copy-start(f32[512]{0:T(512)} %param.18) | copy-start | bytes 6148
  21.4 23.7 %all-to-all-start.2 = ((bf16[32,1,24,128]{3,2,1,0:T(8,128)(2,1)}), bf16[32,1,24,128]{3,2,1,0:T(8,128)(2,1)S(1)}, u32[]{:S(2)}, u32[]{:S(2)}) async-start(bf16[32,1,24,128]{3,2,1,0:T(8,128)(2,1)} %constant_dynamic-slice_fusion), calls=%async_computation.2 | async-start | bytes 393216 | tf_op jit(solution)/shard_map/all_to_all | solution.py:193
  35.1 84.5 %all-gather.2.cloned.1.call-start = ((), (), s32[]{:S(2)}) async-start(), calls=%async_computation.5 | async-start | bytes 3342336 | tf_op jit(solution)/shard_map/all_gather | solution.py:192
  48.1 5.0 %copy-start.7 = (bf16[256,96]{0,1:T(8,128)(2,1)S(1)}, bf16[256,96]{0,1:T(8,128)(2,1)}, u32[]{:S(2)}) copy-start(bf16[256,96]{0,1:T(8,128)(2,1)} %param.15) | copy-start | bytes 147460
  48.1 63.3 %all-to-all-start = ((bf16[32,256,160]{1,2,0:T(8,128)(2,1)}), bf16[32,256,160]{1,2,0:T(8,128)(2,1)}, u32[]{:S(2)}, u32[]{:S(2)}) async-start(bf16[32,256,160]{1,2,0:T(8,128)(2,1)} %broadcast_in_dim.21), calls=%async_computation | async-start | bytes 5242880 | tf_op jit(solution)/shard_map/all_to_all | solution.py:19
  116.8 2.8 %copy-start.11 = (bf16[1,2048,256]{2,1,0:T(8,128)(2,1)S(1)}, bf16[1,2048,256]{2,1,0:T(8,128)(2,1)}, u32[]{:S(2)}) copy-start(bf16[1,2048,256]{2,1,0:T(8,128)(2,1)} %param.25) | copy-start | bytes 3145732
  119.6 4.0 %copy-start.12 = (bf16[1,2048,256]{2,1,0:T(8,128)(2,1)S(1)}, bf16[1,2048,256]{2,1,0:T(8,128)(2,1)}, u32[]{:S(2)}) copy-start(bf16[1,2048,256]{2,1,0:T(8,128)(2,1)} %param.26) | copy-start | bytes 3145732
  135.1 82.7 %all-to-all-start.3 = ((bf16[16,32,1,24,128]{4,3,1,2,0:T(8,128)(2,1)}), bf16[16,32,1,24,128]{4,3,1,2,0:T(8,128)(2,1)}, u32[]{:S(2)}, u32[]{:S(2)}) async-start(bf16[16,32,1,24,128]{4,3,1,2,0:T(8,128)(2,1)} %bitcast.183), calls=%async_computation.3 | async-start | bytes 6291456 | tf_op jit(solution)/shard_map/all_to_all | solution.py:50
  149.3 0.8 copy-start.1
  150.1 1.0 copy-start.2
  154.4 0.8 copy-start.1
  155.2 1.0 copy-start.2
  160.2 1.0 copy-start.2
  165.3 1.0 copy-start.2
  218.7 22.7 %all-to-all-start.1 = ((bf16[16,256,64]{1,2,0:T(8,128)(2,1)}), bf16[16,256,64]{1,2,0:T(8,128)(2,1)S(1)}, u32[]{:S(2)}, u32[]{:S(2)}) async-start(bf16[16,256,64]{1,2,0:T(8,128)(2,1)} %broadcast_in_dim.23), calls=%async_computation.1 | async-start | bytes 1048576 | tf_op jit(solution)/shard_map/all_to_all | solution.py:19
  224.1 22.2 %copy-start.10 = (f32[256,2]{0,1:T(2,128)S(1)}, f32[256,2]{0,1:T(2,128)}, u32[]{:S(2)}) copy-start(f32[256,2]{0,1:T(2,128)} %param.24) | copy-start | bytes 6148
  224.1 22.3 %copy-start.6 = (bf16[1024,128]{1,0:T(8,128)(2,1)S(1)}, bf16[1024,128]{1,0:T(8,128)(2,1)}, u32[]{:S(2)}) copy-start(bf16[1024,128]{1,0:T(8,128)(2,1)} %param.20) | copy-start | bytes 786436
  241.3 16.6 %all-to-all-start.4 = ((bf16[32,1,24,128]{3,2,1,0:T(8,128)(2,1)}), bf16[32,1,24,128]{3,2,1,0:T(8,128)(2,1)S(1)}, u32[]{:S(2)}, u32[]{:S(2)}) async-start(bf16[32,1,24,128]{3,2,1,0:T(8,128)(2,1)} %bitcast.33), calls=%async_computation.4 | async-start | bytes 393216 | tf_op jit(solution)/shard_map/all_to_all | solution.py:209
  (3 other events, 2.3 us)
Sparse Core Ops, SparseCore 0:
  45.9 44.7 all-gather.1
where the time goes:
time: 268 us; the launch traced here: 267 us
  waiting for transfers between devices  143 us (53%)
  starting transfers between devices  40.8 us (15%)
  local copies, waits for them, and re-layouts  35.7 us (13%)
  matrix products  22.8 us (9%)
  between operations  14.4 us (5%)
  other arithmetic  10 us (4%)
    all_to_all x2, waiting for transfers between devices, from_everyone(): lax.all_to_all(jnp.broadcast_to(array[None], (length, *array.shape)), axi...  72.2 us
    all_to_all x1, waiting for transfers between devices, sent_and_summed(): lax.all_to_all(cut_along(array, dim, length), axis, 0, 0, tiled=True)  50.8 us
    all_to_all x1, starting transfers between devices, local(): lax.all_to_all(own_columns, 'ep', split_axis=0, concat_axis=0, tiled=True)  13.7 us
    all_to_all x1, starting transfers between devices, sent_and_summed(): lax.all_to_all(cut_along(array, dim, length), axis, 0, 0, tiled=True)  11.7 us
    all_to_all x1, waiting for transfers between devices, local(): lax.all_to_all(summed, 'ep', split_axis=0, concat_axis=0, tiled=True)  10.5 us
    all_to_all x2, starting transfers between devices, from_everyone(): lax.all_to_all(jnp.broadcast_to(array[None], (length, *array.shape)), axi...  10.4 us
    all_to_all x1, waiting for transfers between devices, local(): lax.all_to_all(own_columns, 'ep', split_axis=0, concat_axis=0, tiled=True)  9.77 us
    dot_general x1, matrix products, local(): jnp.einsum('sexf,efd->sexd', hidden, down_weight, preferred_element_type=...  7.15 us
  transfers between devices with their start and end apart: 6, of which 5 were waited for; matrix products, arithmetic and copies ran while one was open for 12% of the time, Pallas kernels for 0%

commit v1 on v0

v1 whole, which is shorter than its diff:
```python
import math

import jax
import jax.numpy as jnp
from jax import lax
from jax.experimental import pallas as pl
from jax.experimental.pallas import tpu as pltpu
from jax.sharding import PartitionSpec as P

PLAIN_HEAD_DIM = 64
ROPE = 32
VALUE_HEAD_DIM = 64
LANES = 128

EPSILON = 1e-06
ROPE_BASE_VALUE = 10000.0

VMEM = pl.BlockSpec(memory_space=pltpu.VMEM)
SMEM = pl.BlockSpec(memory_space=pltpu.SMEM)


def kernel_call(body, out_shape, in_specs, out_specs, flops, limit=48):
    return pl.pallas_call(
        body,
        out_shape=out_shape,
        in_specs=in_specs,
        out_specs=out_specs,
        compiler_params=pltpu.CompilerParams(vmem_limit_bytes=limit * 1024 * 1024),
        cost_estimate=pl.CostEstimate(flops=flops, transcendentals=0, bytes_accessed=0),
    )


def rms_scale(values, gain_vector):
    floats = values.astype(jnp.float32)
    return (
        floats
        * lax.rsqrt(jnp.mean(floats * floats, axis=-1, keepdims=True) + EPSILON)
        * gain_vector
    )


def to_everyone(array, axis, groups, count):
    return lax.all_to_all(
        jnp.broadcast_to(array[None], (count, *array.shape)),
        axis,
        0,
        0,
        tiled=True,
        axis_index_groups=groups,
    )


def pack_rows(index, moe_input, gain, routes, capacity, expert_total):
    rows, width = moe_input.shape
    places = expert_total * capacity
    top = routes.shape[1]

    def body(index_ref, input_ref, gain_ref, routes_ref, out_ref, place_ref):
        floats = input_ref[...].astype(jnp.float32)
        scale = lax.rsqrt(jnp.mean(floats * floats, axis=-1, keepdims=True) + EPSILON)
        start = pl.multiple_of(index_ref[0] * LANES, LANES)
        own = input_ref[:, pl.ds(start, LANES)].astype(jnp.float32)
        normed = (own * scale * gain_ref[:, pl.ds(start, LANES)]).astype(jnp.bfloat16)
        chosen = routes_ref[...]
        expert = lax.broadcasted_iota(jnp.int32, (rows, expert_total), 1)
        named = [chosen[:, k : k + 1] == expert for k in range(top)]
        either = named[0]
        for other in named[1:]:
            either = either | other
        ones = jnp.where(either, 1.0, 0.0).astype(jnp.bfloat16)
        lower = lax.broadcasted_iota(jnp.int32, (rows, rows), 0) > lax.broadcasted_iota(
            jnp.int32, (rows, rows), 1
        )
        lower = jnp.where(lower, 1.0, 0.0).astype(jnp.bfloat16)
        earlier = jnp.dot(lower, ones, preferred_element_type=jnp.float32)
        value = earlier + expert.astype(jnp.float32) * float(capacity)
        slots = lax.broadcasted_iota(jnp.int32, (rows, places), 1)
        hit = None
        for k in range(top):
            place = jnp.sum(jnp.where(named[k], value, 0.0), axis=1, keepdims=True).astype(
                jnp.int32
            )
            place_ref[:, k : k + 1] = place
            here = slots == place
            hit = here if hit is None else hit | here
        select = jnp.where(hit, 1.0, 0.0).astype(jnp.bfloat16)
        out_ref[...] = lax.dot_general(
            select, normed, (((0,), (0,)), ((), ())), preferred_element_type=jnp.float32
        ).astype(jnp.bfloat16)

    return kernel_call(
        body,
        (
            jax.ShapeDtypeStruct((places, LANES), jnp.bfloat16),
            jax.ShapeDtypeStruct((rows, top), jnp.int32),
        ),
        [SMEM, VMEM, VMEM, VMEM],
        (VMEM, VMEM),
        2 * rows * places * LANES,
    )(index, moe_input, gain, routes)


def attend(query, key_value, score_scale):
    blocks, rows, _ = query.shape
    pieces, _, length = key_value.shape
    factor = score_scale * math.log2(math.e)
    first_value = PLAIN_HEAD_DIM + ROPE

    def body(query_ref, key_ref, out_ref):
        def one_block(i, carry):
            q = query_ref[i]
            scores = [
                jnp.dot(q, key_ref[j, :LANES, :], preferred_element_type=jnp.float32)
                for j in range(pieces)
            ]
            top = scores[0]
            for s in scores[1:]:
                top = jnp.maximum(top, s)
            top = jnp.max(top, axis=1, keepdims=True) * factor
            total = None
            mixed = None
            for j in range(pieces):
                weight = jnp.exp2(scores[j] * factor - top)
                total = weight if total is None else total + weight
                part = lax.dot_general(
                    weight.astype(jnp.bfloat16),
                    key_ref[j, first_value:, :],
                    (((1,), (1,)), ((), ())),
                    preferred_element_type=jnp.float32,
                )
                mixed = part if mixed is None else mixed + part
            total = jnp.sum(total, axis=1, keepdims=True)
            out_ref[i, :, :VALUE_HEAD_DIM] = (mixed / total).astype(jnp.bfloat16)
            log_total = top + jnp.log2(total)
            high = log_total.astype(jnp.bfloat16).astype(jnp.float32)
            middle = (log_total - high).astype(jnp.bfloat16).astype(jnp.float32)
            low = log_total - high - middle
            lane = lax.broadcasted_iota(jnp.int32, (rows, LANES - VALUE_HEAD_DIM), 1)
            out_ref[i, :, VALUE_HEAD_DIM:] = jnp.where(
                lane == 0, high, jnp.where(lane == 1, middle, low)
            ).astype(jnp.bfloat16)
            return carry

        lax.fori_loop(0, blocks, one_block, 0)

    return kernel_call(
        body,
        jax.ShapeDtypeStruct((blocks, rows, LANES), jnp.bfloat16),
        [VMEM, VMEM],
        VMEM,
        4 * blocks * rows * pieces * length * 2 * LANES,
    )(query, key_value)


def experts(rows_in, gates, ups, downs):
    blocks, rows, _ = rows_in.shape
    units = gates[0].shape[1]
    wide = 2 * LANES
    count = len(gates)

    def body(*refs):
        rows_ref = refs[0]
        gate_refs, up_refs, down_refs = (refs[1 + k * count : 1 + (k + 1) * count] for k in range(3))
        out_ref = refs[-1]
        hidden = []
        for gate_ref, up_ref in zip(gate_refs, up_refs):
            gate_value = jnp.zeros((rows, units), jnp.float32)
            up_value = jnp.zeros((rows, units), jnp.float32)
            for b in range(0, blocks, 2):
                part = jnp.concatenate([rows_ref[b], rows_ref[b + 1]], axis=1)
                span = slice(b * LANES, b * LANES + wide)
                gate_value += jnp.dot(part, gate_ref[span, :], preferred_element_type=jnp.float32)
                up_value += jnp.dot(part, up_ref[span, :], preferred_element_type=jnp.float32)
            silu = gate_value / (1.0 + jnp.exp(-gate_value))
            hidden.append((silu * up_value).astype(jnp.bfloat16))
        for b in range(0, blocks, 2):
            span = slice(b * LANES, b * LANES + wide)
            total = None
            for h, down_ref in zip(hidden, down_refs):
                part = jnp.dot(h, down_ref[:, span], preferred_element_type=jnp.float32)
                total = part if total is None else total + part
            total = total.astype(jnp.bfloat16)
            out_ref[b] = total[:, :LANES]
            out_ref[b + 1] = total[:, LANES:]

    return kernel_call(
        body,
        jax.ShapeDtypeStruct((blocks, rows, LANES), jnp.bfloat16),
        [VMEM] * (1 + 3 * count),
        VMEM,
        2 * rows * blocks * LANES * units * 3 * count,
    )(rows_in, *gates, *ups, *downs)


def combine(returned, places, route_weight):
    total, width = returned.shape
    rows, top = places.shape

    def body(rows_ref, place_ref, weight_ref, out_ref):
        slots = lax.broadcasted_iota(jnp.int32, (rows, total), 1)
        result = None
        for k in range(top):
            select = jnp.where(slots == place_ref[:, k : k + 1], 1.0, 0.0).astype(jnp.bfloat16)
            picked = jnp.dot(select, rows_ref[...], preferred_element_type=jnp.float32)
            part = picked * weight_ref[:, k : k + 1]
            result = part if result is None else result + part
        out_ref[...] = result.astype(jnp.bfloat16)

    return kernel_call(
        body,
        jax.ShapeDtypeStruct((rows, width), jnp.bfloat16),
        [VMEM] * 3,
        VMEM,
        2 * rows * total * width * top,
    )(returned, places, route_weight)


def make_local(z_count, x_count, tp_count):
    x_groups = [[x_count * z + x for x in range(x_count)] for z in range(z_count)]
    z_groups = [[x_count * z + x for z in range(z_count)] for x in range(x_count)]
    partner = [(i, i ^ 1) for i in range(tp_count)]

    def local(
        queries,
        compressed_key_value,
        rope_key,
        latent_norm_gain,
        latent_to_key_value,
        out_proj,
        moe_input,
        moe_gain,
        routes,
        route_weight,
        gate_weight,
        up_weight,
        down_weight,
    ):
        row_count = queries.shape[0]
        ep_count = z_count * x_count
        capacity = 3 * row_count // ep_count
        tp_index = lax.axis_index("tp").astype(jnp.int32)

        gates = [gate_weight[0]]
        ups = [up_weight[0]]
        downs = [down_weight[0]]
        for pair in (gates, ups, downs):
            pair.append(lax.ppermute(pair[0], "tp", partner))

        outgoing, places = pack_rows(
            tp_index.reshape(1), moe_input, moe_gain.reshape(1, -1), routes, capacity, ep_count
        )
        arrived = lax.all_to_all(
            outgoing.reshape(ep_count, capacity, LANES), "ep", 0, 0, tiled=True
        )

        offset = lax.axis_index("ep") * row_count
        positions = (offset + jnp.arange(row_count, dtype=jnp.int32)).astype(jnp.float32)
        half = ROPE // 2
        frequency = ROPE_BASE_VALUE ** (-jnp.arange(half, dtype=jnp.float32) * 2.0 / ROPE)
        angles = positions[:, None] * frequency
        cosine, sine = jnp.cos(angles), jnp.sin(angles)

        def rotated(values):
            first, second = values[:, :half], values[:, half:]
            return jnp.concatenate(
                [first * cosine - second * sine, second * cosine + first * sine], axis=1
            ).astype(jnp.bfloat16)

        query = jnp.concatenate(
            [
                queries[:, :PLAIN_HEAD_DIM],
                rotated(queries[:, PLAIN_HEAD_DIM:].astype(jnp.float32)),
                jnp.zeros((row_count, LANES - PLAIN_HEAD_DIM - ROPE), jnp.bfloat16),
            ],
            axis=1,
        )
        latent_normed = rms_scale(compressed_key_value, latent_norm_gain).astype(jnp.bfloat16)
        own_keys = lax.dot_general(
            latent_to_key_value,
            latent_normed,
            (((0,), (1,)), ((), ())),
            preferred_element_type=jnp.float32,
        ).astype(jnp.bfloat16)
        own_rope = rotated(rope_key.astype(jnp.float32)).T
        own_pack = jnp.concatenate(
            [own_keys[:PLAIN_HEAD_DIM], own_rope, own_keys[PLAIN_HEAD_DIM:]], axis=0
        )
        key_value = to_everyone(own_pack, "ep", z_groups, z_count)
        query_all = to_everyone(query, "ep", x_groups, x_count)
        partial_all = attend(query_all, key_value, (PLAIN_HEAD_DIM + ROPE) ** (-0.5))
        partials = lax.all_to_all(
            partial_all, "ep", 0, 0, tiled=True, axis_index_groups=x_groups
        ).astype(jnp.float32)
        log_total = jnp.sum(partials[:, :, VALUE_HEAD_DIM : VALUE_HEAD_DIM + 3], axis=2, keepdims=True)
        share = jnp.exp2(log_total - jnp.max(log_total, axis=0, keepdims=True))
        attended = jnp.sum(partials[:, :, :VALUE_HEAD_DIM] * share, axis=0) / jnp.sum(share, axis=0)
        everyone = lax.all_gather(attended.astype(jnp.bfloat16).T, "tp", axis=0, tiled=True)
        attention_out = lax.dot_general(
            everyone, out_proj, (((0,), (0,)), ((), ())), preferred_element_type=jnp.float32
        ).astype(jnp.bfloat16)

        halves = arrived.reshape(1, 2, ep_count * capacity // 2, LANES)
        spread = jnp.broadcast_to(halves, (tp_count // 2, *halves.shape[1:]))
        rows_in = lax.all_to_all(
            spread.reshape(tp_count, *halves.shape[2:]), "tp", 0, 0, tiled=True
        )
        partial_out = experts(rows_in, gates, ups, downs)
        groups = lax.all_to_all(partial_out, "tp", 0, 0, tiled=True)
        groups = groups.reshape(tp_count // 2, ep_count, capacity, LANES)
        summed = jnp.sum(groups.astype(jnp.float32), axis=0).astype(jnp.bfloat16)
        returned = lax.all_to_all(summed, "ep", 0, 0, tiled=True)
        expert_out = combine(returned.reshape(ep_count * capacity, LANES), places, route_weight)
        return (attention_out, expert_out)

    return local


def solution(mesh):
    ep_count = mesh.shape["ep"]
    x_count = 4
    return jax.shard_map(
        make_local(ep_count // x_count, x_count, mesh.shape["tp"]),
        mesh=mesh,
        in_specs=(
            P("ep", "tp"),
            P("ep", None),
            P("ep", None),
            P(),
            P(None, "tp"),
            P(None, "tp"),
            P("ep", None),
            P(),
            P("ep", None),
            P("ep", None),
            P("ep", None, "tp"),
            P("ep", None, "tp"),
            P("ep", "tp", None),
        ),
        out_specs=(P("ep", "tp"), P("ep", "tp")),
        check_vma=False,
    )
```

time: 268 us -> 186 us (0.69)
  waiting for transfers between devices: 143 us -> 72.8 us
  blocking collectives: 0 us -> 36.2 us
  local copies, waits for them, and re-layouts: 35.7 us -> 6.32 us
  matrix products: 22.8 us -> 1.26 us
  Pallas kernels: 0 us -> 15.1 us
  between operations: 14.4 us -> 0.96 us
  starting transfers between devices: 40.8 us -> 46.7 us
  other arithmetic: 10 us -> 5.56 us
    all_to_all x5 -> x6, waiting for transfers between devices: 143 us -> 72.8 us  [the longest x1 36.5 us: local(): groups = lax.all_to_all(partial_out, 'tp', 0, 0, tiled=True)]
    dot_general x16 -> x2, matrix products: 22.8 us -> 1.26 us  [the longest x1 0.97 us: local(): lax.dot_general(everyone, out_proj, (((0,), (0,)), ((), ())), preferred_e...]
    all_to_all x0 -> x1, blocking collectives: none -> 19.6 us  [to_everyone(): lax.all_to_all(jnp.broadcast_to(array[None], (count, *array.shape)), axis...]
    all_gather x0 -> x1, blocking collectives: none -> 16.7 us  [local(): lax.all_gather(attended.astype(jnp.bfloat16).T, 'tp', axis=0, tiled=True)]
    pallas_call x0 -> x4, Pallas kernels: none -> 15.1 us  [the longest x1 6.36 us: attend(): kernel_call(body, jax.ShapeDtypeStruct((blocks, rows, LANES), jnp.bfloat1...]
    reshape x6 -> x0, local copies, waits for them, and re-layouts: 10.7 us -> none  [the longest x1 4.39 us: cut_along(): array.reshape(*lengths[:dim], length, lengths[dim] // length, *lengths[di...]
    ppermute x0 -> x3, starting transfers between devices: none -> 6.39 us  [local(): pair.append(lax.ppermute(pair[0], 'tp', partner))]
    gather x2 -> x0, local copies, waits for them, and re-layouts: 5.59 us -> none  [the longest x1 4.26 us: local(): padded[source_table].reshape(ep_count, expert_local, capacity, model_width)]
  transfers between devices with their start and end apart: 6 -> 9, of which waited for: 5 -> 5; matrix products, arithmetic and copies ran while one was open for 12% -> 2% of each run, Pallas kernels for 0% -> 8%
where the time goes in v1:
time: 186 us; the launch traced here: 185 us
  waiting for transfers between devices  72.8 us (39%)
  starting transfers between devices  46.7 us (25%)
  blocking collectives  36.2 us (19%)
  Pallas kernels  15.1 us (8%)
  local copies, waits for them, and re-layouts  6.32 us (3%)
  other arithmetic  5.56 us (3%)
    all_to_all x1, waiting for transfers between devices, local(): groups = lax.all_to_all(partial_out, 'tp', 0, 0, tiled=True)  36.5 us
    all_to_all x1, waiting for transfers between devices, local(): lax.all_to_all(spread.reshape(tp_count, *halves.shape[2:]), 'tp', 0, 0, t...  23.1 us
    all_to_all x1, blocking collectives, to_everyone(): lax.all_to_all(jnp.broadcast_to(array[None], (count, *array.shape)), axis...  19.6 us
    all_gather x1, blocking collectives, local(): lax.all_gather(attended.astype(jnp.bfloat16).T, 'tp', axis=0, tiled=True)  16.7 us
    all_to_all x1, starting transfers between devices, local(): lax.all_to_all(spread.reshape(tp_count, *halves.shape[2:]), 'tp', 0, 0, t...  12.2 us
    all_to_all x1, starting transfers between devices, local(): lax.all_to_all(outgoing.reshape(ep_count, capacity, LANES), 'ep', 0, 0, t...  11 us
    all_to_all x1, waiting for transfers between devices, local(): lax.all_to_all(outgoing.reshape(ep_count, capacity, LANES), 'ep', 0, 0, t...  9.86 us
    ppermute x3, starting transfers between devices, local(): pair.append(lax.ppermute(pair[0], 'tp', partner))  6.39 us
  transfers between devices with their start and end apart: 9, of which 5 were waited for; matrix products, arithmetic and copies ran while one was open for 2% of the time, Pallas kernels for 8%

profile of v1, /device:TPU:1, one launch (start us, length us, event | category | flops | bytes accessed | tf_op | source)
XLA Modules:
  0.0 185.0 jit_solution(17985310096768115938)
XLA Ops:
  4.2 4.8 %all-to-all-start = ((bf16[4,256,128]{2,1,0:T(8,128)(2,1)}), bf16[4,256,128]{2,1,0:T(8,128)(2,1)S(1)}, u32[]{:S(2)}, u32[]{:S(2)}) async-start(bf16[4,256,128]{2,1,0:T(8,128)(2,1)} %broadcast_in_dim.11), calls=%async_computation | async-start | bytes 524288 | tf_op jit(solution)/shard_map/all_to_all | solution.py:43
  9.1 1.1 fusion.1
  10.3 1.5 shard_map.141
  12.1 2.5 %all-to-all-done.query_ref = bf16[4,256,128]{2,1,0:T(8,128)(2,1)S(1)} async-done(((bf16[4,256,128]{2,1,0:T(8,128)(2,1)}), bf16[4,256,128]{2,1,0:T(8,128)(2,1)S(1)}, u32[]{:S(2)}, u32[]{:S(2)}) %all-to-all-start) | async-done | bytes 262176 | tf_op jit(solution)/shard_map/all_to_all | solution.py:43
  14.6 11.0 %all-to-all-start.3 = ((bf16[32,24,128]{2,1,0:T(8,128)(2,1)}), bf16[32,24,128]{2,1,0:T(8,128)(2,1)S(1)}, u32[]{:S(2)}, u32[]{:S(2)}) async-start(bf16[32,24,128]{2,1,0:T(8,128)(2,1)} %bitcast.5), calls=%async_computation.3 | async-start | bytes 393216 | tf_op jit(solution)/shard_map/all_to_all | solution.py:252
  25.7 9.9 %all-to-all-done.3 = bf16[32,24,128]{2,1,0:T(8,128)(2,1)S(1)} async-done(((bf16[32,24,128]{2,1,0:T(8,128)(2,1)}), bf16[32,24,128]{2,1,0:T(8,128)(2,1)S(1)}, u32[]{:S(2)}, u32[]{:S(2)}) %all-to-all-start.3) | async-done | bytes 196640 | tf_op jit(solution)/shard_map/all_to_all | solution.py:252
  35.6 19.6 %all_to_all.35.key_ref = bf16[8,160,256]{2,1,0:T(8,128)(2,1)} all-to-all(bf16[8,160,256]{2,1,0:T(8,128)(2,1)S(1)} %broadcast_in_dim.12), channel_id=1, replica_groups={{0,64,128,192,256,320,384,448},{16,80,144,208,272,336,400,464},{32,96,1..., dimensions={0} | all-to-all | bytes 1310720 | tf_op jit(solution)/shard_map/all_to_all | solution.py:43
  55.1 1.4 broadcast_in_dim.14
  56.6 12.2 %all-to-all-start.4 = ((bf16[16,384,128]{2,1,0:T(8,128)(2,1)}), bf16[16,384,128]{2,1,0:T(8,128)(2,1)}, u32[]{:S(2)}, u32[]{:S(2)}) async-start(bf16[16,384,128]{2,1,0:T(8,128)(2,1)} %bitcast.28), calls=%async_computation.4 | async-start | bytes 3145728 | tf_op jit(solution)/shard_map/all_to_all | solution.py:304
  68.8 2.1 %collective-permute-start = (bf16[2048,256]{1,0:T(8,128)(2,1)S(1)}, bf16[2048,256]{1,0:T(8,128)(2,1)}, u32[]{:S(2)}, u32[]{:S(2)}) collective-permute-start(bf16[2048,256]{1,0:T(8,128)(2,1)S(1)} %bitcast.19), channel_id=1, source_target_pairs={{0,1},{1,0},{2,3},{3,2},{4,5},{5,4},{6,7},{7,6},{8,9},{9,8},{10,11... | collective-permute-start | bytes 3145736 | tf_op jit(solution)/shard_map/ppermute | solution.py:247
  70.9 2.3 %collective-permute-start.1 = (bf16[2048,256]{1,0:T(8,128)(2,1)S(1)}, bf16[2048,256]{1,0:T(8,128)(2,1)}, u32[]{:S(2)}, u32[]{:S(2)}) collective-permute-start(bf16[2048,256]{1,0:T(8,128)(2,1)S(1)} %bitcast.21), channel_id=1, source_target_pairs={{0,1},{1,0},{2,3},{3,2},{4,5},{5,4},{6,7},{7,6},{8,9},{9,8},{10,11... | collective-permute-start | bytes 3145736 | tf_op jit(solution)/shard_map/ppermute | solution.py:247
  73.1 2.1 %collective-permute-start.2 = (bf16[256,2048]{1,0:T(8,128)(2,1)S(1)}, bf16[256,2048]{1,0:T(8,128)(2,1)}, u32[]{:S(2)}, u32[]{:S(2)}) collective-permute-start(bf16[256,2048]{1,0:T(8,128)(2,1)S(1)} %bitcast.23), channel_id=1, source_target_pairs={{0,1},{1,0},{2,3},{3,2},{4,5},{5,4},{6,7},{7,6},{8,9},{9,8},{10,11... | collective-permute-start | bytes 3145736 | tf_op jit(solution)/shard_map/ppermute | solution.py:247
  75.2 1.1 copy-done.5
  77.3 6.4 %shard_map.140 = bf16[4,256,128]{2,1,0:T(8,128)(2,1)S(1)} custom-call(bf16[4,256,128]{2,1,0:T(8,128)(2,1)S(1)} %copy-done.7, bf16[8,160,256]{2,1,0:T(8,128)(2,1)S(1)} %copy-done.5), custom_call_target="tpu_custom_call" | custom-call | flops 2147483648 | tf_op jit(solution)/shard_map/pallas_call | solution.py:146
  84.3 23.1 %all-to-all-done.4.refs_0_ = bf16[16,384,128]{2,1,0:T(8,128)(2,1)} async-done(((bf16[16,384,128]{2,1,0:T(8,128)(2,1)}), bf16[16,384,128]{2,1,0:T(8,128)(2,1)}, u32[]{:S(2)}, u32[]{:S(2)}) %all-to-all-start.4) | async-done | bytes 1572896 | tf_op jit(solution)/shard_map/all_to_all | solution.py:304
  107.4 4.0 %all-to-all-start.2 = ((bf16[4,256,128]{2,1,0:T(8,128)(2,1)}), bf16[4,256,128]{2,1,0:T(8,128)(2,1)}, u32[]{:S(2)}, u32[]{:S(2)}) async-start(bf16[4,256,128]{2,1,0:T(8,128)(2,1)} %copy-done.8), calls=%async_computation.2 | async-start | bytes 524288 | tf_op jit(solution)/shard_map/all_to_all | solution.py:291
  111.5 6.2 %shard_map.142 = bf16[16,384,128]{2,1,0:T(8,128)(2,1)} custom-call(bf16[16,384,128]{2,1,0:T(8,128)(2,1)} %all-to-all-done.4.refs_0_, bf16[2048,256]{1,0:T(8,128)(2,1)S(1)} %bitcast.20, bf16[2048,256]{1,0:T(8,128)(2,1)} %collective-permute-done.refs_2_, bf16[2048,256]{1,0:T(8,128)(2,1)S(1)} %bitcast.22, bf16[2048,256]{1,0:T(8,128)(2,1)} %collective-permute-done.1.refs_4_, ...), custom_call_target="tpu_custom_call" | custom-call | flops 2415919104 | tf_op jit(solution)/shard_map/pallas_call | solution.py:186
  118.5 4.4 %all-to-all-start.5 = ((bf16[16,384,128]{2,1,0:T(8,128)(2,1)}), bf16[16,384,128]{2,1,0:T(8,128)(2,1)S(1)}, u32[]{:S(2)}, u32[]{:S(2)}) async-start(bf16[16,384,128]{2,1,0:T(8,128)(2,1)} %shard_map.142), calls=%async_computation.5 | async-start | bytes 3145728 | tf_op jit(solution)/shard_map/all_to_all | solution.py:308
  123.0 1.0 convert_element_type.49
  124.9 36.5 %all-to-all-done.5 = bf16[16,384,128]{2,1,0:T(8,128)(2,1)S(1)} async-done(((bf16[16,384,128]{2,1,0:T(8,128)(2,1)}), bf16[16,384,128]{2,1,0:T(8,128)(2,1)S(1)}, u32[]{:S(2)}, u32[]{:S(2)}) %all-to-all-start.5) | async-done | bytes 1572896 | tf_op jit(solution)/shard_map/all_to_all | solution.py:308
  162.3 3.9 %all-to-all-start.6 = ((bf16[32,24,128]{2,1,0:T(8,128)(2,1)}), bf16[32,24,128]{2,1,0:T(8,128)(2,1)S(1)}, u32[]{:S(2)}, u32[]{:S(2)}) async-start(bf16[32,24,128]{2,1,0:T(8,128)(2,1)} %reduce_sum.52), calls=%async_computation.6 | async-start | bytes 393216 | tf_op jit(solution)/shard_map/all_to_all | solution.py:311
  166.2 16.7 %all_gather.3 = bf16[1024,256]{1,0:T(8,128)(2,1)S(1)} all-gather(bf16[64,256]{1,0:T(8,128)(2,1)S(1)} %copy.22), channel_id=1, replica_groups=mesh['ep'=32,'tp'=16] {'tp'}, dimensions={0}, use_global_device_ids=true | all-gather | bytes 557056 | tf_op jit(solution)/shard_map/all_gather | solution.py:297
  182.9 1.0 convolution_convert_fusion
  183.9 1.1 shard_map.143
  (60 shorter events, 8.5 us)
Async XLA Ops:
  0.6 182.3 %copy-start = (bf16[1024,128]{1,0:T(8,128)(2,1)S(1)}, bf16[1024,128]{1,0:T(8,128)(2,1)}, u32[]{:S(2)}) copy-start(bf16[1024,128]{1,0:T(8,128)(2,1)} %param.18) | copy-start | bytes 786436
  0.6 11.2 %copy-start.10 = (bf16[256,512]{1,0:T(8,128)(2,1)S(1)}, bf16[256,512]{1,0:T(8,128)(2,1)}, u32[]{:S(2)}) copy-start(bf16[256,512]{1,0:T(8,128)(2,1)} %param.14) | copy-start | bytes 786436
  0.7 9.5 %copy-start.11 = (s32[256,2]{0,1:T(2,128)S(1)}, s32[256,2]{0,1:T(2,128)}, u32[]{:S(2)}) copy-start(s32[256,2]{0,1:T(2,128)} %param.21) | copy-start | bytes 6148
  0.7 9.6 %copy-start.9 = (f32[2048]{0:T(1024)S(1)}, f32[2048]{0:T(1024)}, u32[]{:S(2)}) copy-start(f32[2048]{0:T(1024)} %param.20) | copy-start | bytes 24580
  0.7 9.6 %copy-start.4 = (bf16[256,2048]{1,0:T(8,128)(2,1)S(1)}, bf16[256,2048]{1,0:T(8,128)(2,1)}, u32[]{:S(2)}) copy-start(bf16[256,2048]{1,0:T(8,128)(2,1)} %input_ref.1) | copy-start | bytes 3145732
  0.7 11.1 %copy-start.14 = (f32[512]{0:T(512)S(1)}, f32[512]{0:T(512)}, u32[]{:S(2)}) copy-start(f32[512]{0:T(512)} %param.16) | copy-start | bytes 6148
  0.7 11.1 %copy-start.13 = (bf16[512,128]{1,0:T(8,128)(2,1)S(1)}, bf16[512,128]{1,0:T(8,128)(2,1)}, u32[]{:S(2)}) copy-start(bf16[512,128]{1,0:T(8,128)(2,1)} %param.17) | copy-start | bytes 393220
  4.2 10.4 %all-to-all-start = ((bf16[4,256,128]{2,1,0:T(8,128)(2,1)}), bf16[4,256,128]{2,1,0:T(8,128)(2,1)S(1)}, u32[]{:S(2)}, u32[]{:S(2)}) async-start(bf16[4,256,128]{2,1,0:T(8,128)(2,1)} %broadcast_in_dim.11), calls=%async_computation | async-start | bytes 524288 | tf_op jit(solution)/shard_map/all_to_all | solution.py:43
  14.6 42.0 %copy-start.6 = (bf16[4,256,128]{2,1,0:T(8,128)(2,1)}, bf16[4,256,128]{2,1,0:T(8,128)(2,1)S(1)}, u32[]{:S(2)}) copy-start(bf16[4,256,128]{2,1,0:T(8,128)(2,1)S(1)} %all-to-all-done.query_ref) | copy-start | bytes 786436
  14.6 20.9 %all-to-all-start.3 = ((bf16[32,24,128]{2,1,0:T(8,128)(2,1)}), bf16[32,24,128]{2,1,0:T(8,128)(2,1)S(1)}, u32[]{:S(2)}, u32[]{:S(2)}) async-start(bf16[32,24,128]{2,1,0:T(8,128)(2,1)} %bitcast.5), calls=%async_computation.3 | async-start | bytes 393216 | tf_op jit(solution)/shard_map/all_to_all | solution.py:252
  56.6 12.2 %copy-start.1 = (bf16[1,2048,256]{2,1,0:T(8,128)(2,1)S(1)}, bf16[1,2048,256]{2,1,0:T(8,128)(2,1)}, u32[]{:S(2)}) copy-start(bf16[1,2048,256]{2,1,0:T(8,128)(2,1)} %param.23) | copy-start | bytes 3145732
  56.6 14.3 %copy-start.2 = (bf16[1,2048,256]{2,1,0:T(8,128)(2,1)S(1)}, bf16[1,2048,256]{2,1,0:T(8,128)(2,1)}, u32[]{:S(2)}) copy-start(bf16[1,2048,256]{2,1,0:T(8,128)(2,1)} %param.24) | copy-start | bytes 3145732
  56.6 16.5 %copy-start.3 = (bf16[1,256,2048]{2,1,0:T(8,128)(2,1)S(1)}, bf16[1,256,2048]{2,1,0:T(8,128)(2,1)}, u32[]{:S(2)}) copy-start(bf16[1,256,2048]{2,1,0:T(8,128)(2,1)} %param.25) | copy-start | bytes 3145732
  56.6 50.8 %all-to-all-start.4 = ((bf16[16,384,128]{2,1,0:T(8,128)(2,1)}), bf16[16,384,128]{2,1,0:T(8,128)(2,1)}, u32[]{:S(2)}, u32[]{:S(2)}) async-start(bf16[16,384,128]{2,1,0:T(8,128)(2,1)} %bitcast.28), calls=%async_computation.4 | async-start | bytes 3145728 | tf_op jit(solution)/shard_map/all_to_all | solution.py:304
  68.8 42.7 %collective-permute-start = (bf16[2048,256]{1,0:T(8,128)(2,1)S(1)}, bf16[2048,256]{1,0:T(8,128)(2,1)}, u32[]{:S(2)}, u32[]{:S(2)}) collective-permute-start(bf16[2048,256]{1,0:T(8,128)(2,1)S(1)} %bitcast.19), channel_id=1, source_target_pairs={{0,1},{1,0},{2,3},{3,2},{4,5},{5,4},{6,7},{7,6},{8,9},{9,8},{10,11... | collective-permute-start | bytes 3145736 | tf_op jit(solution)/shard_map/ppermute | solution.py:247
  70.9 40.6 %collective-permute-start.1 = (bf16[2048,256]{1,0:T(8,128)(2,1)S(1)}, bf16[2048,256]{1,0:T(8,128)(2,1)}, u32[]{:S(2)}, u32[]{:S(2)}) collective-permute-start(bf16[2048,256]{1,0:T(8,128)(2,1)S(1)} %bitcast.21), channel_id=1, source_target_pairs={{0,1},{1,0},{2,3},{3,2},{4,5},{5,4},{6,7},{7,6},{8,9},{9,8},{10,11... | collective-permute-start | bytes 3145736 | tf_op jit(solution)/shard_map/ppermute | solution.py:247
  73.1 38.3 %collective-permute-start.2 = (bf16[256,2048]{1,0:T(8,128)(2,1)S(1)}, bf16[256,2048]{1,0:T(8,128)(2,1)}, u32[]{:S(2)}, u32[]{:S(2)}) collective-permute-start(bf16[256,2048]{1,0:T(8,128)(2,1)S(1)} %bitcast.23), channel_id=1, source_target_pairs={{0,1},{1,0},{2,3},{3,2},{4,5},{5,4},{6,7},{7,6},{8,9},{9,8},{10,11... | collective-permute-start | bytes 3145736 | tf_op jit(solution)/shard_map/ppermute | solution.py:247
  75.2 1.1 copy-start.5
  76.3 0.9 copy-start.7
  83.6 0.7 copy-start.8
  107.4 11.1 %all-to-all-start.2 = ((bf16[4,256,128]{2,1,0:T(8,128)(2,1)}), bf16[4,256,128]{2,1,0:T(8,128)(2,1)}, u32[]{:S(2)}, u32[]{:S(2)}) async-start(bf16[4,256,128]{2,1,0:T(8,128)(2,1)} %copy-done.8), calls=%async_computation.2 | async-start | bytes 524288 | tf_op jit(solution)/shard_map/all_to_all | solution.py:291
  117.6 5.2 %copy-start.12 = (f32[256,2]{0,1:T(2,128)S(1)}, f32[256,2]{0,1:T(2,128)}, u32[]{:S(2)}) copy-start(f32[256,2]{0,1:T(2,128)} %param.22) | copy-start | bytes 6148
  118.5 42.9 %all-to-all-start.5 = ((bf16[16,384,128]{2,1,0:T(8,128)(2,1)}), bf16[16,384,128]{2,1,0:T(8,128)(2,1)S(1)}, u32[]{:S(2)}, u32[]{:S(2)}) async-start(bf16[16,384,128]{2,1,0:T(8,128)(2,1)} %shard_map.142), calls=%async_computation.5 | async-start | bytes 3145728 | tf_op jit(solution)/shard_map/all_to_all | solution.py:308
  162.3 21.5 %all-to-all-start.6 = ((bf16[32,24,128]{2,1,0:T(8,128)(2,1)}), bf16[32,24,128]{2,1,0:T(8,128)(2,1)S(1)}, u32[]{:S(2)}, u32[]{:S(2)}) async-start(bf16[32,24,128]{2,1,0:T(8,128)(2,1)} %reduce_sum.52), calls=%async_computation.6 | async-start | bytes 393216 | tf_op jit(solution)/shard_map/all_to_all | solution.py:311

commit v2 on v1

v2 whole, which is shorter than its diff:
```python
import math

import jax
import jax.numpy as jnp
from jax import lax
from jax.experimental import pallas as pl
from jax.experimental.pallas import tpu as pltpu
from jax.sharding import PartitionSpec as P

PLAIN_HEAD_DIM = 64
ROPE = 32
VALUE_HEAD_DIM = 64
LANES = 128

EPSILON = 1e-06
ROPE_BASE_VALUE = 10000.0

VMEM = pl.BlockSpec(memory_space=pltpu.VMEM)
SMEM = pl.BlockSpec(memory_space=pltpu.SMEM)
ANY = pl.BlockSpec(memory_space=pl.ANY)


def kernel_call(body, out_shape, in_specs, out_specs, flops, limit=48):
    return pl.pallas_call(
        body,
        out_shape=out_shape,
        in_specs=in_specs,
        out_specs=out_specs,
        compiler_params=pltpu.CompilerParams(vmem_limit_bytes=limit * 1024 * 1024),
        cost_estimate=pl.CostEstimate(flops=flops, transcendentals=0, bytes_accessed=0),
    )


def rms_scale(values, gain_vector):
    floats = values.astype(jnp.float32)
    return (
        floats
        * lax.rsqrt(jnp.mean(floats * floats, axis=-1, keepdims=True) + EPSILON)
        * gain_vector
    )


def sequenced(array, *earlier):
    def body(array_ref, *refs):
        refs[-1][...] = array_ref[...]

    return kernel_call(
        body,
        jax.ShapeDtypeStruct(array.shape, array.dtype),
        [VMEM] + [ANY] * len(earlier),
        VMEM,
        array.size,
    )(array, *earlier)


LEAD = 8


def unpacked(message):
    blocks = message.shape[0]
    tails = message[:, 2 * LEAD :].reshape(blocks // 2, 2, LEAD, LANES)
    even, odd = tails[:, 0], tails[:, 1]
    upper = lax.broadcasted_iota(jnp.int32, even.shape, 1) < LEAD // 2
    left = jnp.where(upper, even, pltpu.roll(odd, LEAD // 2, 1))
    right = jnp.where(upper, pltpu.roll(even, LEAD // 2, 1), odd)
    return tuple(
        jnp.concatenate([lead.reshape(-1, LANES), tail.reshape(-1, LANES)], axis=0)
        for lead, tail in ((message[:, :LEAD], left), (message[:, LEAD : 2 * LEAD], right))
    )


def packed(left, right):
    blocks = left.shape[0] // (LEAD + LEAD // 2)
    split = blocks * LEAD
    left_tail = left[split:].reshape(blocks // 2, LEAD, LANES)
    right_tail = right[split:].reshape(blocks // 2, LEAD, LANES)
    upper = lax.broadcasted_iota(jnp.int32, left_tail.shape, 1) < LEAD // 2
    even = jnp.where(upper, left_tail, pltpu.roll(right_tail, LEAD // 2, 1))
    odd = jnp.where(upper, pltpu.roll(left_tail, LEAD // 2, 1), right_tail)
    tails = jnp.concatenate([even[:, None], odd[:, None]], axis=1).reshape(blocks, LEAD, LANES)
    return jnp.concatenate(
        [
            left[:split].reshape(blocks, LEAD, LANES),
            right[:split].reshape(blocks, LEAD, LANES),
            tails,
        ],
        axis=1,
    )


def pack_rows(index, moe_input, gain, routes, capacity, expert_total):
    rows, width = moe_input.shape
    places = expert_total * capacity
    half = capacity // 2
    top = routes.shape[1]
    wide = 2 * LANES

    def body(index_ref, input_ref, gain_ref, routes_ref, out_ref, place_ref):
        floats = input_ref[...].astype(jnp.float32)
        scale = lax.rsqrt(jnp.mean(floats * floats, axis=-1, keepdims=True) + EPSILON)
        start = pl.multiple_of(index_ref[0] * wide, wide)
        own = input_ref[:, pl.ds(start, wide)].astype(jnp.float32)
        normed = (own * scale * gain_ref[:, pl.ds(start, wide)]).astype(jnp.bfloat16)
        chosen = routes_ref[...]
        expert = lax.broadcasted_iota(jnp.int32, (rows, expert_total), 1)
        named = [chosen[:, k : k + 1] == expert for k in range(top)]
        either = named[0]
        for other in named[1:]:
            either = either | other
        ones = jnp.where(either, 1.0, 0.0).astype(jnp.bfloat16)
        lower = lax.broadcasted_iota(jnp.int32, (rows, rows), 0) > lax.broadcasted_iota(
            jnp.int32, (rows, rows), 1
        )
        lower = jnp.where(lower, 1.0, 0.0).astype(jnp.bfloat16)
        earlier = jnp.dot(lower, ones, preferred_element_type=jnp.float32)
        slot = earlier - (index_ref[1] * half).astype(jnp.float32)
        valid = (slot >= 0.0) & (slot < float(half))
        base = slot + expert.astype(jnp.float32) * float(capacity) + 1.0
        step = float(LEAD)
        values = (
            jnp.where(slot < step, base, base + step),
            jnp.where(slot < step, base + step, base + step + float(LEAD // 2)),
        )
        slots = lax.broadcasted_iota(jnp.int32, (rows, places), 1)
        total = None
        for side, value in enumerate(values):
            hit = None
            for k in range(top):
                place = jnp.sum(jnp.where(named[k] & valid, value, 0.0), axis=1, keepdims=True)
                place = place.astype(jnp.int32) - 1
                column = side * top + k
                place_ref[:, column : column + 1] = place
                here = slots == place
                hit = here if hit is None else hit | here
            part = lax.dot_general(
                jnp.where(hit, 1.0, 0.0).astype(jnp.bfloat16),
                normed[:, side * LANES : (side + 1) * LANES],
                (((0,), (0,)), ((), ())),
                preferred_element_type=jnp.float32,
            )
            total = part if total is None else total + part
        out_ref[...] = total.astype(jnp.bfloat16)

    return kernel_call(
        body,
        (
            jax.ShapeDtypeStruct((places, LANES), jnp.bfloat16),
            jax.ShapeDtypeStruct((rows, 2 * top), jnp.int32),
        ),
        [SMEM, VMEM, VMEM, VMEM],
        (VMEM, VMEM),
        4 * rows * places * LANES,
    )(index, moe_input, gain, routes)


def fan_out(arrived, copies):
    blocks = arrived.shape[0]
    rows = blocks * (LEAD + LEAD // 2)

    def body(in_ref, out_ref):
        left, right = unpacked(in_ref[...].astype(jnp.float32))
        both = jnp.concatenate([left, right], axis=1).astype(jnp.bfloat16)
        for i in range(copies):
            out_ref[i] = both

    return kernel_call(
        body,
        jax.ShapeDtypeStruct((copies, rows, 2 * LANES), jnp.bfloat16),
        [VMEM],
        VMEM,
        1,
    )(arrived)


def add_up(parts, blocks):
    count = parts.shape[0]

    def body(in_ref, out_ref):
        total = in_ref[0].astype(jnp.float32)
        for i in range(1, count):
            total += in_ref[i].astype(jnp.float32)
        out_ref[...] = packed(total[:, :LANES], total[:, LANES:]).astype(jnp.bfloat16)

    return kernel_call(
        body,
        jax.ShapeDtypeStruct((blocks, 3 * LEAD, LANES), jnp.bfloat16),
        [VMEM],
        VMEM,
        1,
    )(parts)


def attend(index, query, key_value, score_scale):
    blocks, rows, _ = query.shape
    pieces, _, length = key_value.shape
    factor = score_scale * math.log2(math.e)
    first_value = PLAIN_HEAD_DIM + ROPE

    def body(index_ref, query_ref, key_ref, *out_refs):
        for i, out_ref in enumerate(out_refs):
            q = query_ref[(index_ref[0] + i) % blocks]
            scores = [
                jnp.dot(q, key_ref[j, :LANES, :], preferred_element_type=jnp.float32)
                for j in range(pieces)
            ]
            top = scores[0]
            for s in scores[1:]:
                top = jnp.maximum(top, s)
            top = jnp.max(top, axis=1, keepdims=True) * factor
            total = None
            mixed = None
            for j in range(pieces):
                weight = jnp.exp2(scores[j] * factor - top)
                total = weight if total is None else total + weight
                part = lax.dot_general(
                    weight.astype(jnp.bfloat16),
                    key_ref[j, first_value:, :],
                    (((1,), (1,)), ((), ())),
                    preferred_element_type=jnp.float32,
                )
                mixed = part if mixed is None else mixed + part
            total = jnp.sum(total, axis=1, keepdims=True)
            out_ref[:, :VALUE_HEAD_DIM] = (mixed / total).astype(jnp.bfloat16)
            log_total = top + jnp.log2(total)
            high = log_total.astype(jnp.bfloat16).astype(jnp.float32)
            middle = (log_total - high).astype(jnp.bfloat16).astype(jnp.float32)
            low = log_total - high - middle
            lane = lax.broadcasted_iota(jnp.int32, (rows, LANES - VALUE_HEAD_DIM), 1)
            out_ref[:, VALUE_HEAD_DIM:] = jnp.where(
                lane == 0, high, jnp.where(lane == 1, middle, low)
            ).astype(jnp.bfloat16)

    return kernel_call(
        body,
        tuple(jax.ShapeDtypeStruct((rows, LANES), jnp.bfloat16) for _ in range(blocks)),
        [SMEM, VMEM, VMEM],
        (VMEM,) * blocks,
        4 * blocks * rows * pieces * length * 2 * LANES,
    )(index, query, key_value)


def merge(partials):
    rows = partials[0].shape[0]

    def body(*refs):
        out_ref = refs[-1]
        values = [r[...].astype(jnp.float32) for r in refs[:-1]]
        first = VALUE_HEAD_DIM
        logs = [
            v[:, first : first + 1] + v[:, first + 1 : first + 2] + v[:, first + 2 : first + 3]
            for v in values
        ]
        top = logs[0]
        for log in logs[1:]:
            top = jnp.maximum(top, log)
        shares = [jnp.exp2(log - top) for log in logs]
        mixed = values[0] * shares[0]
        total = shares[0]
        for value, share in zip(values[1:], shares[1:]):
            mixed += value * share
            total += share
        out_ref[...] = (mixed / total).T[:VALUE_HEAD_DIM].astype(jnp.bfloat16)

    return kernel_call(
        body,
        jax.ShapeDtypeStruct((VALUE_HEAD_DIM, rows), jnp.bfloat16),
        [VMEM] * len(partials),
        VMEM,
        1,
    )(*partials)


def experts(rows_in, gates, ups, downs):
    blocks, rows, wide = rows_in.shape
    units = gates[0].shape[1]
    count = len(gates)

    def body(*refs):
        rows_ref = refs[0]
        gate_refs, up_refs, down_refs = (refs[1 + k * count : 1 + (k + 1) * count] for k in range(3))
        out_ref = refs[-1]
        hidden = []
        for gate_ref, up_ref in zip(gate_refs, up_refs):
            gate_value = jnp.zeros((rows, units), jnp.float32)
            up_value = jnp.zeros((rows, units), jnp.float32)
            for b in range(blocks):
                part = rows_ref[b]
                span = slice(b * wide, (b + 1) * wide)
                gate_value += jnp.dot(part, gate_ref[span, :], preferred_element_type=jnp.float32)
                up_value += jnp.dot(part, up_ref[span, :], preferred_element_type=jnp.float32)
            silu = gate_value / (1.0 + jnp.exp(-gate_value))
            hidden.append((silu * up_value).astype(jnp.bfloat16))
        for b in range(blocks):
            span = slice(b * wide, (b + 1) * wide)
            total = None
            for h, down_ref in zip(hidden, down_refs):
                part = jnp.dot(h, down_ref[:, span], preferred_element_type=jnp.float32)
                total = part if total is None else total + part
            out_ref[b] = total.astype(jnp.bfloat16)

    return kernel_call(
        body,
        jax.ShapeDtypeStruct((blocks, rows, wide), jnp.bfloat16),
        [VMEM] * (1 + 3 * count),
        VMEM,
        2 * rows * blocks * wide * units * 3 * count,
    )(rows_in, *gates, *ups, *downs)


def combine(index, returned, places, route_weight):
    total, width = returned.shape
    rows, top = route_weight.shape

    def body(index_ref, rows_ref, place_ref, weight_ref, own_ref, other_ref):
        slots = lax.broadcasted_iota(jnp.int32, (rows, total), 1)
        sides = []
        for side in range(2):
            result = None
            for k in range(top):
                column = side * top + k
                select = jnp.where(slots == place_ref[:, column : column + 1], 1.0, 0.0)
                picked = jnp.dot(
                    select.astype(jnp.bfloat16), rows_ref[...], preferred_element_type=jnp.float32
                )
                part = picked * weight_ref[:, k : k + 1]
                result = part if result is None else result + part
            sides.append(result)
        first = index_ref[1] == 0
        own_ref[...] = jnp.where(first, sides[0], sides[1])
        other_ref[...] = jnp.where(first, sides[1], sides[0])

    shape = jax.ShapeDtypeStruct((rows, width), jnp.float32)
    return kernel_call(
        body,
        (shape, shape),
        [SMEM, VMEM, VMEM, VMEM],
        (VMEM, VMEM),
        4 * rows * total * width * top,
    )(index, returned, places, route_weight)


def make_local(z_count, x_count, tp_count):
    cores = 2
    y_count = tp_count // cores
    ep_count = z_count * x_count
    x_groups = [[x_count * z + x for x in range(x_count)] for z in range(z_count)]
    z_groups = [[x_count * z + x for z in range(z_count)] for x in range(x_count)]
    y_groups = [[cores * y + c for y in range(y_count)] for c in range(cores)]
    partner = [(i, i ^ 1) for i in range(tp_count)]

    def local(
        queries,
        compressed_key_value,
        rope_key,
        latent_norm_gain,
        latent_to_key_value,
        out_proj,
        moe_input,
        moe_gain,
        routes,
        route_weight,
        gate_weight,
        up_weight,
        down_weight,
    ):
        row_count = queries.shape[0]
        capacity = 3 * row_count // ep_count
        tp_index = lax.axis_index("tp").astype(jnp.int32)
        ep_index = lax.axis_index("ep").astype(jnp.int32)
        place_index = jnp.stack([tp_index // cores, tp_index % cores])

        outgoing, places = pack_rows(
            place_index, moe_input, moe_gain.reshape(1, -1), routes, capacity, ep_count
        )
        arrived = lax.all_to_all(
            outgoing.reshape(ep_count, capacity, LANES), "ep", 0, 0, tiled=True
        )

        gates, ups, downs = [gate_weight[0]], [up_weight[0]], [down_weight[0]]
        for pair in (gates, ups, downs):
            pair.append(lax.ppermute(pair[0], "tp", partner))

        positions = (ep_index * row_count + jnp.arange(row_count, dtype=jnp.int32)).astype(
            jnp.float32
        )
        half = ROPE // 2
        frequency = ROPE_BASE_VALUE ** (-jnp.arange(half, dtype=jnp.float32) * 2.0 / ROPE)
        angles = positions[:, None] * frequency
        cosine, sine = jnp.cos(angles), jnp.sin(angles)

        def rotated(values):
            first, second = values[:, :half], values[:, half:]
            return jnp.concatenate(
                [first * cosine - second * sine, second * cosine + first * sine], axis=1
            ).astype(jnp.bfloat16)

        query = jnp.concatenate(
            [
                queries[:, :PLAIN_HEAD_DIM],
                rotated(queries[:, PLAIN_HEAD_DIM:].astype(jnp.float32)),
                jnp.zeros((row_count, LANES - PLAIN_HEAD_DIM - ROPE), jnp.bfloat16),
            ],
            axis=1,
        )
        latent_normed = rms_scale(compressed_key_value, latent_norm_gain).astype(jnp.bfloat16)
        own_keys = lax.dot_general(
            latent_to_key_value,
            latent_normed,
            (((0,), (1,)), ((), ())),
            preferred_element_type=jnp.float32,
        ).astype(jnp.bfloat16)
        own_rope = rotated(rope_key.astype(jnp.float32)).T
        own_pack = jnp.concatenate(
            [own_keys[:PLAIN_HEAD_DIM], own_rope, own_keys[PLAIN_HEAD_DIM:]], axis=0
        )
        query_all = lax.all_gather(
            sequenced(query, outgoing), "ep", axis=0, axis_index_groups=x_groups
        )
        key_value = lax.all_gather(
            sequenced(own_pack, arrived), "ep", axis=0, axis_index_groups=z_groups
        )
        partial_all = attend(
            (ep_index % x_count).reshape(1),
            query_all,
            key_value,
            (PLAIN_HEAD_DIM + ROPE) ** (-0.5),
        )

        rows_in = lax.all_to_all(
            fan_out(arrived, y_count), "tp", 0, 0, tiled=True, axis_index_groups=y_groups
        )
        partial_out = experts(rows_in, gates, ups, downs)
        groups = lax.all_to_all(
            partial_out, "tp", 0, 0, tiled=True, axis_index_groups=y_groups
        )

        partials = [sequenced(partial_all[0], partial_out)] + [
            lax.ppermute(
                sequenced(partial_all[i], partial_out),
                "ep",
                [
                    (x_count * z + x, x_count * z + (x + i) % x_count)
                    for z in range(z_count)
                    for x in range(x_count)
                ],
            )
            for i in range(1, x_count)
        ]
        everyone = lax.all_gather(merge(partials), "tp", axis=0, tiled=True)
        attention_out = lax.dot_general(
            everyone, out_proj, (((0,), (0,)), ((), ())), preferred_element_type=jnp.float32
        ).astype(jnp.bfloat16)

        returned = lax.all_to_all(add_up(groups, ep_count), "ep", 0, 0, tiled=True)
        own, other = combine(
            place_index, returned.reshape(ep_count * capacity, LANES), places, route_weight
        )
        expert_out = (own + lax.ppermute(other, "tp", partner)).astype(jnp.bfloat16)
        return (attention_out, expert_out)

    return local


def solution(mesh):
    ep_count = mesh.shape["ep"]
    x_count = 4
    return jax.shard_map(
        make_local(ep_count // x_count, x_count, mesh.shape["tp"]),
        mesh=mesh,
        in_specs=(
            P("ep", "tp"),
            P("ep", None),
            P("ep", None),
            P(),
            P(None, "tp"),
            P(None, "tp"),
            P("ep", None),
            P(),
            P("ep", None),
            P("ep", None),
            P("ep", None, "tp"),
            P("ep", None, "tp"),
            P("ep", "tp", None),
        ),
        out_specs=(P("ep", "tp"), P("ep", "tp")),
        check_vma=False,
    )
```

time: 186 us -> 179 us (0.962)
  blocking collectives: 36.2 us -> 76.9 us
  waiting for transfers between devices: 72.8 us -> 37.5 us
  starting transfers between devices: 46.7 us -> 37.1 us
  other arithmetic: 5.56 us -> 1.16 us
  local copies, waits for them, and re-layouts: 6.32 us -> 9.1 us
    all_to_all x6 -> x3, waiting for transfers between devices: 72.8 us -> 34.1 us  [the longest x1 28.7 us: local(): lax.all_to_all(fan_out(arrived, y_count), 'tp', 0, 0, tiled=True, axis_in...]
    all_gather x1 -> x3, blocking collectives: 16.7 us -> 53.4 us  [the longest x1 22 us: local(): everyone = lax.all_gather(merge(partials), 'tp', axis=0, tiled=True)]
    all_to_all x6 -> x3, starting transfers between devices: 40.3 us -> 15.3 us  [the longest x1 6.95 us: local(): lax.all_to_all(fan_out(arrived, y_count), 'tp', 0, 0, tiled=True, axis_in...]
    ppermute x0 -> x4, starting transfers between devices: none -> 12.6 us  [the longest x3 10.5 us: local(): lax.ppermute(sequenced(partial_all[i], partial_out), 'ep', [(x_count * z...]
    unnamed x32 -> x37, local copies, waits for them, and re-layouts: 3.04 us -> 8.77 us
    all_to_all x1, blocking collectives: 19.6 us -> 23.5 us  [local(): lax.all_to_all(outgoing.reshape(ep_count, capacity, LANES), 'ep', 0, 0, t...]
    ppermute x0 -> x4, waiting for transfers between devices: none -> 2.85 us  [the longest x3 2.66 us: local(): lax.ppermute(sequenced(partial_all[i], partial_out), 'ep', [(x_count * z...]
    ppermute x3, starting transfers between devices: 6.39 us -> 9.14 us  [local(): pair.append(lax.ppermute(pair[0], 'tp', partner))]
  transfers between devices with their start and end apart: 9 -> 10, of which waited for: 5 -> 5; matrix products, arithmetic and copies ran while one was open for 2% -> 1% of each run, Pallas kernels for 8% -> 2%
where the time goes in v2:
time: 179 us
  blocking collectives  76.9 us (43%)
  waiting for transfers between devices  37.5 us (21%)
  starting transfers between devices  37.1 us (21%)
  Pallas kernels  14.6 us (8%)
  local copies, waits for them, and re-layouts  9.1 us (5%)
    all_to_all x1, waiting for transfers between devices, local(): lax.all_to_all(fan_out(arrived, y_count), 'tp', 0, 0, tiled=True, axis_in...  28.7 us
    all_to_all x1, blocking collectives, local(): lax.all_to_all(outgoing.reshape(ep_count, capacity, LANES), 'ep', 0, 0, t...  23.5 us
    all_gather x1, blocking collectives, local(): everyone = lax.all_gather(merge(partials), 'tp', axis=0, tiled=True)  22 us
    all_gather x1, blocking collectives, local(): lax.all_gather(sequenced(own_pack, arrived), 'ep', axis=0, axis_index_gro...  21.5 us
    ppermute x3, starting transfers between devices, local(): lax.ppermute(sequenced(partial_all[i], partial_out), 'ep', [(x_count * z...  10.5 us
    all_gather x1, blocking collectives, local(): lax.all_gather(sequenced(query, outgoing), 'ep', axis=0, axis_index_group...  9.96 us
    ppermute x3, starting transfers between devices, local(): pair.append(lax.ppermute(pair[0], 'tp', partner))  9.14 us
    unnamed x37, local copies, waits for them, and re-layouts  8.77 us
  transfers between devices with their start and end apart: 10, of which 5 were waited for; matrix products, arithmetic and copies ran while one was open for 1% of the time, Pallas kernels for 2%

profile of v2, /device:TPU:1, one launch (start us, length us, event | category | flops | bytes accessed | tf_op | source)
XLA Modules:
  0.0 178.7 jit_solution(7915331081080086289)
XLA Ops:
  1.6 1.2 copy-done.9
  3.5 1.7 shard_map.140
  5.3 23.5 %all_to_all.20.refs_0_.in_ref = bf16[32,24,128]{2,1,0:T(8,128)(2,1)S(1)} all-to-all(bf16[32,24,128]{2,1,0:T(8,128)(2,1)S(1)} %bitcast.24), channel_id=1, replica_groups=mesh['ep'=32,'tp'=16] {'ep'}, dimensions={0} | all-to-all | bytes 393216 | tf_op jit(solution)/shard_map/all_to_all | solution.py:375
  28.8 1.3 shard_map.144
  30.0 7.0 %all-to-all-start.1 = ((bf16[8,384,256]{2,1,0:T(8,128)(2,1)}), bf16[8,384,256]{2,1,0:T(8,128)(2,1)}, u32[]{:S(2)}, u32[]{:S(2)}) async-start(bf16[8,384,256]{2,1,0:T(8,128)(2,1)} %shard_map.144), calls=%async_computation.1 | async-start | bytes 3145728 | tf_op jit(solution)/shard_map/all_to_all | solution.py:429
  37.0 4.8 %collective-permute-start = (bf16[2048,256]{1,0:T(8,128)(2,1)S(1)}, bf16[2048,256]{1,0:T(8,128)(2,1)S(1)}, u32[]{:S(2)}, u32[]{:S(2)}) collective-permute-start(bf16[2048,256]{1,0:T(8,128)(2,1)S(1)} %bitcast.18), channel_id=1, source_target_pairs={{0,1},{1,0},{2,3},{3,2},{4,5},{5,4},{6,7},{7,6},{8,9},{9,8},{10,11... | collective-permute-start | bytes 3145736 | tf_op jit(solution)/shard_map/ppermute | solution.py:381
  41.8 1.9 %collective-permute-start.1 = (bf16[2048,256]{1,0:T(8,128)(2,1)S(1)}, bf16[2048,256]{1,0:T(8,128)(2,1)S(1)}, u32[]{:S(2)}, u32[]{:S(2)}) collective-permute-start(bf16[2048,256]{1,0:T(8,128)(2,1)S(1)} %bitcast.20), channel_id=1, source_target_pairs={{0,1},{1,0},{2,3},{3,2},{4,5},{5,4},{6,7},{7,6},{8,9},{9,8},{10,11... | collective-permute-start | bytes 3145736 | tf_op jit(solution)/shard_map/ppermute | solution.py:381
  43.7 2.4 %collective-permute-start.2 = (bf16[256,2048]{1,0:T(8,128)(2,1)}, bf16[256,2048]{1,0:T(8,128)(2,1)}, u32[]{:S(2)}, u32[]{:S(2)}) collective-permute-start(bf16[256,2048]{1,0:T(8,128)(2,1)} %bitcast.22), channel_id=1, source_target_pairs={{0,1},{1,0},{2,3},{3,2},{4,5},{5,4},{6,7},{7,6},{8,9},{9,8},{10,11... | collective-permute-start | bytes 3145736 | tf_op jit(solution)/shard_map/ppermute | solution.py:381
  48.8 28.7 %all-to-all-done.1.refs_0_ = bf16[8,384,256]{2,1,0:T(8,128)(2,1)} async-done(((bf16[8,384,256]{2,1,0:T(8,128)(2,1)}), bf16[8,384,256]{2,1,0:T(8,128)(2,1)}, u32[]{:S(2)}, u32[]{:S(2)}) %all-to-all-start.1) | async-done | bytes 1572896 | tf_op jit(solution)/shard_map/all_to_all | solution.py:429
  77.5 1.2 copy-done.4
  78.7 1.2 copy-done.6
  81.2 5.5 %shard_map.145.refs_0_ = bf16[8,384,256]{2,1,0:T(8,128)(2,1)} custom-call(bf16[8,384,256]{2,1,0:T(8,128)(2,1)} %all-to-all-done.1.refs_0_, bf16[2048,256]{1,0:T(8,128)(2,1)S(1)} %bitcast.19, bf16[2048,256]{1,0:T(8,128)(2,1)S(1)} %copy-done.6, bf16[2048,256]{1,0:T(8,128)(2,1)S(1)} %bitcast.21, bf16[2048,256]{1,0:T(8,128)(2,1)S(1)} %copy-done.8, ...), custom_call_target="tpu_custom_call" | custom-call | flops 2415919104 | tf_op jit(solution)/shard_map/pallas_call | solution.py:301
  86.7 3.7 %all-to-all-start.2 = ((bf16[8,384,256]{2,1,0:T(8,128)(2,1)}), bf16[8,384,256]{2,1,0:T(8,128)(2,1)S(1)}, u32[]{:S(2)}, u32[]{:S(2)}) async-start(bf16[8,384,256]{2,1,0:T(8,128)(2,1)} %shard_map.145.refs_0_), calls=%async_computation.2 | async-start | bytes 3145728 | tf_op jit(solution)/shard_map/all_to_all | solution.py:433
  91.3 10.0 %all-gather = bf16[1024,128]{1,0:T(8,128)(2,1)S(1)} all-gather(bf16[256,128]{1,0:T(8,128)(2,1)S(1)} %shard_map.141), channel_id=2, replica_groups={{0,16,32,48},{64,80,96,112},{128,144,160,176},{192,208,224,240},{256,27..., dimensions={0}, use_global_device_ids=true | all-gather | bytes 327680 | tf_op jit(solution)/shard_map/all_gather | solution.py:416
  101.8 21.5 %all-gather.1 = bf16[1280,256]{1,0:T(8,128)(2,1)S(1)} all-gather(bf16[160,256]{1,0:T(8,128)(2,1)S(1)} %shard_map.142), channel_id=3, replica_groups={{0,64,128,192,256,320,384,448},{16,80,144,208,272,336,400,464},{32,96,1..., dimensions={0}, use_global_device_ids=true | all-gather | bytes 737280 | tf_op jit(solution)/shard_map/all_gather | solution.py:419
  123.3 5.3 %all-to-all-done.2.in_ref = bf16[8,384,256]{2,1,0:T(8,128)(2,1)S(1)} async-done(((bf16[8,384,256]{2,1,0:T(8,128)(2,1)}), bf16[8,384,256]{2,1,0:T(8,128)(2,1)S(1)}, u32[]{:S(2)}, u32[]{:S(2)}) %all-to-all-start.2) | async-done | bytes 1572896 | tf_op jit(solution)/shard_map/all_to_all | solution.py:433
  129.5 4.7 %all-to-all-start.3 = ((bf16[32,24,128]{2,1,0:T(8,128)(2,1)}), bf16[32,24,128]{2,1,0:T(8,128)(2,1)S(1)}, u32[]{:S(2)}, u32[]{:S(2)}) async-start(bf16[32,24,128]{2,1,0:T(8,128)(2,1)} %shard_map.151), calls=%async_computation.3 | async-start | bytes 393216 | tf_op jit(solution)/shard_map/all_to_all | solution.py:454
  134.2 3.4 %shard_map.143 = (bf16[256,128]{1,0:T(8,128)(2,1)S(1)}, bf16[256,128]{1,0:T(8,128)(2,1)S(1)}, bf16[256,128]{1,0:T(8,128)(2,1)S(1)}, bf16[256,128]{1,0:T(8,128)(2,1)S(1)}) custom-call(s32[1]{0:T(128)} %bitcast.index_ref, bf16[4,256,128]{2,1,0:T(8,128)(2,1)S(1)} %bitcast.26, bf16[8,160,256]{2,1,0:T(8,128)(2,1)S(1)} %bitcast.25), custom_call_target="tpu_custom_call" | custom-call | flops 2147483648 | tf_op jit(solution)/shard_map/pallas_call | solution.py:233
  137.6 3.1 %collective-permute-start.3 = (bf16[256,128]{1,0:T(8,128)(2,1)S(1)}, bf16[256,128]{1,0:T(8,128)(2,1)S(1)}, u32[]{:S(2)}, u32[]{:S(2)}) collective-permute-start(bf16[256,128]{1,0:T(8,128)(2,1)S(1)} %shard_map.147), channel_id=1, source_target_pairs={{0,16},{16,32},{32,48},{48,0},{64,80},{80,96},{96,112},{112,64},{1... | collective-permute-start | bytes 196616 | tf_op jit(solution)/shard_map/ppermute | solution.py:438
  140.8 4.3 %collective-permute-start.4 = (bf16[256,128]{1,0:T(8,128)(2,1)S(1)}, bf16[256,128]{1,0:T(8,128)(2,1)S(1)}, u32[]{:S(2)}, u32[]{:S(2)}) collective-permute-start(bf16[256,128]{1,0:T(8,128)(2,1)S(1)} %shard_map.148), channel_id=1, source_target_pairs={{0,32},{16,48},{32,0},{48,16},{64,96},{80,112},{96,64},{112,80},{1... | collective-permute-start | bytes 196616 | tf_op jit(solution)/shard_map/ppermute | solution.py:438
  145.1 3.1 %collective-permute-start.5 = (bf16[256,128]{1,0:T(8,128)(2,1)S(1)}, bf16[256,128]{1,0:T(8,128)(2,1)S(1)}, u32[]{:S(2)}, u32[]{:S(2)}) collective-permute-start(bf16[256,128]{1,0:T(8,128)(2,1)S(1)} %shard_map.149), channel_id=1, source_target_pairs={{0,48},{16,0},{32,16},{48,32},{64,112},{80,64},{96,80},{112,96},{1... | collective-permute-start | bytes 196616 | tf_op jit(solution)/shard_map/ppermute | solution.py:438
  148.4 2.7 %collective-permute-done.5.refs_3_ = bf16[256,128]{1,0:T(8,128)(2,1)S(1)} collective-permute-done((bf16[256,128]{1,0:T(8,128)(2,1)S(1)}, bf16[256,128]{1,0:T(8,128)(2,1)S(1)}, u32[]{:S(2)}, u32[]{:S(2)}) %collective-permute-start.5) | collective-permute-done | bytes 65568 | tf_op jit(solution)/shard_map/ppermute | solution.py:438
  151.6 22.0 %all_gather.19 = bf16[1024,256]{1,0:T(8,128)(2,1)S(1)} all-gather(bf16[64,256]{1,0:T(8,128)(2,1)S(1)} %shard_map.150), channel_id=1, replica_groups=mesh['ep'=32,'tp'=16] {'tp'}, dimensions={0}, use_global_device_ids=true | all-gather | bytes 557056 | tf_op jit(solution)/shard_map/all_gather | solution.py:449
  174.8 2.1 %collective-permute-start.6 = (f32[256,128]{1,0:T(8,128)S(1)}, f32[256,128]{1,0:T(8,128)S(1)}, u32[]{:S(2)}, u32[]{:S(2)}) collective-permute-start(f32[256,128]{1,0:T(8,128)S(1)} %get-tuple-element.17), channel_id=1, source_target_pairs={{0,1},{1,0},{2,3},{3,2},{4,5},{5,4},{6,7},{7,6},{8,9},{9,8},{10,11... | collective-permute-start | bytes 393224 | tf_op jit(solution)/shard_map/ppermute | solution.py:458
  (71 shorter events, 11.2 us)
Async XLA Ops:
  0.6 176.2 %copy-start = (bf16[1024,128]{1,0:T(8,128)(2,1)S(1)}, bf16[1024,128]{1,0:T(8,128)(2,1)}, u32[]{:S(2)}) copy-start(bf16[1024,128]{1,0:T(8,128)(2,1)} %param.18) | copy-start | bytes 786436
  1.6 1.2 copy-start.9
  30.0 7.0 %copy-start.2 = (bf16[1,2048,256]{2,1,0:T(8,128)(2,1)S(1)}, bf16[1,2048,256]{2,1,0:T(8,128)(2,1)}, u32[]{:S(2)}) copy-start(bf16[1,2048,256]{2,1,0:T(8,128)(2,1)} %param.23) | copy-start | bytes 3145732
  30.0 11.8 %copy-start.3 = (bf16[1,2048,256]{2,1,0:T(8,128)(2,1)S(1)}, bf16[1,2048,256]{2,1,0:T(8,128)(2,1)}, u32[]{:S(2)}) copy-start(bf16[1,2048,256]{2,1,0:T(8,128)(2,1)} %param.24) | copy-start | bytes 3145732
  30.0 47.5 %all-to-all-start.1 = ((bf16[8,384,256]{2,1,0:T(8,128)(2,1)}), bf16[8,384,256]{2,1,0:T(8,128)(2,1)}, u32[]{:S(2)}, u32[]{:S(2)}) async-start(bf16[8,384,256]{2,1,0:T(8,128)(2,1)} %shard_map.144), calls=%async_computation.1 | async-start | bytes 3145728 | tf_op jit(solution)/shard_map/all_to_all | solution.py:429
  37.0 9.2 %collective-permute-start = (bf16[2048,256]{1,0:T(8,128)(2,1)S(1)}, bf16[2048,256]{1,0:T(8,128)(2,1)S(1)}, u32[]{:S(2)}, u32[]{:S(2)}) collective-permute-start(bf16[2048,256]{1,0:T(8,128)(2,1)S(1)} %bitcast.18), channel_id=1, source_target_pairs={{0,1},{1,0},{2,3},{3,2},{4,5},{5,4},{6,7},{7,6},{8,9},{9,8},{10,11... | collective-permute-start | bytes 3145736 | tf_op jit(solution)/shard_map/ppermute | solution.py:381
  41.8 5.4 %collective-permute-start.1 = (bf16[2048,256]{1,0:T(8,128)(2,1)S(1)}, bf16[2048,256]{1,0:T(8,128)(2,1)S(1)}, u32[]{:S(2)}, u32[]{:S(2)}) collective-permute-start(bf16[2048,256]{1,0:T(8,128)(2,1)S(1)} %bitcast.20), channel_id=1, source_target_pairs={{0,1},{1,0},{2,3},{3,2},{4,5},{5,4},{6,7},{7,6},{8,9},{9,8},{10,11... | collective-permute-start | bytes 3145736 | tf_op jit(solution)/shard_map/ppermute | solution.py:381
  43.7 5.0 %collective-permute-start.2 = (bf16[256,2048]{1,0:T(8,128)(2,1)}, bf16[256,2048]{1,0:T(8,128)(2,1)}, u32[]{:S(2)}, u32[]{:S(2)}) collective-permute-start(bf16[256,2048]{1,0:T(8,128)(2,1)} %bitcast.22), channel_id=1, source_target_pairs={{0,1},{1,0},{2,3},{3,2},{4,5},{5,4},{6,7},{7,6},{8,9},{9,8},{10,11... | collective-permute-start | bytes 3145736 | tf_op jit(solution)/shard_map/ppermute | solution.py:381
  77.5 1.2 copy-start.4
  78.7 1.2 copy-start.6
  86.7 3.8 %copy-start.13 = (bf16[256,32]{0,1:T(8,128)(2,1)S(1)}, bf16[256,32]{0,1:T(8,128)(2,1)}, u32[]{:S(2)}) copy-start(bf16[256,32]{0,1:T(8,128)(2,1)} %param.15) | copy-start | bytes 49156
  86.7 3.8 %copy-start.12 = (bf16[256,96]{0,1:T(8,128)(2,1)S(1)}, bf16[256,96]{0,1:T(8,128)(2,1)}, u32[]{:S(2)}) copy-start(bf16[256,96]{0,1:T(8,128)(2,1)} %param.13) | copy-start | bytes 147460
  86.7 4.2 %slice-start = ((bf16[256,96]{0,1:T(8,128)(2,1)}), bf16[256,64]{0,1:T(8,128)(2,1)S(1)}, s32[]{:S(2)}) async-start(bf16[256,96]{0,1:T(8,128)(2,1)} %param.13), calls=%async_computation.4 | async-start | bytes 65536 | tf_op jit(solution)/shard_map/slice | solution.py:399
  86.7 14.6 %copy-start.11 = (bf16[256,512]{1,0:T(8,128)(2,1)S(1)}, bf16[256,512]{1,0:T(8,128)(2,1)}, u32[]{:S(2)}) copy-start(bf16[256,512]{1,0:T(8,128)(2,1)} %param.14) | copy-start | bytes 786436
  86.7 41.9 %all-to-all-start.2 = ((bf16[8,384,256]{2,1,0:T(8,128)(2,1)}), bf16[8,384,256]{2,1,0:T(8,128)(2,1)S(1)}, u32[]{:S(2)}, u32[]{:S(2)}) async-start(bf16[8,384,256]{2,1,0:T(8,128)(2,1)} %shard_map.145.refs_0_), calls=%async_computation.2 | async-start | bytes 3145728 | tf_op jit(solution)/shard_map/all_to_all | solution.py:433
  90.5 11.0 %copy-start.15 = (bf16[512,128]{1,0:T(8,128)(2,1)S(1)}, bf16[512,128]{1,0:T(8,128)(2,1)}, u32[]{:S(2)}) copy-start(bf16[512,128]{1,0:T(8,128)(2,1)} %param.17) | copy-start | bytes 393220
  90.5 11.0 %copy-start.16 = (f32[512]{0:T(512)S(1)}, f32[512]{0:T(512)}, u32[]{:S(2)}) copy-start(f32[512]{0:T(512)} %param.16) | copy-start | bytes 6148
  129.5 44.1 %all-to-all-start.3 = ((bf16[32,24,128]{2,1,0:T(8,128)(2,1)}), bf16[32,24,128]{2,1,0:T(8,128)(2,1)S(1)}, u32[]{:S(2)}, u32[]{:S(2)}) async-start(bf16[32,24,128]{2,1,0:T(8,128)(2,1)} %shard_map.151), calls=%async_computation.3 | async-start | bytes 393216 | tf_op jit(solution)/shard_map/all_to_all | solution.py:454
  134.2 3.5 %copy-start.1 = (bf16[8,384,256]{2,1,0:T(8,128)(2,1)S(1)}, bf16[8,384,256]{2,1,0:T(8,128)(2,1)}, u32[]{:S(2)}) copy-start(bf16[8,384,256]{2,1,0:T(8,128)(2,1)} %shard_map.145.refs_0_) | copy-start | bytes 4718596
  137.6 10.8 %collective-permute-start.3 = (bf16[256,128]{1,0:T(8,128)(2,1)S(1)}, bf16[256,128]{1,0:T(8,128)(2,1)S(1)}, u32[]{:S(2)}, u32[]{:S(2)}) collective-permute-start(bf16[256,128]{1,0:T(8,128)(2,1)S(1)} %shard_map.147), channel_id=1, source_target_pairs={{0,16},{16,32},{32,48},{48,0},{64,80},{80,96},{96,112},{112,64},{1... | collective-permute-start | bytes 196616 | tf_op jit(solution)/shard_map/ppermute | solution.py:438
  140.8 7.5 %copy-start.14 = (f32[256,2]{0,1:T(2,128)S(1)}, f32[256,2]{0,1:T(2,128)}, u32[]{:S(2)}) copy-start(f32[256,2]{0,1:T(2,128)} %param.22) | copy-start | bytes 6148
  140.8 7.6 %collective-permute-start.4 = (bf16[256,128]{1,0:T(8,128)(2,1)S(1)}, bf16[256,128]{1,0:T(8,128)(2,1)S(1)}, u32[]{:S(2)}, u32[]{:S(2)}) collective-permute-start(bf16[256,128]{1,0:T(8,128)(2,1)S(1)} %shard_map.148), channel_id=1, source_target_pairs={{0,32},{16,48},{32,0},{48,16},{64,96},{80,112},{96,64},{112,80},{1... | collective-permute-start | bytes 196616 | tf_op jit(solution)/shard_map/ppermute | solution.py:438
  145.1 5.9 %collective-permute-start.5 = (bf16[256,128]{1,0:T(8,128)(2,1)S(1)}, bf16[256,128]{1,0:T(8,128)(2,1)S(1)}, u32[]{:S(2)}, u32[]{:S(2)}) collective-permute-start(bf16[256,128]{1,0:T(8,128)(2,1)S(1)} %shard_map.149), channel_id=1, source_target_pairs={{0,48},{16,0},{32,16},{48,32},{64,112},{80,64},{96,80},{112,96},{1... | collective-permute-start | bytes 196616 | tf_op jit(solution)/shard_map/ppermute | solution.py:438
  174.8 3.2 %collective-permute-start.6 = (f32[256,128]{1,0:T(8,128)S(1)}, f32[256,128]{1,0:T(8,128)S(1)}, u32[]{:S(2)}, u32[]{:S(2)}) collective-permute-start(f32[256,128]{1,0:T(8,128)S(1)} %get-tuple-element.17), channel_id=1, source_target_pairs={{0,1},{1,0},{2,3},{3,2},{4,5},{5,4},{6,7},{7,6},{8,9},{9,8},{10,11... | collective-permute-start | bytes 393224 | tf_op jit(solution)/shard_map/ppermute | solution.py:458
  (4 other events, 4.0 us)

commit v3 on v2

--- a/solution.py
+++ b/solution.py
@@ -98,9 +98,7 @@
     def body(index_ref, input_ref, gain_ref, routes_ref, out_ref, place_ref):
         floats = input_ref[...].astype(jnp.float32)
         scale = lax.rsqrt(jnp.mean(floats * floats, axis=-1, keepdims=True) + EPSILON)
-        start = pl.multiple_of(index_ref[0] * wide, wide)
-        own = input_ref[:, pl.ds(start, wide)].astype(jnp.float32)
-        normed = (own * scale * gain_ref[:, pl.ds(start, wide)]).astype(jnp.bfloat16)
+        normed = (floats * scale * gain_ref[...]).astype(jnp.bfloat16)
         chosen = routes_ref[...]
         expert = lax.broadcasted_iota(jnp.int32, (rows, expert_total), 1)
         named = [chosen[:, k : k + 1] == expert for k in range(top)]
@@ -122,7 +120,7 @@
             jnp.where(slot < step, base + step, base + step + float(LEAD // 2)),
         )
         slots = lax.broadcasted_iota(jnp.int32, (rows, places), 1)
-        total = None
+        selects = []
         for side, value in enumerate(values):
             hit = None
             for k in range(top):
@@ -132,50 +130,37 @@
                 place_ref[:, column : column + 1] = place
                 here = slots == place
                 hit = here if hit is None else hit | here
-            part = lax.dot_general(
-                jnp.where(hit, 1.0, 0.0).astype(jnp.bfloat16),
-                normed[:, side * LANES : (side + 1) * LANES],
-                (((0,), (0,)), ((), ())),
-                preferred_element_type=jnp.float32,
-            )
-            total = part if total is None else total + part
-        out_ref[...] = total.astype(jnp.bfloat16)
+            selects.append(jnp.where(hit, 1.0, 0.0).astype(jnp.bfloat16))
+        for b in range(width // wide):
+            total = None
+            for side, select in enumerate(selects):
+                first = b * wide + side * LANES
+                part = lax.dot_general(
+                    select,
+                    normed[:, first : first + LANES],
+                    (((0,), (0,)), ((), ())),
+                    preferred_element_type=jnp.float32,
+                )
+                total = part if total is None else total + part
+            out_ref[:, b] = total.reshape(expert_total, capacity, LANES).astype(jnp.bfloat16)
 
     return kernel_call(
         body,
         (
-            jax.ShapeDtypeStruct((places, LANES), jnp.bfloat16),
+            jax.ShapeDtypeStruct((expert_total, width // wide, capacity, LANES), jnp.bfloat16),
             jax.ShapeDtypeStruct((rows, 2 * top), jnp.int32),
         ),
         [SMEM, VMEM, VMEM, VMEM],
         (VMEM, VMEM),
-        4 * rows * places * LANES,
+        2 * rows * places * width,
     )(index, moe_input, gain, routes)
 
 
-def fan_out(arrived, copies):
-    blocks = arrived.shape[0]
-    rows = blocks * (LEAD + LEAD // 2)
-
-    def body(in_ref, out_ref):
-        left, right = unpacked(in_ref[...].astype(jnp.float32))
-        both = jnp.concatenate([left, right], axis=1).astype(jnp.bfloat16)
-        for i in range(copies):
-            out_ref[i] = both
-
-    return kernel_call(
-        body,
-        jax.ShapeDtypeStruct((copies, rows, 2 * LANES), jnp.bfloat16),
-        [VMEM],
-        VMEM,
-        1,
-    )(arrived)
-
-
-def add_up(parts, blocks):
+def add_up(parts, blocks, *earlier):
     count = parts.shape[0]
 
-    def body(in_ref, out_ref):
+    def body(in_ref, *refs):
+        out_ref = refs[-1]
         total = in_ref[0].astype(jnp.float32)
         for i in range(1, count):
             total += in_ref[i].astype(jnp.float32)
@@ -184,10 +169,10 @@
     return kernel_call(
         body,
         jax.ShapeDtypeStruct((blocks, 3 * LEAD, LANES), jnp.bfloat16),
-        [VMEM],
+        [VMEM] + [ANY] * len(earlier),
         VMEM,
         1,
-    )(parts)
+    )(parts, *earlier)
 
 
 def attend(index, query, key_value, score_scale):
@@ -270,8 +255,10 @@
     )(*partials)
 
 
-def experts(rows_in, gates, ups, downs):
-    blocks, rows, wide = rows_in.shape
+def experts(messages, gates, ups, downs, *earlier):
+    sources, blocks, _, _ = messages.shape
+    rows = sources * (LEAD + LEAD // 2)
+    wide = 2 * LANES
     units = gates[0].shape[1]
     count = len(gates)
 
@@ -280,11 +267,14 @@
         gate_refs, up_refs, down_refs = (refs[1 + k * count : 1 + (k + 1) * count] for k in range(3))
         out_ref = refs[-1]
         hidden = []
+        parts = [
+            jnp.concatenate(unpacked(rows_ref[:, b].astype(jnp.float32)), axis=1).astype(jnp.bfloat16)
+            for b in range(blocks)
+        ]
         for gate_ref, up_ref in zip(gate_refs, up_refs):
             gate_value = jnp.zeros((rows, units), jnp.float32)
             up_value = jnp.zeros((rows, units), jnp.float32)
-            for b in range(blocks):
-                part = rows_ref[b]
+            for b, part in enumerate(parts):
                 span = slice(b * wide, (b + 1) * wide)
                 gate_value += jnp.dot(part, gate_ref[span, :], preferred_element_type=jnp.float32)
                 up_value += jnp.dot(part, up_ref[span, :], preferred_element_type=jnp.float32)
@@ -301,10 +291,10 @@
     return kernel_call(
         body,
         jax.ShapeDtypeStruct((blocks, rows, wide), jnp.bfloat16),
-        [VMEM] * (1 + 3 * count),
+        [VMEM] * (1 + 3 * count) + [ANY] * len(earlier),
         VMEM,
         2 * rows * blocks * wide * units * 3 * count,
-    )(rows_in, *gates, *ups, *downs)
+    )(messages, *gates, *ups, *downs, *earlier)
 
 
 def combine(index, returned, places, route_weight):
@@ -372,9 +362,7 @@
         outgoing, places = pack_rows(
             place_index, moe_input, moe_gain.reshape(1, -1), routes, capacity, ep_count
         )
-        arrived = lax.all_to_all(
-            outgoing.reshape(ep_count, capacity, LANES), "ep", 0, 0, tiled=True
-        )
+        arrived = lax.all_to_all(outgoing, "ep", 0, 0, tiled=True)
 
         gates, ups, downs = [gate_weight[0]], [up_weight[0]], [down_weight[0]]
         for pair in (gates, ups, downs):
@@ -413,11 +401,17 @@
         own_pack = jnp.concatenate(
             [own_keys[:PLAIN_HEAD_DIM], own_rope, own_keys[PLAIN_HEAD_DIM:]], axis=0
         )
+        key_value = lax.all_gather(
+            sequenced(own_pack, outgoing), "ep", axis=0, axis_index_groups=z_groups
+        )
+
+        partial_out = experts(arrived, gates, ups, downs, key_value)
+        groups = lax.all_to_all(
+            partial_out, "tp", 0, 0, tiled=True, axis_index_groups=y_groups
+        )
+
         query_all = lax.all_gather(
-            sequenced(query, outgoing), "ep", axis=0, axis_index_groups=x_groups
-        )
-        key_value = lax.all_gather(
-            sequenced(own_pack, arrived), "ep", axis=0, axis_index_groups=z_groups
+            sequenced(query, partial_out), "ep", axis=0, axis_index_groups=x_groups
         )
         partial_all = attend(
             (ep_index % x_count).reshape(1),
@@ -425,18 +419,9 @@
             key_value,
             (PLAIN_HEAD_DIM + ROPE) ** (-0.5),
         )
-
-        rows_in = lax.all_to_all(
-            fan_out(arrived, y_count), "tp", 0, 0, tiled=True, axis_index_groups=y_groups
-        )
-        partial_out = experts(rows_in, gates, ups, downs)
-        groups = lax.all_to_all(
-            partial_out, "tp", 0, 0, tiled=True, axis_index_groups=y_groups
-        )
-
-        partials = [sequenced(partial_all[0], partial_out)] + [
+        partials = [partial_all[0]] + [
             lax.ppermute(
-                sequenced(partial_all[i], partial_out),
+                partial_all[i],
                 "ep",
                 [
                     (x_count * z + x, x_count * z + (x + i) % x_count)
@@ -446,12 +431,14 @@
             )
             for i in range(1, x_count)
         ]
-        everyone = lax.all_gather(merge(partials), "tp", axis=0, tiled=True)
+        attended = merge(partials)
+        summed = add_up(groups, ep_count, attended)
+        everyone = lax.all_gather(sequenced(attended, summed), "tp", axis=0, tiled=True)
         attention_out = lax.dot_general(
             everyone, out_proj, (((0,), (0,)), ((), ())), preferred_element_type=jnp.float32
         ).astype(jnp.bfloat16)
 
-        returned = lax.all_to_all(add_up(groups, ep_count), "ep", 0, 0, tiled=True)
+        returned = lax.all_to_all(summed, "ep", 0, 0, tiled=True)
         own, other = combine(
             place_index, returned.reshape(ep_count * capacity, LANES), places, route_weight
         )

time: 179 us -> 163 us (0.911)
  waiting for transfers between devices: 37.5 us -> 7.22 us
  starting transfers between devices: 37.1 us -> 47.3 us
  other arithmetic: 1.16 us -> 3.87 us
  Pallas kernels: 14.6 us -> 17 us
    all_to_all x2, waiting for transfers between devices: 28.7 us -> 0.01 us  [the longest x1 0.01 us: local(): returned = lax.all_to_all(summed, 'ep', 0, 0, tiled=True)]
    all_gather x3, blocking collectives: 53.4 us -> 77.1 us  [the longest x1 42.8 us: local(): lax.all_gather(sequenced(own_pack, outgoing), 'ep', axis=0, axis_index_gr...]
    all_to_all x1 -> x0, blocking collectives: 23.5 us -> none  [local(): lax.all_to_all(outgoing.reshape(ep_count, capacity, LANES), 'ep', 0, 0, t...]
    all_to_all x2, starting transfers between devices: 11.6 us -> 22 us  [the longest x1 14 us: local(): arrived = lax.all_to_all(outgoing, 'ep', 0, 0, tiled=True)]
    all_to_all x1, starting transfers between devices: 3.72 us -> 6.95 us  [local(): lax.all_to_all(partial_out, 'tp', 0, 0, tiled=True, axis_index_groups=y_g...]
    unnamed x37, local copies, waits for them, and re-layouts: 8.77 us -> 6.81 us
    ppermute x3, starting transfers between devices: 9.14 us -> 7.19 us  [local(): pair.append(lax.ppermute(pair[0], 'tp', partner))]
    pallas_call x2 -> x1, Pallas kernels: 3.01 us -> 4.35 us  [pack_rows(): kernel_call(body, (jax.ShapeDtypeStruct((expert_total, width // wide, cap...]
  transfers between devices with their start and end apart: 10 -> 10, of which waited for: 5 -> 4; matrix products, arithmetic and copies ran while one was open for 1% -> 5% of each run, Pallas kernels for 2% -> 3%
where the time goes in v3:
time: 163 us; the launch traced here: 162 us
  blocking collectives  77.1 us (47%)
  starting transfers between devices  47.3 us (29%)
  Pallas kernels  17 us (10%)
  local copies, waits for them, and re-layouts  7.66 us (5%)
  waiting for transfers between devices  7.22 us (4%)
  other arithmetic  3.87 us (2%)
    all_gather x1, blocking collectives, local(): lax.all_gather(sequenced(own_pack, outgoing), 'ep', axis=0, axis_index_gr...  42.8 us
    all_gather x1, blocking collectives, local(): lax.all_gather(sequenced(attended, summed), 'tp', axis=0, tiled=True)  24.4 us
    all_to_all x1, starting transfers between devices, local(): arrived = lax.all_to_all(outgoing, 'ep', 0, 0, tiled=True)  14 us
    all_gather x1, blocking collectives, local(): lax.all_gather(sequenced(query, partial_out), 'ep', axis=0, axis_index_gr...  9.89 us
    ppermute x3, starting transfers between devices, local(): lax.ppermute(partial_all[i], 'ep', [(x_count * z + x, x_count * z + (x +...  9.02 us
    all_to_all x1, starting transfers between devices, local(): returned = lax.all_to_all(summed, 'ep', 0, 0, tiled=True)  8.08 us
    ppermute x3, starting transfers between devices, local(): pair.append(lax.ppermute(pair[0], 'tp', partner))  7.19 us
    all_to_all x1, starting transfers between devices, local(): lax.all_to_all(partial_out, 'tp', 0, 0, tiled=True, axis_index_groups=y_g...  6.95 us
  transfers between devices with their start and end apart: 10, of which 4 were waited for; matrix products, arithmetic and copies ran while one was open for 5% of the time, Pallas kernels for 3%

profile of v3, /device:TPU:1, one launch (start us, length us, event | category | flops | bytes accessed | tf_op | source)
XLA Modules:
  0.0 162.5 jit_solution(4600221881165230816)
XLA Ops:
  1.6 1.2 copy-done.6
  3.5 4.3 %shard_map.140 = (bf16[32,8,24,128]{3,2,1,0:T(8,128)(2,1)}, s32[256,4]{1,0:T(8,128)S(1)}) custom-call(s32[2]{0:T(128)S(1)} %pad_add_fusion.index_ref, bf16[256,2048]{1,0:T(8,128)(2,1)S(1)} %copy-done.6, f32[1,2048]{1,0:T(1,128)S(1)} %bitcast.25, s32[256,2]{1,0:T(8,128)S(1)} %copy.31.routes_ref), custom_call_target="tpu_custom_call" | custom-call | flops 805306368 | tf_op jit(solution)/shard_map/pallas_call | solution.py:147
  8.6 14.0 %all-to-all-start = ((bf16[32,8,24,128]{3,2,1,0:T(8,128)(2,1)}), bf16[32,8,24,128]{3,2,1,0:T(8,128)(2,1)}, u32[]{:S(2)}, u32[]{:S(2)}) async-start(bf16[32,8,24,128]{3,2,1,0:T(8,128)(2,1)} %get-tuple-element.10.refs_0_), calls=%async_computation | async-start | bytes 3145728 | tf_op jit(solution)/shard_map/all_to_all | solution.py:365
  22.6 2.9 %collective-permute-start = (bf16[2048,256]{1,0:T(8,128)(2,1)S(1)}, bf16[2048,256]{1,0:T(8,128)(2,1)}, u32[]{:S(2)}, u32[]{:S(2)}) collective-permute-start(bf16[2048,256]{1,0:T(8,128)(2,1)S(1)} %bitcast.19), channel_id=1, source_target_pairs={{0,1},{1,0},{2,3},{3,2},{4,5},{5,4},{6,7},{7,6},{8,9},{9,8},{10,11... | collective-permute-start | bytes 3145736 | tf_op jit(solution)/shard_map/ppermute | solution.py:369
  25.4 1.9 %collective-permute-start.1 = (bf16[2048,256]{1,0:T(8,128)(2,1)S(1)}, bf16[2048,256]{1,0:T(8,128)(2,1)}, u32[]{:S(2)}, u32[]{:S(2)}) collective-permute-start(bf16[2048,256]{1,0:T(8,128)(2,1)S(1)} %bitcast.21), channel_id=1, source_target_pairs={{0,1},{1,0},{2,3},{3,2},{4,5},{5,4},{6,7},{7,6},{8,9},{9,8},{10,11... | collective-permute-start | bytes 3145736 | tf_op jit(solution)/shard_map/ppermute | solution.py:369
  27.4 2.4 %collective-permute-start.2 = (bf16[256,2048]{1,0:T(8,128)(2,1)}, bf16[256,2048]{1,0:T(8,128)(2,1)}, u32[]{:S(2)}, u32[]{:S(2)}) collective-permute-start(bf16[256,2048]{1,0:T(8,128)(2,1)} %bitcast.6.refs_5_), channel_id=1, source_target_pairs={{0,1},{1,0},{2,3},{3,2},{4,5},{5,4},{6,7},{7,6},{8,9},{9,8},{10,11... | collective-permute-start | bytes 3145736 | tf_op jit(solution)/shard_map/ppermute | solution.py:369
  31.2 42.8 %all-gather = bf16[1280,256]{1,0:T(8,128)(2,1)S(1)} all-gather(bf16[160,256]{1,0:T(8,128)(2,1)S(1)} %shard_map.141), channel_id=2, replica_groups={{0,64,128,192,256,320,384,448},{16,80,144,208,272,336,400,464},{32,96,1..., dimensions={0}, use_global_device_ids=true | all-gather | bytes 737280 | tf_op jit(solution)/shard_map/all_gather | solution.py:404
  74.1 6.5 %shard_map.142.refs_0_ = bf16[8,384,256]{2,1,0:T(8,128)(2,1)} custom-call(bf16[32,8,24,128]{3,2,1,0:T(8,128)(2,1)} %all-to-all-done.refs_0_, bf16[2048,256]{1,0:T(8,128)(2,1)S(1)} %bitcast.20, bf16[2048,256]{1,0:T(8,128)(2,1)} %collective-permute-done.refs_2_, bf16[2048,256]{1,0:T(8,128)(2,1)S(1)} %bitcast.22, ...), custom_call_target="tpu_custom_call" | custom-call | flops 2415919104 | tf_op jit(solution)/shard_map/pallas_call | solution.py:291
  81.5 7.0 %all-to-all-start.1 = ((bf16[8,384,256]{2,1,0:T(8,128)(2,1)}), bf16[8,384,256]{2,1,0:T(8,128)(2,1)S(1)}, u32[]{:S(2)}, u32[]{:S(2)}) async-start(bf16[8,384,256]{2,1,0:T(8,128)(2,1)} %shard_map.142.refs_0_), calls=%async_computation.1 | async-start | bytes 3145728 | tf_op jit(solution)/shard_map/all_to_all | solution.py:409
  90.6 1.5 copy.36
  92.8 1.0 maximum_maximum_fusion.array_ref
  93.8 9.9 %all-gather.1 = bf16[1024,128]{1,0:T(8,128)(2,1)S(1)} all-gather(bf16[256,128]{1,0:T(8,128)(2,1)S(1)} %shard_map.143), channel_id=3, replica_groups={{0,16,32,48},{64,80,96,112},{128,144,160,176},{192,208,224,240},{256,27..., dimensions={0}, use_global_device_ids=true | all-gather | bytes 327680 | tf_op jit(solution)/shard_map/all_gather | solution.py:413
  103.7 3.5 %shard_map.144 = (bf16[256,128]{1,0:T(8,128)(2,1)S(1)}, bf16[256,128]{1,0:T(8,128)(2,1)S(1)}, bf16[256,128]{1,0:T(8,128)(2,1)S(1)}, bf16[256,128]{1,0:T(8,128)(2,1)S(1)}) custom-call(s32[1]{0:T(128)} %bitcast.index_ref, bf16[4,256,128]{2,1,0:T(8,128)(2,1)S(1)} %bitcast.23, bf16[8,160,256]{2,1,0:T(8,128)(2,1)S(1)} %bitcast.18), custom_call_target="tpu_custom_call" | custom-call | flops 2147483648 | tf_op jit(solution)/shard_map/pallas_call | solution.py:218
  107.3 2.8 %collective-permute-start.3 = (bf16[256,128]{1,0:T(8,128)(2,1)S(1)}, bf16[256,128]{1,0:T(8,128)(2,1)S(1)}, u32[]{:S(2)}, u32[]{:S(2)}) collective-permute-start(bf16[256,128]{1,0:T(8,128)(2,1)S(1)} %get-tuple-element.12), channel_id=1, source_target_pairs={{0,16},{16,32},{32,48},{48,0},{64,80},{80,96},{96,112},{112,64},{1... | collective-permute-start | bytes 196616 | tf_op jit(solution)/shard_map/ppermute | solution.py:423
  110.1 4.3 %collective-permute-start.4 = (bf16[256,128]{1,0:T(8,128)(2,1)S(1)}, bf16[256,128]{1,0:T(8,128)(2,1)S(1)}, u32[]{:S(2)}, u32[]{:S(2)}) collective-permute-start(bf16[256,128]{1,0:T(8,128)(2,1)S(1)} %get-tuple-element.13), channel_id=1, source_target_pairs={{0,32},{16,48},{32,0},{48,16},{64,96},{80,112},{96,64},{112,80},{1... | collective-permute-start | bytes 196616 | tf_op jit(solution)/shard_map/ppermute | solution.py:423
  114.4 1.9 %collective-permute-start.5 = (bf16[256,128]{1,0:T(8,128)(2,1)S(1)}, bf16[256,128]{1,0:T(8,128)(2,1)S(1)}, u32[]{:S(2)}, u32[]{:S(2)}) collective-permute-start(bf16[256,128]{1,0:T(8,128)(2,1)S(1)} %get-tuple-element.14), channel_id=1, source_target_pairs={{0,48},{16,0},{32,16},{48,32},{64,112},{80,64},{96,80},{112,96},{1... | collective-permute-start | bytes 196616 | tf_op jit(solution)/shard_map/ppermute | solution.py:423
  116.9 2.8 %collective-permute-done.5.refs_3_ = bf16[256,128]{1,0:T(8,128)(2,1)S(1)} collective-permute-done((bf16[256,128]{1,0:T(8,128)(2,1)S(1)}, bf16[256,128]{1,0:T(8,128)(2,1)S(1)}, u32[]{:S(2)}, u32[]{:S(2)}) %collective-permute-start.5) | collective-permute-done | bytes 65568 | tf_op jit(solution)/shard_map/ppermute | solution.py:423
  120.2 3.6 %all-to-all-done.1.in_ref = bf16[8,384,256]{2,1,0:T(8,128)(2,1)S(1)} async-done(((bf16[8,384,256]{2,1,0:T(8,128)(2,1)}), bf16[8,384,256]{2,1,0:T(8,128)(2,1)S(1)}, u32[]{:S(2)}, u32[]{:S(2)}) %all-to-all-start.1) | async-done | bytes 1572896 | tf_op jit(solution)/shard_map/all_to_all | solution.py:409
  123.9 0.9 shard_map.146.refs_0_
  124.8 8.1 %all-to-all-start.2 = ((bf16[32,24,128]{2,1,0:T(8,128)(2,1)}), bf16[32,24,128]{2,1,0:T(8,128)(2,1)S(1)}, u32[]{:S(2)}, u32[]{:S(2)}) async-start(bf16[32,24,128]{2,1,0:T(8,128)(2,1)} %shard_map.146.refs_0_), calls=%async_computation.2 | async-start | bytes 393216 | tf_op jit(solution)/shard_map/all_to_all | solution.py:441
  133.0 24.4 %all_gather.19 = bf16[1024,256]{1,0:T(8,128)(2,1)S(1)} all-gather(bf16[64,256]{1,0:T(8,128)(2,1)S(1)} %shard_map.147), channel_id=1, replica_groups=mesh['ep'=32,'tp'=16] {'tp'}, dimensions={0}, use_global_device_ids=true | all-gather | bytes 557056 | tf_op jit(solution)/shard_map/all_gather | solution.py:436
  157.4 1.2 shard_map.148
  158.6 2.1 %collective-permute-start.6 = (f32[256,128]{1,0:T(8,128)S(1)}, f32[256,128]{1,0:T(8,128)S(1)}, u32[]{:S(2)}, u32[]{:S(2)}) collective-permute-start(f32[256,128]{1,0:T(8,128)S(1)} %get-tuple-element.17), channel_id=1, source_target_pairs={{0,1},{1,0},{2,3},{3,2},{4,5},{5,4},{6,7},{7,6},{8,9},{9,8},{10,11... | collective-permute-start | bytes 393224 | tf_op jit(solution)/shard_map/ppermute | solution.py:445
  160.7 1.0 convolution_convert_fusion
  (68 shorter events, 9.5 us)
Async XLA Ops:
  0.6 160.0 %copy-start = (bf16[1024,128]{1,0:T(8,128)(2,1)S(1)}, bf16[1024,128]{1,0:T(8,128)(2,1)}, u32[]{:S(2)}) copy-start(bf16[1024,128]{1,0:T(8,128)(2,1)} %param.18) | copy-start | bytes 786436
  1.6 1.2 copy-start.6
  8.5 14.0 %copy-start.4 = (bf16[1,2048,256]{2,1,0:T(8,128)(2,1)S(1)}, bf16[1,2048,256]{2,1,0:T(8,128)(2,1)}, u32[]{:S(2)}) copy-start(bf16[1,2048,256]{2,1,0:T(8,128)(2,1)} %param.23) | copy-start | bytes 3145732
  8.5 16.9 %copy-start.5 = (bf16[1,2048,256]{2,1,0:T(8,128)(2,1)S(1)}, bf16[1,2048,256]{2,1,0:T(8,128)(2,1)}, u32[]{:S(2)}) copy-start(bf16[1,2048,256]{2,1,0:T(8,128)(2,1)} %param.24) | copy-start | bytes 3145732
  8.5 21.2 %copy-start.12 = (bf16[256,32]{0,1:T(8,128)(2,1)S(1)}, bf16[256,32]{0,1:T(8,128)(2,1)}, u32[]{:S(2)}) copy-start(bf16[256,32]{0,1:T(8,128)(2,1)} %param.15) | copy-start | bytes 49156
  8.5 22.2 %copy-start.10 = (bf16[256,512]{1,0:T(8,128)(2,1)S(1)}, bf16[256,512]{1,0:T(8,128)(2,1)}, u32[]{:S(2)}) copy-start(bf16[256,512]{1,0:T(8,128)(2,1)} %param.14) | copy-start | bytes 786436
  8.6 22.3 %copy-start.14 = (bf16[512,128]{1,0:T(8,128)(2,1)S(1)}, bf16[512,128]{1,0:T(8,128)(2,1)}, u32[]{:S(2)}) copy-start(bf16[512,128]{1,0:T(8,128)(2,1)} %param.17) | copy-start | bytes 393220
  8.6 22.3 %copy-start.15 = (f32[512]{0:T(512)S(1)}, f32[512]{0:T(512)}, u32[]{:S(2)}) copy-start(f32[512]{0:T(512)} %param.16) | copy-start | bytes 6148
  8.6 65.5 %all-to-all-start = ((bf16[32,8,24,128]{3,2,1,0:T(8,128)(2,1)}), bf16[32,8,24,128]{3,2,1,0:T(8,128)(2,1)}, u32[]{:S(2)}, u32[]{:S(2)}) async-start(bf16[32,8,24,128]{3,2,1,0:T(8,128)(2,1)} %get-tuple-element.10.refs_0_), calls=%async_computation | async-start | bytes 3145728 | tf_op jit(solution)/shard_map/all_to_all | solution.py:365
  22.6 51.5 %collective-permute-start = (bf16[2048,256]{1,0:T(8,128)(2,1)S(1)}, bf16[2048,256]{1,0:T(8,128)(2,1)}, u32[]{:S(2)}, u32[]{:S(2)}) collective-permute-start(bf16[2048,256]{1,0:T(8,128)(2,1)S(1)} %bitcast.19), channel_id=1, source_target_pairs={{0,1},{1,0},{2,3},{3,2},{4,5},{5,4},{6,7},{7,6},{8,9},{9,8},{10,11... | collective-permute-start | bytes 3145736 | tf_op jit(solution)/shard_map/ppermute | solution.py:369
  25.4 48.7 %collective-permute-start.1 = (bf16[2048,256]{1,0:T(8,128)(2,1)S(1)}, bf16[2048,256]{1,0:T(8,128)(2,1)}, u32[]{:S(2)}, u32[]{:S(2)}) collective-permute-start(bf16[2048,256]{1,0:T(8,128)(2,1)S(1)} %bitcast.21), channel_id=1, source_target_pairs={{0,1},{1,0},{2,3},{3,2},{4,5},{5,4},{6,7},{7,6},{8,9},{9,8},{10,11... | collective-permute-start | bytes 3145736 | tf_op jit(solution)/shard_map/ppermute | solution.py:369
  27.4 46.7 %collective-permute-start.2 = (bf16[256,2048]{1,0:T(8,128)(2,1)}, bf16[256,2048]{1,0:T(8,128)(2,1)}, u32[]{:S(2)}, u32[]{:S(2)}) collective-permute-start(bf16[256,2048]{1,0:T(8,128)(2,1)} %bitcast.6.refs_5_), channel_id=1, source_target_pairs={{0,1},{1,0},{2,3},{3,2},{4,5},{5,4},{6,7},{7,6},{8,9},{9,8},{10,11... | collective-permute-start | bytes 3145736 | tf_op jit(solution)/shard_map/ppermute | solution.py:369
  81.5 7.0 %copy-start.11 = (bf16[256,96]{0,1:T(8,128)(2,1)S(1)}, bf16[256,96]{0,1:T(8,128)(2,1)}, u32[]{:S(2)}) copy-start(bf16[256,96]{0,1:T(8,128)(2,1)} %param.13) | copy-start | bytes 147460
  81.5 7.6 %slice-start = ((bf16[256,96]{0,1:T(8,128)(2,1)}), bf16[256,32]{0,1:T(8,128)(2,1)S(1)}, s32[]{:S(2)}) async-start(bf16[256,96]{0,1:T(8,128)(2,1)} %param.13), calls=%async_computation.3 | async-start | bytes 32768 | tf_op jit(solution)/shard_map/slice | solution.py:388
  81.5 12.3 %copy-start.1 = (bf16[8,384,256]{2,1,0:T(8,128)(2,1)S(1)}, bf16[8,384,256]{2,1,0:T(8,128)(2,1)}, u32[]{:S(2)}) copy-start(bf16[8,384,256]{2,1,0:T(8,128)(2,1)} %shard_map.142.refs_0_) | copy-start | bytes 4718596
  81.5 42.4 %all-to-all-start.1 = ((bf16[8,384,256]{2,1,0:T(8,128)(2,1)}), bf16[8,384,256]{2,1,0:T(8,128)(2,1)S(1)}, u32[]{:S(2)}, u32[]{:S(2)}) async-start(bf16[8,384,256]{2,1,0:T(8,128)(2,1)} %shard_map.142.refs_0_), calls=%async_computation.1 | async-start | bytes 3145728 | tf_op jit(solution)/shard_map/all_to_all | solution.py:409
  93.8 9.9 %copy-start.3 = (bf16[1280,256]{1,0:T(8,128)(2,1)S(1)}, bf16[1280,256]{1,0:T(8,128)(2,1)}, u32[]{:S(2)}) copy-start(bf16[1280,256]{1,0:T(8,128)(2,1)} %copy-done.2) | copy-start | bytes 1966084
  107.3 25.6 %copy-start.13 = (f32[256,2]{0,1:T(2,128)S(1)}, f32[256,2]{0,1:T(2,128)}, u32[]{:S(2)}) copy-start(f32[256,2]{0,1:T(2,128)} %param.22) | copy-start | bytes 6148
  107.3 9.0 %collective-permute-start.3 = (bf16[256,128]{1,0:T(8,128)(2,1)S(1)}, bf16[256,128]{1,0:T(8,128)(2,1)S(1)}, u32[]{:S(2)}, u32[]{:S(2)}) collective-permute-start(bf16[256,128]{1,0:T(8,128)(2,1)S(1)} %get-tuple-element.12), channel_id=1, source_target_pairs={{0,16},{16,32},{32,48},{48,0},{64,80},{80,96},{96,112},{112,64},{1... | collective-permute-start | bytes 196616 | tf_op jit(solution)/shard_map/ppermute | solution.py:423
  110.1 6.8 %collective-permute-start.4 = (bf16[256,128]{1,0:T(8,128)(2,1)S(1)}, bf16[256,128]{1,0:T(8,128)(2,1)S(1)}, u32[]{:S(2)}, u32[]{:S(2)}) collective-permute-start(bf16[256,128]{1,0:T(8,128)(2,1)S(1)} %get-tuple-element.13), channel_id=1, source_target_pairs={{0,32},{16,48},{32,0},{48,16},{64,96},{80,112},{96,64},{112,80},{1... | collective-permute-start | bytes 196616 | tf_op jit(solution)/shard_map/ppermute | solution.py:423
  114.4 5.3 %collective-permute-start.5 = (bf16[256,128]{1,0:T(8,128)(2,1)S(1)}, bf16[256,128]{1,0:T(8,128)(2,1)S(1)}, u32[]{:S(2)}, u32[]{:S(2)}) collective-permute-start(bf16[256,128]{1,0:T(8,128)(2,1)S(1)} %get-tuple-element.14), channel_id=1, source_target_pairs={{0,48},{16,0},{32,16},{48,32},{64,112},{80,64},{96,80},{112,96},{1... | collective-permute-start | bytes 196616 | tf_op jit(solution)/shard_map/ppermute | solution.py:423
  120.2 37.2 %copy-start.9 = (s32[256,4]{1,0:T(8,128)S(1)}, s32[256,4]{1,0:T(8,128)}, u32[]{:S(2)}) copy-start(s32[256,4]{1,0:T(8,128)} %copy-done.8) | copy-start | bytes 12292
  124.8 32.6 %all-to-all-start.2 = ((bf16[32,24,128]{2,1,0:T(8,128)(2,1)}), bf16[32,24,128]{2,1,0:T(8,128)(2,1)S(1)}, u32[]{:S(2)}, u32[]{:S(2)}) async-start(bf16[32,24,128]{2,1,0:T(8,128)(2,1)} %shard_map.146.refs_0_), calls=%async_computation.2 | async-start | bytes 393216 | tf_op jit(solution)/shard_map/all_to_all | solution.py:441
  158.6 3.2 %collective-permute-start.6 = (f32[256,128]{1,0:T(8,128)S(1)}, f32[256,128]{1,0:T(8,128)S(1)}, u32[]{:S(2)}, u32[]{:S(2)}) collective-permute-start(f32[256,128]{1,0:T(8,128)S(1)} %get-tuple-element.17), channel_id=1, source_target_pairs={{0,1},{1,0},{2,3},{3,2},{4,5},{5,4},{6,7},{7,6},{8,9},{9,8},{10,11... | collective-permute-start | bytes 393224 | tf_op jit(solution)/shard_map/ppermute | solution.py:445
  (3 other events, 2.2 us)

commit v4 on v3

--- a/solution.py
+++ b/solution.py
@@ -7,6 +7,7 @@
 from jax.experimental.pallas import tpu as pltpu
 from jax.sharding import PartitionSpec as P
 
+
 PLAIN_HEAD_DIM = 64
 ROPE = 32
 VALUE_HEAD_DIM = 64
@@ -14,6 +15,7 @@
 
 EPSILON = 1e-06
 ROPE_BASE_VALUE = 10000.0
+
 
 VMEM = pl.BlockSpec(memory_space=pltpu.VMEM)
 SMEM = pl.BlockSpec(memory_space=pltpu.SMEM)
@@ -40,6 +42,17 @@
     )
 
 
+def to_everyone(array, axis, groups, count):
+    return lax.all_to_all(
+        jnp.broadcast_to(array[None], (count, *array.shape)),
+        axis,
+        0,
+        0,
+        tiled=True,
+        axis_index_groups=groups,
+    )
+
+
 def sequenced(array, *earlier):
     def body(array_ref, *refs):
         refs[-1][...] = array_ref[...]
@@ -53,47 +66,21 @@
     )(array, *earlier)
 
 
-LEAD = 8
-
-
-def unpacked(message):
-    blocks = message.shape[0]
-    tails = message[:, 2 * LEAD :].reshape(blocks // 2, 2, LEAD, LANES)
-    even, odd = tails[:, 0], tails[:, 1]
-    upper = lax.broadcasted_iota(jnp.int32, even.shape, 1) < LEAD // 2
-    left = jnp.where(upper, even, pltpu.roll(odd, LEAD // 2, 1))
-    right = jnp.where(upper, pltpu.roll(even, LEAD // 2, 1), odd)
-    return tuple(
-        jnp.concatenate([lead.reshape(-1, LANES), tail.reshape(-1, LANES)], axis=0)
-        for lead, tail in ((message[:, :LEAD], left), (message[:, LEAD : 2 * LEAD], right))
-    )
-
-
-def packed(left, right):
-    blocks = left.shape[0] // (LEAD + LEAD // 2)
-    split = blocks * LEAD
-    left_tail = left[split:].reshape(blocks // 2, LEAD, LANES)
-    right_tail = right[split:].reshape(blocks // 2, LEAD, LANES)
-    upper = lax.broadcasted_iota(jnp.int32, left_tail.shape, 1) < LEAD // 2
-    even = jnp.where(upper, left_tail, pltpu.roll(right_tail, LEAD // 2, 1))
-    odd = jnp.where(upper, pltpu.roll(left_tail, LEAD // 2, 1), right_tail)
-    tails = jnp.concatenate([even[:, None], odd[:, None]], axis=1).reshape(blocks, LEAD, LANES)
-    return jnp.concatenate(
-        [
-            left[:split].reshape(blocks, LEAD, LANES),
-            right[:split].reshape(blocks, LEAD, LANES),
-            tails,
-        ],
-        axis=1,
-    )
+SHARE = 6
+PARTS = 4
+
+
+def message_rows(shape, dim):
+    place = lax.broadcasted_iota(jnp.int32, shape, dim)
+    source = jnp.floor((place.astype(jnp.float32) + 0.5) * (1.0 / SHARE)).astype(jnp.int32)
+    return place + source * (SHARE * (PARTS - 1))
 
 
 def pack_rows(index, moe_input, gain, routes, capacity, expert_total):
     rows, width = moe_input.shape
     places = expert_total * capacity
-    half = capacity // 2
     top = routes.shape[1]
-    wide = 2 * LANES
+    wide = PARTS * LANES
 
     def body(index_ref, input_ref, gain_ref, routes_ref, out_ref, place_ref):
         floats = input_ref[...].astype(jnp.float32)
@@ -111,38 +98,51 @@
         )
         lower = jnp.where(lower, 1.0, 0.0).astype(jnp.bfloat16)
         earlier = jnp.dot(lower, ones, preferred_element_type=jnp.float32)
-        slot = earlier - (index_ref[1] * half).astype(jnp.float32)
-        valid = (slot >= 0.0) & (slot < float(half))
-        base = slot + expert.astype(jnp.float32) * float(capacity) + 1.0
-        step = float(LEAD)
-        values = (
-            jnp.where(slot < step, base, base + step),
-            jnp.where(slot < step, base + step, base + step + float(LEAD // 2)),
-        )
+        first_row = expert.astype(jnp.float32) * float(capacity)
+        share = float(SHARE)
+
+        def within(part):
+            slot = earlier - part.astype(jnp.float32) * share
+            return slot, (slot >= 0.0) & (slot < share)
+
+        def pick(k, value, valid):
+            chosen_value = jnp.where(named[k] & valid, value + 1.0, 0.0)
+            return jnp.sum(chosen_value, axis=1, keepdims=True).astype(jnp.int32) - 1
+
+        slot, valid = within(index_ref[0])
+        starts = [pick(k, slot + first_row, valid) for k in range(top)]
         slots = lax.broadcasted_iota(jnp.int32, (rows, places), 1)
         selects = []
-        for side, value in enumerate(values):
+        for part in range(PARTS):
             hit = None
-            for k in range(top):
-                place = jnp.sum(jnp.where(named[k] & valid, value, 0.0), axis=1, keepdims=True)
-                place = place.astype(jnp.int32) - 1
-                column = side * top + k
-                place_ref[:, column : column + 1] = place
-                here = slots == place
+            for start in starts:
+                target = jnp.where(start < 0, -1, start + part * SHARE)
+                here = slots == target
                 hit = here if hit is None else hit | here
             selects.append(jnp.where(hit, 1.0, 0.0).astype(jnp.bfloat16))
         for b in range(width // wide):
             total = None
-            for side, select in enumerate(selects):
-                first = b * wide + side * LANES
-                part = lax.dot_general(
+            for part, select in enumerate(selects):
+                first = b * wide + part * LANES
+                piece = lax.dot_general(
                     select,
                     normed[:, first : first + LANES],
                     (((0,), (0,)), ((), ())),
                     preferred_element_type=jnp.float32,
                 )
-                total = part if total is None else total + part
+                total = piece if total is None else total + piece
             out_ref[:, b] = total.reshape(expert_total, capacity, LANES).astype(jnp.bfloat16)
+
+        low_slot, low_valid = within(index_ref[1])
+        high_slot, high_valid = within(index_ref[1] + 2)
+        value = jnp.where(low_valid, low_slot, high_slot + 2.0 * share) + first_row
+        for k in range(top):
+            start = pick(k, value, low_valid | high_valid)
+            for side in range(2):
+                column = side * top + k
+                place_ref[:, column : column + 1] = jnp.where(
+                    start < 0, -1, start + side * SHARE
+                )
 
     return kernel_call(
         body,
@@ -157,33 +157,48 @@
 
 
 def add_up(parts, blocks, *earlier):
-    count = parts.shape[0]
+    count, rows, _ = parts.shape
+    capacity = SHARE * PARTS
 
     def body(in_ref, *refs):
         out_ref = refs[-1]
-        total = in_ref[0].astype(jnp.float32)
-        for i in range(1, count):
-            total += in_ref[i].astype(jnp.float32)
-        out_ref[...] = packed(total[:, :LANES], total[:, LANES:]).astype(jnp.bfloat16)
-
-    return kernel_call(
-        body,
-        jax.ShapeDtypeStruct((blocks, 3 * LEAD, LANES), jnp.bfloat16),
+        targets = message_rows((blocks * capacity, rows), 1)
+        lines = lax.broadcasted_iota(jnp.int32, (blocks * capacity, rows), 0)
+        total = None
+        for parity in range(2):
+            added = in_ref[parity].astype(jnp.float32)
+            for i in range(parity + 2, count, 2):
+                added += in_ref[i].astype(jnp.float32)
+            added = added.astype(jnp.bfloat16)
+            for side in range(2):
+                offset = (2 * parity + side) * SHARE
+                select = jnp.where(lines == targets + offset, 1.0, 0.0).astype(jnp.bfloat16)
+                part = jnp.dot(
+                    select,
+                    added[:, side * LANES : (side + 1) * LANES],
+                    preferred_element_type=jnp.float32,
+                )
+                total = part if total is None else total + part
+        out_ref[...] = total.reshape(blocks, capacity, LANES).astype(jnp.bfloat16)
+
+    return kernel_call(
+        body,
+        jax.ShapeDtypeStruct((blocks, capacity, LANES), jnp.bfloat16),
         [VMEM] + [ANY] * len(earlier),
         VMEM,
         1,
     )(parts, *earlier)
 
 
-def attend(index, query, key_value, score_scale):
+def attend(query, key_value, score_scale):
     blocks, rows, _ = query.shape
     pieces, _, length = key_value.shape
     factor = score_scale * math.log2(math.e)
     first_value = PLAIN_HEAD_DIM + ROPE
 
-    def body(index_ref, query_ref, key_ref, *out_refs):
-        for i, out_ref in enumerate(out_refs):
-            q = query_ref[(index_ref[0] + i) % blocks]
+    def body(query_ref, key_ref, out_ref):
+        for i in range(blocks):
+            q = query_ref[i]
             scores = [
                 jnp.dot(q, key_ref[j, :LANES, :], preferred_element_type=jnp.float32)
                 for j in range(pieces)
@@ -205,31 +220,30 @@
                 )
                 mixed = part if mixed is None else mixed + part
             total = jnp.sum(total, axis=1, keepdims=True)
-            out_ref[:, :VALUE_HEAD_DIM] = (mixed / total).astype(jnp.bfloat16)
+            out_ref[i, :, :VALUE_HEAD_DIM] = (mixed / total).astype(jnp.bfloat16)
             log_total = top + jnp.log2(total)
             high = log_total.astype(jnp.bfloat16).astype(jnp.float32)
             middle = (log_total - high).astype(jnp.bfloat16).astype(jnp.float32)
             low = log_total - high - middle
             lane = lax.broadcasted_iota(jnp.int32, (rows, LANES - VALUE_HEAD_DIM), 1)
-            out_ref[:, VALUE_HEAD_DIM:] = jnp.where(
+            out_ref[i, :, VALUE_HEAD_DIM:] = jnp.where(
                 lane == 0, high, jnp.where(lane == 1, middle, low)
             ).astype(jnp.bfloat16)
 
     return kernel_call(
         body,
-        tuple(jax.ShapeDtypeStruct((rows, LANES), jnp.bfloat16) for _ in range(blocks)),
-        [SMEM, VMEM, VMEM],
-        (VMEM,) * blocks,
+        jax.ShapeDtypeStruct((blocks, rows, LANES), jnp.bfloat16),
+        [VMEM, VMEM],
+        VMEM,
         4 * blocks * rows * pieces * length * 2 * LANES,
-    )(index, query, key_value)
+    )(query, key_value)
 
 
 def merge(partials):
-    rows = partials[0].shape[0]
-
-    def body(*refs):
-        out_ref = refs[-1]
-        values = [r[...].astype(jnp.float32) for r in refs[:-1]]
+    count, rows, _ = partials.shape
+
+    def body(in_ref, out_ref):
+        values = [in_ref[i].astype(jnp.float32) for i in range(count)]
         first = VALUE_HEAD_DIM
         logs = [
             v[:, first : first + 1] + v[:, first + 1 : first + 2] + v[:, first + 2 : first + 3]
@@ -249,29 +263,38 @@
     return kernel_call(
         body,
         jax.ShapeDtypeStruct((VALUE_HEAD_DIM, rows), jnp.bfloat16),
-        [VMEM] * len(partials),
+        [VMEM],
         VMEM,
         1,
-    )(*partials)
-
-
-def experts(messages, gates, ups, downs, *earlier):
-    sources, blocks, _, _ = messages.shape
-    rows = sources * (LEAD + LEAD // 2)
-    wide = 2 * LANES
+    )(partials)
+
+
+def hidden_units(messages, gates, ups):
+    sources, blocks, capacity, _ = messages.shape
+    rows = sources * SHARE
     units = gates[0].shape[1]
     count = len(gates)
-
-    def body(*refs):
-        rows_ref = refs[0]
-        gate_refs, up_refs, down_refs = (refs[1 + k * count : 1 + (k + 1) * count] for k in range(3))
-        out_ref = refs[-1]
-        hidden = []
-        parts = [
-            jnp.concatenate(unpacked(rows_ref[:, b].astype(jnp.float32)), axis=1).astype(jnp.bfloat16)
-            for b in range(blocks)
+    wide = 2 * LANES
+
+    def body(rows_ref, *refs):
+        gate_refs, up_refs, out_ref = refs[:count], refs[count : 2 * count], refs[-1]
+        targets = message_rows((rows, sources * capacity), 0)
+        lines = lax.broadcasted_iota(jnp.int32, (rows, sources * capacity), 1)
+        selects = [
+            jnp.where(lines == targets + part * SHARE, 1.0, 0.0).astype(jnp.bfloat16)
+            for part in range(PARTS)
         ]
-        for gate_ref, up_ref in zip(gate_refs, up_refs):
+        parts = []
+        for b in range(blocks):
+            block = rows_ref[:, b].astype(jnp.float32).reshape(sources * capacity, LANES)
+            block = block.astype(jnp.bfloat16)
+            columns = [
+                jnp.dot(select, block, preferred_element_type=jnp.float32).astype(jnp.bfloat16)
+                for select in selects
+            ]
+            for part in range(0, PARTS, 2):
+                parts.append(jnp.concatenate(columns[part : part + 2], axis=1))
+        for g, (gate_ref, up_ref) in enumerate(zip(gate_refs, up_refs)):
             gate_value = jnp.zeros((rows, units), jnp.float32)
             up_value = jnp.zeros((rows, units), jnp.float32)
             for b, part in enumerate(parts):
@@ -279,22 +302,40 @@
                 gate_value += jnp.dot(part, gate_ref[span, :], preferred_element_type=jnp.float32)
                 up_value += jnp.dot(part, up_ref[span, :], preferred_element_type=jnp.float32)
             silu = gate_value / (1.0 + jnp.exp(-gate_value))
-            hidden.append((silu * up_value).astype(jnp.bfloat16))
+            out_ref[g] = (silu * up_value).astype(jnp.bfloat16)
+
+    return kernel_call(
+        body,
+        jax.ShapeDtypeStruct((count, rows, units), jnp.bfloat16),
+        [VMEM] * (1 + 2 * count),
+        VMEM,
+        4 * rows * gates[0].shape[0] * units * count,
+    )(messages, *gates, *ups)
+
+
+def project_down(hidden, downs, blocks, *earlier):
+    count, rows, units = hidden.shape
+    wide = downs[0].shape[1] // blocks
+
+    def body(hidden_ref, *refs):
+        out_ref = refs[-1]
         for b in range(blocks):
             span = slice(b * wide, (b + 1) * wide)
             total = None
-            for h, down_ref in zip(hidden, down_refs):
-                part = jnp.dot(h, down_ref[:, span], preferred_element_type=jnp.float32)
+            for g in range(count):
+                part = jnp.dot(
+                    hidden_ref[g], refs[g][:, span], preferred_element_type=jnp.float32
+                )
                 total = part if total is None else total + part
             out_ref[b] = total.astype(jnp.bfloat16)
 
     return kernel_call(
         body,
         jax.ShapeDtypeStruct((blocks, rows, wide), jnp.bfloat16),
-        [VMEM] * (1 + 3 * count) + [ANY] * len(earlier),
+        [VMEM] * (1 + count) + [ANY] * len(earlier),
         VMEM,
-        2 * rows * blocks * wide * units * 3 * count,
-    )(messages, *gates, *ups, *downs, *earlier)
+        2 * rows * units * count * wide * blocks,
+    )(hidden, *downs, *earlier)
 
 
 def combine(index, returned, places, route_weight):
@@ -337,6 +378,7 @@
     z_groups = [[x_count * z + x for z in range(z_count)] for x in range(x_count)]
     y_groups = [[cores * y + c for y in range(y_count)] for c in range(cores)]
     partner = [(i, i ^ 1) for i in range(tp_count)]
+    neighbour = [(i, i ^ cores) for i in range(tp_count)]
 
     def local(
         queries,
@@ -357,16 +399,20 @@
         capacity = 3 * row_count // ep_count
         tp_index = lax.axis_index("tp").astype(jnp.int32)
         ep_index = lax.axis_index("ep").astype(jnp.int32)
-        place_index = jnp.stack([tp_index // cores, tp_index % cores])
+        place_index = jnp.stack([tp_index % PARTS, tp_index % cores])
+
+        groups_of = [[gate_weight[0]], [up_weight[0]], [down_weight[0]]]
+        for group in groups_of:
+            group.append(lax.ppermute(group[0], "tp", neighbour))
 
         outgoing, places = pack_rows(
             place_index, moe_input, moe_gain.reshape(1, -1), routes, capacity, ep_count
         )
         arrived = lax.all_to_all(outgoing, "ep", 0, 0, tiled=True)
 
-        gates, ups, downs = [gate_weight[0]], [up_weight[0]], [down_weight[0]]
-        for pair in (gates, ups, downs):
-            pair.append(lax.ppermute(pair[0], "tp", partner))
+        for group in groups_of:
+            group += [lax.ppermute(weight, "tp", partner) for weight in group[:2]]
+        gates, ups, downs = groups_of
 
         positions = (ep_index * row_count + jnp.arange(row_count, dtype=jnp.int32)).astype(
             jnp.float32
@@ -401,39 +447,23 @@
         own_pack = jnp.concatenate(
             [own_keys[:PLAIN_HEAD_DIM], own_rope, own_keys[PLAIN_HEAD_DIM:]], axis=0
         )
-        key_value = lax.all_gather(
-            sequenced(own_pack, outgoing), "ep", axis=0, axis_index_groups=z_groups
-        )
-
-        partial_out = experts(arrived, gates, ups, downs, key_value)
+        key_value = to_everyone(sequenced(own_pack, arrived), "ep", z_groups, z_count)
+        hidden = hidden_units(arrived, gates, ups)
+        query_all = to_everyone(sequenced(query, key_value, hidden), "ep", x_groups, x_count)
+        partial_all = attend(query_all, key_value, (PLAIN_HEAD_DIM + ROPE) ** (-0.5))
+        partials = lax.all_to_all(
+            partial_all, "ep", 0, 0, tiled=True, axis_index_groups=x_groups
+        )
+
+        partial_out = project_down(hidden, downs, y_count, partials)
         groups = lax.all_to_all(
             partial_out, "tp", 0, 0, tiled=True, axis_index_groups=y_groups
         )
-
-        query_all = lax.all_gather(
-            sequenced(query, partial_out), "ep", axis=0, axis_index_groups=x_groups
-        )
-        partial_all = attend(
-            (ep_index % x_count).reshape(1),
-            query_all,
-            key_value,
-            (PLAIN_HEAD_DIM + ROPE) ** (-0.5),
-        )
-        partials = [partial_all[0]] + [
-            lax.ppermute(
-                partial_all[i],
-                "ep",
-                [
-                    (x_count * z + x, x_count * z + (x + i) % x_count)
-                    for z in range(z_count)
-                    for x in range(x_count)
-                ],
-            )
-            for i in range(1, x_count)
-        ]
         attended = merge(partials)
-        summed = add_up(groups, ep_count, attended)
-        everyone = lax.all_gather(sequenced(attended, summed), "tp", axis=0, tiled=True)
+        everyone = lax.all_gather(
+            sequenced(attended, partial_out), "tp", axis=0, tiled=True
+        )
+        summed = add_up(groups, ep_count, everyone)
         attention_out = lax.dot_general(
             everyone, out_proj, (((0,), (0,)), ((), ())), preferred_element_type=jnp.float32
         ).astype(jnp.bfloat16)
@@ -451,8 +481,10 @@
 def solution(mesh):
     ep_count = mesh.shape["ep"]
     x_count = 4
+    local = make_local(ep_count // x_count, x_count, mesh.shape["tp"])
+
     return jax.shard_map(
-        make_local(ep_count // x_count, x_count, mesh.shape["tp"]),
+        local,
         mesh=mesh,
         in_specs=(
             P("ep", "tp"),

time: 163 us -> 199 us (1.22)
  waiting for transfers between devices: 7.22 us -> 48.9 us
  blocking collectives: 77.1 us -> 42.8 us
  starting transfers between devices: 47.3 us -> 72.4 us
  Pallas kernels: 17 us -> 21.6 us
    all_gather x3 -> x1, blocking collectives: 77.1 us -> 32.5 us  [local(): lax.all_gather(sequenced(attended, partial_out), 'tp', axis=0, tiled=True)]
    ppermute x6 -> x9, waiting for transfers between devices: 3.38 us -> 33.2 us  [the longest x3 33.1 us: local(): group.append(lax.ppermute(group[0], 'tp', neighbour))]
    ppermute x6 -> x9, starting transfers between devices: 16.2 us -> 30 us  [the longest x6 21.5 us: local(): group += [lax.ppermute(weight, 'tp', partner) for weight in group[:2]]]
    all_to_all x1, waiting for transfers between devices: 0.01 us -> 10.5 us  [local(): returned = lax.all_to_all(summed, 'ep', 0, 0, tiled=True)]
    all_to_all x0 -> x2, starting transfers between devices: none -> 10.3 us  [the longest x1 6.7 us: to_everyone(): lax.all_to_all(jnp.broadcast_to(array[None], (count, *array.shape)), axis...]
    all_to_all x0 -> x1, blocking collectives: none -> 10.3 us  [to_everyone(): lax.all_to_all(jnp.broadcast_to(array[None], (count, *array.shape)), axis...]
    all_to_all x0 -> x2, waiting for transfers between devices: none -> 5.3 us  [the longest x1 5.3 us: local(): lax.all_to_all(partial_all, 'ep', 0, 0, tiled=True, axis_index_groups=x_g...]
    pallas_call x3 -> x4, Pallas kernels: 11 us -> 15.8 us  [the longest x1 6.23 us: hidden_units(): kernel_call(body, jax.ShapeDtypeStruct((count, rows, units), jnp.bfloat16...]
  transfers between devices with their start and end apart: 10 -> 15, of which waited for: 4 -> 5; matrix products, arithmetic and copies ran while one was open for 5% -> 2% of each run, Pallas kernels for 3% -> 6%
where the time goes in v4:
time: 199 us; the launch traced here: 197 us
  starting transfers between devices  72.4 us (36%)
  waiting for transfers between devices  48.9 us (25%)
  blocking collectives  42.8 us (22%)
  Pallas kernels  21.6 us (11%)
  local copies, waits for them, and re-layouts  7.13 us (4%)
  other arithmetic  2.18 us (1%)
    ppermute x3, waiting for transfers between devices, local(): group.append(lax.ppermute(group[0], 'tp', neighbour))  33.1 us
    all_gather x1, blocking collectives, local(): lax.all_gather(sequenced(attended, partial_out), 'tp', axis=0, tiled=True)  32.5 us
    ppermute x6, starting transfers between devices, local(): group += [lax.ppermute(weight, 'tp', partner) for weight in group[:2]]  21.5 us
    all_to_all x1, starting transfers between devices, local(): arrived = lax.all_to_all(outgoing, 'ep', 0, 0, tiled=True)  13.8 us
    all_to_all x1, waiting for transfers between devices, local(): returned = lax.all_to_all(summed, 'ep', 0, 0, tiled=True)  10.5 us
    all_to_all x1, blocking collectives, to_everyone(): lax.all_to_all(jnp.broadcast_to(array[None], (count, *array.shape)), axis...  10.3 us
    ppermute x3, starting transfers between devices, local(): group.append(lax.ppermute(group[0], 'tp', neighbour))  8.49 us
    all_to_all x1, starting transfers between devices, local(): returned = lax.all_to_all(summed, 'ep', 0, 0, tiled=True)  7.59 us
  transfers between devices with their start and end apart: 15, of which 5 were waited for; matrix products, arithmetic and copies ran while one was open for 2% of the time, Pallas kernels for 6%

profile of v4, /device:TPU:1, one launch (start us, length us, event | category | flops | bytes accessed | tf_op | source)
XLA Modules:
  0.0 197.4 jit_solution(18431665130681373819)
XLA Ops:
  3.5 4.1 %shard_map.140 = (bf16[32,4,24,128]{3,2,1,0:T(8,128)(2,1)}, s32[256,4]{1,0:T(8,128)S(1)}) custom-call(s32[2]{0:T(128)S(1)} %pad_add_fusion.index_ref, bf16[256,2048]{1,0:T(8,128)(2,1)S(1)} %copy-done.2, f32[1,2048]{1,0:T(1,128)S(1)} %bitcast.18, s32[256,2]{1,0:T(8,128)S(1)} %copy.34.routes_ref), custom_call_target="tpu_custom_call" | custom-call | flops 805306368 | tf_op jit(solution)/shard_map/pallas_call | solution.py:147
  7.5 13.8 %all-to-all-start = ((bf16[32,4,24,128]{3,2,1,0:T(8,128)(2,1)}), bf16[32,4,24,128]{3,2,1,0:T(8,128)(2,1)S(1)}, u32[]{:S(2)}, u32[]{:S(2)}) async-start(bf16[32,4,24,128]{3,2,1,0:T(8,128)(2,1)} %get-tuple-element.6), calls=%async_computation | async-start | bytes 1572864 | tf_op jit(solution)/shard_map/all_to_all | solution.py:411
  21.4 3.2 %collective-permute-start = (bf16[2048,256]{1,0:T(8,128)(2,1)S(1)}, bf16[2048,256]{1,0:T(8,128)(2,1)}, u32[]{:S(2)}, u32[]{:S(2)}) collective-permute-start(bf16[2048,256]{1,0:T(8,128)(2,1)S(1)} %bitcast.14), channel_id=1, source_target_pairs={{0,2},{1,3},{2,0},{3,1},{4,6},{5,7},{6,4},{7,5},{8,10},{9,11},{10,... | collective-permute-start | bytes 3145736 | tf_op jit(solution)/shard_map/ppermute | solution.py:406
  24.6 3.1 %collective-permute-start.1 = (bf16[2048,256]{1,0:T(8,128)(2,1)S(1)}, bf16[2048,256]{1,0:T(8,128)(2,1)}, u32[]{:S(2)}, u32[]{:S(2)}) collective-permute-start(bf16[2048,256]{1,0:T(8,128)(2,1)S(1)} %bitcast.15), channel_id=1, source_target_pairs={{0,1},{1,0},{2,3},{3,2},{4,5},{5,4},{6,7},{7,6},{8,9},{9,8},{10,11... | collective-permute-start | bytes 3145736 | tf_op jit(solution)/shard_map/ppermute | solution.py:414
  29.8 2.2 %collective-permute-start.4 = (bf16[2048,256]{1,0:T(8,128)(2,1)}, bf16[2048,256]{1,0:T(8,128)(2,1)}, u32[]{:S(2)}, u32[]{:S(2)}) collective-permute-start(bf16[2048,256]{1,0:T(8,128)(2,1)} %bitcast.6.refs_4_), channel_id=1, source_target_pairs={{0,1},{1,0},{2,3},{3,2},{4,5},{5,4},{6,7},{7,6},{8,9},{9,8},{10,11... | collective-permute-start | bytes 3145736 | tf_op jit(solution)/shard_map/ppermute | solution.py:414
  32.0 3.2 %collective-permute-start.6 = (bf16[256,2048]{1,0:T(8,128)(2,1)}, bf16[256,2048]{1,0:T(8,128)(2,1)}, u32[]{:S(2)}, u32[]{:S(2)}) collective-permute-start(bf16[256,2048]{1,0:T(8,128)(2,1)} %bitcast.7.refs_0_), channel_id=1, source_target_pairs={{0,2},{1,3},{2,0},{3,1},{4,6},{5,7},{6,4},{7,5},{8,10},{9,11},{10,... | collective-permute-start | bytes 3145736 | tf_op jit(solution)/shard_map/ppermute | solution.py:406
  38.0 9.2 %collective-permute-done.refs_1_ = bf16[2048,256]{1,0:T(8,128)(2,1)} collective-permute-done((bf16[2048,256]{1,0:T(8,128)(2,1)S(1)}, bf16[2048,256]{1,0:T(8,128)(2,1)}, u32[]{:S(2)}, u32[]{:S(2)}) %collective-permute-start) | collective-permute-done | bytes 1048608 | tf_op jit(solution)/shard_map/ppermute | solution.py:406
  47.1 5.1 %collective-permute-start.2 = (bf16[2048,256]{1,0:T(8,128)(2,1)}, bf16[2048,256]{1,0:T(8,128)(2,1)}, u32[]{:S(2)}, u32[]{:S(2)}) collective-permute-start(bf16[2048,256]{1,0:T(8,128)(2,1)} %collective-permute-done.refs_1_), channel_id=1, source_target_pairs={{0,1},{1,0},{2,3},{3,2},{4,5},{5,4},{6,7},{7,6},{8,9},{9,8},{10,11... | collective-permute-start | bytes 3145736 | tf_op jit(solution)/shard_map/ppermute | solution.py:414
  52.3 17.3 %collective-permute-done.3.refs_5_ = bf16[2048,256]{1,0:T(8,128)(2,1)} collective-permute-done((bf16[2048,256]{1,0:T(8,128)(2,1)}, bf16[2048,256]{1,0:T(8,128)(2,1)}, u32[]{:S(2)}, u32[]{:S(2)}) %collective-permute-start.3) | collective-permute-done | bytes 1048608 | tf_op jit(solution)/shard_map/ppermute | solution.py:406
  69.6 5.1 %collective-permute-start.5 = (bf16[2048,256]{1,0:T(8,128)(2,1)}, bf16[2048,256]{1,0:T(8,128)(2,1)}, u32[]{:S(2)}, u32[]{:S(2)}) collective-permute-start(bf16[2048,256]{1,0:T(8,128)(2,1)} %collective-permute-done.3.refs_5_), channel_id=1, source_target_pairs={{0,1},{1,0},{2,3},{3,2},{4,5},{5,4},{6,7},{7,6},{8,9},{9,8},{10,11... | collective-permute-start | bytes 3145736 | tf_op jit(solution)/shard_map/ppermute | solution.py:414
  75.7 6.7 %all-to-all-start.1 = ((bf16[8,160,256]{2,1,0:T(8,128)(2,1)}), bf16[8,160,256]{2,1,0:T(8,128)(2,1)S(1)}, u32[]{:S(2)}, u32[]{:S(2)}) async-start(bf16[8,160,256]{2,1,0:T(8,128)(2,1)} %broadcast_in_dim.7), calls=%async_computation.1 | async-start | bytes 1310720 | tf_op jit(solution)/shard_map/all_to_all | solution.py:46
  85.4 6.6 %collective-permute-done.6.refs_1_ = bf16[256,2048]{1,0:T(8,128)(2,1)} collective-permute-done((bf16[256,2048]{1,0:T(8,128)(2,1)}, bf16[256,2048]{1,0:T(8,128)(2,1)}, u32[]{:S(2)}, u32[]{:S(2)}) %collective-permute-start.6) | collective-permute-done | bytes 1048608 | tf_op jit(solution)/shard_map/ppermute | solution.py:406
  92.1 3.7 %collective-permute-start.8 = (bf16[256,2048]{1,0:T(8,128)(2,1)}, bf16[256,2048]{1,0:T(8,128)(2,1)}, u32[]{:S(2)}, u32[]{:S(2)}) collective-permute-start(bf16[256,2048]{1,0:T(8,128)(2,1)} %collective-permute-done.6.refs_1_), channel_id=1, source_target_pairs={{0,1},{1,0},{2,3},{3,2},{4,5},{5,4},{6,7},{7,6},{8,9},{9,8},{10,11... | collective-permute-start | bytes 3145736 | tf_op jit(solution)/shard_map/ppermute | solution.py:414
  97.5 6.2 %shard_map.142.refs_1_.hidden_ref = bf16[4,192,256]{2,1,0:T(8,128)(2,1)S(1)} custom-call(bf16[32,4,24,128]{3,2,1,0:T(8,128)(2,1)S(1)} %all-to-all-done.refs_0_.rows_ref, bf16[2048,256]{1,0:T(8,128)(2,1)S(1)} %bitcast.16, bf16[2048,256]{1,0:T(8,128)(2,1)} %collective-permute-done.refs_1_, bf16[2048,256]{1,0:T(8,128)(2,1)} %collective-permute-done.1.refs_2_, ...), custom_call_target="tpu_custom_call" | custom-call | flops 1610612736 | tf_op jit(solution)/shard_map/pallas_call | solution.py:307
  103.8 10.3 %all_to_all.30.query_ref = bf16[4,256,128]{2,1,0:T(8,128)(2,1)S(1)} all-to-all(bf16[4,256,128]{2,1,0:T(8,128)(2,1)S(1)} %broadcast_in_dim.8), channel_id=1, replica_groups={{0,16,32,48},{64,80,96,112},{128,144,160,176},{192,208,224,240},{256,27..., dimensions={0} | all-to-all | bytes 524288 | tf_op jit(solution)/shard_map/all_to_all | solution.py:46
  114.1 4.2 %shard_map.144 = bf16[4,256,128]{2,1,0:T(8,128)(2,1)} custom-call(bf16[4,256,128]{2,1,0:T(8,128)(2,1)S(1)} %all_to_all.30.query_ref, bf16[8,160,256]{2,1,0:T(8,128)(2,1)S(1)} %all-to-all-done.1.refs_0_.key_ref), custom_call_target="tpu_custom_call" | custom-call | flops 2147483648 | tf_op jit(solution)/shard_map/pallas_call | solution.py:233
  118.3 3.6 %all-to-all-start.3 = ((bf16[4,256,128]{2,1,0:T(8,128)(2,1)}), bf16[4,256,128]{2,1,0:T(8,128)(2,1)S(1)}, u32[]{:S(2)}, u32[]{:S(2)}) async-start(bf16[4,256,128]{2,1,0:T(8,128)(2,1)} %shard_map.144), calls=%async_computation.3 | async-start | bytes 524288 | tf_op jit(solution)/shard_map/all_to_all | solution.py:454
  121.9 5.3 %all-to-all-done.3.in_ref.refs_4_ = bf16[4,256,128]{2,1,0:T(8,128)(2,1)S(1)} async-done(((bf16[4,256,128]{2,1,0:T(8,128)(2,1)}), bf16[4,256,128]{2,1,0:T(8,128)(2,1)S(1)}, u32[]{:S(2)}, u32[]{:S(2)}) %all-to-all-start.3) | async-done | bytes 262176 | tf_op jit(solution)/shard_map/all_to_all | solution.py:454
  127.2 4.1 %shard_map.146.refs_0_ = bf16[8,192,256]{2,1,0:T(8,128)(2,1)} custom-call(bf16[4,192,256]{2,1,0:T(8,128)(2,1)S(1)} %shard_map.142.refs_1_.hidden_ref, bf16[256,2048]{1,0:T(8,128)(2,1)} %bitcast.7.refs_0_, bf16[256,2048]{1,0:T(8,128)(2,1)} %collective-permute-done.6.refs_1_, bf16[256,2048]{1,0:T(8,128)(2,1)} %collective-permute-done.7.refs_2_, ...), custom_call_target="tpu_custom_call" | custom-call | flops 805306368 | tf_op jit(solution)/shard_map/pallas_call | solution.py:332
  131.3 6.8 %all-to-all-start.4 = ((bf16[8,192,256]{2,1,0:T(8,128)(2,1)}), bf16[8,192,256]{2,1,0:T(8,128)(2,1)S(1)}, u32[]{:S(2)}, u32[]{:S(2)}) async-start(bf16[8,192,256]{2,1,0:T(8,128)(2,1)} %shard_map.146.refs_0_), calls=%async_computation.4 | async-start | bytes 1572864 | tf_op jit(solution)/shard_map/all_to_all | solution.py:459
  138.7 32.5 %all_gather.3.refs_0_ = bf16[1024,256]{1,0:T(8,128)(2,1)S(1)} all-gather(bf16[64,256]{1,0:T(8,128)(2,1)S(1)} %shard_map.147), channel_id=1, replica_groups=mesh['ep'=32,'tp'=16] {'tp'}, dimensions={0}, use_global_device_ids=true | all-gather | bytes 557056 | tf_op jit(solution)/shard_map/all_gather | solution.py:463
  172.5 7.6 %all-to-all-start.5 = ((bf16[32,24,128]{2,1,0:T(8,128)(2,1)}), bf16[32,24,128]{2,1,0:T(8,128)(2,1)S(1)}, u32[]{:S(2)}, u32[]{:S(2)}) async-start(bf16[32,24,128]{2,1,0:T(8,128)(2,1)} %shard_map.148), calls=%async_computation.5 | async-start | bytes 393216 | tf_op jit(solution)/shard_map/all_to_all | solution.py:471
  180.3 10.5 %all-to-all-done.5 = bf16[32,24,128]{2,1,0:T(8,128)(2,1)S(1)} async-done(((bf16[32,24,128]{2,1,0:T(8,128)(2,1)}), bf16[32,24,128]{2,1,0:T(8,128)(2,1)S(1)}, u32[]{:S(2)}, u32[]{:S(2)}) %all-to-all-start.5) | async-done | bytes 196640 | tf_op jit(solution)/shard_map/all_to_all | solution.py:471
  191.9 3.9 %collective-permute-start.9 = (f32[256,128]{1,0:T(8,128)S(1)}, f32[256,128]{1,0:T(8,128)S(1)}, u32[]{:S(2)}, u32[]{:S(2)}) collective-permute-start(f32[256,128]{1,0:T(8,128)S(1)} %get-tuple-element.9), channel_id=1, source_target_pairs={{0,1},{1,0},{2,3},{3,2},{4,5},{5,4},{6,7},{7,6},{8,9},{9,8},{10,11... | collective-permute-start | bytes 393224 | tf_op jit(solution)/shard_map/ppermute | solution.py:475
  (69 shorter events, 17.9 us)
Async XLA Ops:
  0.6 195.2 %copy-start = (bf16[1024,128]{1,0:T(8,128)(2,1)S(1)}, bf16[1024,128]{1,0:T(8,128)(2,1)}, u32[]{:S(2)}) copy-start(bf16[1024,128]{1,0:T(8,128)(2,1)} %param.18) | copy-start | bytes 786436
  0.7 0.7 copy-start.6
  2.2 1.2 copy-start.2
  7.5 13.9 %copy-start.1 = (bf16[1,2048,256]{2,1,0:T(8,128)(2,1)S(1)}, bf16[1,2048,256]{2,1,0:T(8,128)(2,1)}, u32[]{:S(2)}) copy-start(bf16[1,2048,256]{2,1,0:T(8,128)(2,1)} %param.23) | copy-start | bytes 3145732
  7.5 27.8 %copy-start.4 = (bf16[256,512]{1,0:T(8,128)(2,1)S(1)}, bf16[256,512]{1,0:T(8,128)(2,1)}, u32[]{:S(2)}) copy-start(bf16[256,512]{1,0:T(8,128)(2,1)} %param.14) | copy-start | bytes 786436
  7.5 67.2 %all-to-all-start = ((bf16[32,4,24,128]{3,2,1,0:T(8,128)(2,1)}), bf16[32,4,24,128]{3,2,1,0:T(8,128)(2,1)S(1)}, u32[]{:S(2)}, u32[]{:S(2)}) async-start(bf16[32,4,24,128]{3,2,1,0:T(8,128)(2,1)} %get-tuple-element.6), calls=%async_computation | async-start | bytes 1572864 | tf_op jit(solution)/shard_map/all_to_all | solution.py:411
  21.4 25.8 %collective-permute-start = (bf16[2048,256]{1,0:T(8,128)(2,1)S(1)}, bf16[2048,256]{1,0:T(8,128)(2,1)}, u32[]{:S(2)}, u32[]{:S(2)}) collective-permute-start(bf16[2048,256]{1,0:T(8,128)(2,1)S(1)} %bitcast.14), channel_id=1, source_target_pairs={{0,2},{1,3},{2,0},{3,1},{4,6},{5,7},{6,4},{7,5},{8,10},{9,11},{10,... | collective-permute-start | bytes 3145736 | tf_op jit(solution)/shard_map/ppermute | solution.py:406
  24.6 58.6 %collective-permute-start.1 = (bf16[2048,256]{1,0:T(8,128)(2,1)S(1)}, bf16[2048,256]{1,0:T(8,128)(2,1)}, u32[]{:S(2)}, u32[]{:S(2)}) collective-permute-start(bf16[2048,256]{1,0:T(8,128)(2,1)S(1)} %bitcast.15), channel_id=1, source_target_pairs={{0,1},{1,0},{2,3},{3,2},{4,5},{5,4},{6,7},{7,6},{8,9},{9,8},{10,11... | collective-permute-start | bytes 3145736 | tf_op jit(solution)/shard_map/ppermute | solution.py:414
  27.7 41.9 %collective-permute-start.3 = (bf16[2048,256]{1,0:T(8,128)(2,1)}, bf16[2048,256]{1,0:T(8,128)(2,1)}, u32[]{:S(2)}, u32[]{:S(2)}) collective-permute-start(bf16[2048,256]{1,0:T(8,128)(2,1)} %bitcast.6.refs_4_), channel_id=1, source_target_pairs={{0,2},{1,3},{2,0},{3,1},{4,6},{5,7},{6,4},{7,5},{8,10},{9,11},{10,... | collective-permute-start | bytes 3145736 | tf_op jit(solution)/shard_map/ppermute | solution.py:406
  29.8 67.6 %collective-permute-start.4 = (bf16[2048,256]{1,0:T(8,128)(2,1)}, bf16[2048,256]{1,0:T(8,128)(2,1)}, u32[]{:S(2)}, u32[]{:S(2)}) collective-permute-start(bf16[2048,256]{1,0:T(8,128)(2,1)} %bitcast.6.refs_4_), channel_id=1, source_target_pairs={{0,1},{1,0},{2,3},{3,2},{4,5},{5,4},{6,7},{7,6},{8,9},{9,8},{10,11... | collective-permute-start | bytes 3145736 | tf_op jit(solution)/shard_map/ppermute | solution.py:414
  32.0 60.0 %collective-permute-start.6 = (bf16[256,2048]{1,0:T(8,128)(2,1)}, bf16[256,2048]{1,0:T(8,128)(2,1)}, u32[]{:S(2)}, u32[]{:S(2)}) collective-permute-start(bf16[256,2048]{1,0:T(8,128)(2,1)} %bitcast.7.refs_0_), channel_id=1, source_target_pairs={{0,2},{1,3},{2,0},{3,1},{4,6},{5,7},{6,4},{7,5},{8,10},{9,11},{10,... | collective-permute-start | bytes 3145736 | tf_op jit(solution)/shard_map/ppermute | solution.py:406
  36.0 0.9 copy-start.8
  36.1 0.8 copy-start.9
  47.1 50.3 %collective-permute-start.2 = (bf16[2048,256]{1,0:T(8,128)(2,1)}, bf16[2048,256]{1,0:T(8,128)(2,1)}, u32[]{:S(2)}, u32[]{:S(2)}) collective-permute-start(bf16[2048,256]{1,0:T(8,128)(2,1)} %collective-permute-done.refs_1_), channel_id=1, source_target_pairs={{0,1},{1,0},{2,3},{3,2},{4,5},{5,4},{6,7},{7,6},{8,9},{9,8},{10,11... | collective-permute-start | bytes 3145736 | tf_op jit(solution)/shard_map/ppermute | solution.py:414
  69.6 27.9 %collective-permute-start.5 = (bf16[2048,256]{1,0:T(8,128)(2,1)}, bf16[2048,256]{1,0:T(8,128)(2,1)}, u32[]{:S(2)}, u32[]{:S(2)}) collective-permute-start(bf16[2048,256]{1,0:T(8,128)(2,1)} %collective-permute-done.3.refs_5_), channel_id=1, source_target_pairs={{0,1},{1,0},{2,3},{3,2},{4,5},{5,4},{6,7},{7,6},{8,9},{9,8},{10,11... | collective-permute-start | bytes 3145736 | tf_op jit(solution)/shard_map/ppermute | solution.py:414
  75.7 28.1 %all-to-all-start.1 = ((bf16[8,160,256]{2,1,0:T(8,128)(2,1)}), bf16[8,160,256]{2,1,0:T(8,128)(2,1)S(1)}, u32[]{:S(2)}, u32[]{:S(2)}) async-start(bf16[8,160,256]{2,1,0:T(8,128)(2,1)} %broadcast_in_dim.7), calls=%async_computation.1 | async-start | bytes 1310720 | tf_op jit(solution)/shard_map/all_to_all | solution.py:46
  83.2 38.6 %collective-permute-start.7 = (bf16[256,2048]{1,0:T(8,128)(2,1)}, bf16[256,2048]{1,0:T(8,128)(2,1)}, u32[]{:S(2)}, u32[]{:S(2)}) collective-permute-start(bf16[256,2048]{1,0:T(8,128)(2,1)} %bitcast.7.refs_0_), channel_id=1, source_target_pairs={{0,1},{1,0},{2,3},{3,2},{4,5},{5,4},{6,7},{7,6},{8,9},{9,8},{10,11... | collective-permute-start | bytes 3145736 | tf_op jit(solution)/shard_map/ppermute | solution.py:414
  92.1 29.8 %collective-permute-start.8 = (bf16[256,2048]{1,0:T(8,128)(2,1)}, bf16[256,2048]{1,0:T(8,128)(2,1)}, u32[]{:S(2)}, u32[]{:S(2)}) collective-permute-start(bf16[256,2048]{1,0:T(8,128)(2,1)} %collective-permute-done.6.refs_1_), channel_id=1, source_target_pairs={{0,1},{1,0},{2,3},{3,2},{4,5},{5,4},{6,7},{7,6},{8,9},{9,8},{10,11... | collective-permute-start | bytes 3145736 | tf_op jit(solution)/shard_map/ppermute | solution.py:414
  96.4 0.8 slice-start.1
  118.3 8.9 %all-to-all-start.3 = ((bf16[4,256,128]{2,1,0:T(8,128)(2,1)}), bf16[4,256,128]{2,1,0:T(8,128)(2,1)S(1)}, u32[]{:S(2)}, u32[]{:S(2)}) async-start(bf16[4,256,128]{2,1,0:T(8,128)(2,1)} %shard_map.144), calls=%async_computation.3 | async-start | bytes 524288 | tf_op jit(solution)/shard_map/all_to_all | solution.py:454
  131.3 39.9 %all-to-all-start.4 = ((bf16[8,192,256]{2,1,0:T(8,128)(2,1)}), bf16[8,192,256]{2,1,0:T(8,128)(2,1)S(1)}, u32[]{:S(2)}, u32[]{:S(2)}) async-start(bf16[8,192,256]{2,1,0:T(8,128)(2,1)} %shard_map.146.refs_0_), calls=%async_computation.4 | async-start | bytes 1572864 | tf_op jit(solution)/shard_map/all_to_all | solution.py:459
  172.5 7.6 %copy-start.7 = (f32[256,2]{0,1:T(2,128)S(1)}, f32[256,2]{0,1:T(2,128)}, u32[]{:S(2)}) copy-start(f32[256,2]{0,1:T(2,128)} %param.22) | copy-start | bytes 6148
  172.5 18.2 %all-to-all-start.5 = ((bf16[32,24,128]{2,1,0:T(8,128)(2,1)}), bf16[32,24,128]{2,1,0:T(8,128)(2,1)S(1)}, u32[]{:S(2)}, u32[]{:S(2)}) async-start(bf16[32,24,128]{2,1,0:T(8,128)(2,1)} %shard_map.148), calls=%async_computation.5 | async-start | bytes 393216 | tf_op jit(solution)/shard_map/all_to_all | solution.py:471
  191.9 4.9 %collective-permute-start.9 = (f32[256,128]{1,0:T(8,128)S(1)}, f32[256,128]{1,0:T(8,128)S(1)}, u32[]{:S(2)}, u32[]{:S(2)}) collective-permute-start(f32[256,128]{1,0:T(8,128)S(1)} %get-tuple-element.9), channel_id=1, source_target_pairs={{0,1},{1,0},{2,3},{3,2},{4,5},{5,4},{6,7},{7,6},{8,9},{9,8},{10,11... | collective-permute-start | bytes 393224 | tf_op jit(solution)/shard_map/ppermute | solution.py:475
  (3 other events, 2.1 us)

commit v5 on v4

--- a/solution.py
+++ b/solution.py
@@ -190,15 +190,15 @@
     )(parts, *earlier)
 
 
-def attend(query, key_value, score_scale):
+def attend(index, query, key_value, score_scale, *earlier):
     blocks, rows, _ = query.shape
     pieces, _, length = key_value.shape
     factor = score_scale * math.log2(math.e)
     first_value = PLAIN_HEAD_DIM + ROPE
 
-    def body(query_ref, key_ref, out_ref):
-        for i in range(blocks):
-            q = query_ref[i]
+    def body(index_ref, query_ref, key_ref, *refs):
+        for i, out_ref in enumerate(refs[-blocks:]):
+            q = query_ref[(index_ref[0] + i) % blocks]
             scores = [
                 jnp.dot(q, key_ref[j, :LANES, :], preferred_element_type=jnp.float32)
                 for j in range(pieces)
@@ -220,30 +220,31 @@
                 )
                 mixed = part if mixed is None else mixed + part
             total = jnp.sum(total, axis=1, keepdims=True)
-            out_ref[i, :, :VALUE_HEAD_DIM] = (mixed / total).astype(jnp.bfloat16)
+            out_ref[:, :VALUE_HEAD_DIM] = (mixed / total).astype(jnp.bfloat16)
             log_total = top + jnp.log2(total)
             high = log_total.astype(jnp.bfloat16).astype(jnp.float32)
             middle = (log_total - high).astype(jnp.bfloat16).astype(jnp.float32)
             low = log_total - high - middle
             lane = lax.broadcasted_iota(jnp.int32, (rows, LANES - VALUE_HEAD_DIM), 1)
-            out_ref[i, :, VALUE_HEAD_DIM:] = jnp.where(
+            out_ref[:, VALUE_HEAD_DIM:] = jnp.where(
                 lane == 0, high, jnp.where(lane == 1, middle, low)
             ).astype(jnp.bfloat16)
 
     return kernel_call(
         body,
-        jax.ShapeDtypeStruct((blocks, rows, LANES), jnp.bfloat16),
-        [VMEM, VMEM],
-        VMEM,
+        tuple(jax.ShapeDtypeStruct((rows, LANES), jnp.bfloat16) for _ in range(blocks)),
+        [SMEM, VMEM, VMEM] + [ANY] * len(earlier),
+        (VMEM,) * blocks,
         4 * blocks * rows * pieces * length * 2 * LANES,
-    )(query, key_value)
+    )(index, query, key_value, *earlier)
 
 
 def merge(partials):
-    count, rows, _ = partials.shape
-
-    def body(in_ref, out_ref):
-        values = [in_ref[i].astype(jnp.float32) for i in range(count)]
+    rows = partials[0].shape[0]
+
+    def body(*refs):
+        out_ref = refs[-1]
+        values = [r[...].astype(jnp.float32) for r in refs[:-1]]
         first = VALUE_HEAD_DIM
         logs = [
             v[:, first : first + 1] + v[:, first + 1 : first + 2] + v[:, first + 2 : first + 3]
@@ -263,10 +264,10 @@
     return kernel_call(
         body,
         jax.ShapeDtypeStruct((VALUE_HEAD_DIM, rows), jnp.bfloat16),
-        [VMEM],
+        [VMEM] * len(partials),
         VMEM,
         1,
-    )(partials)
+    )(*partials)
 
 
 def hidden_units(messages, gates, ups):
@@ -411,7 +412,8 @@
         arrived = lax.all_to_all(outgoing, "ep", 0, 0, tiled=True)
 
         for group in groups_of:
-            group += [lax.ppermute(weight, "tp", partner) for weight in group[:2]]
+            for weight in group[:2]:
+                group.append(lax.ppermute(weight, "tp", partner))
         gates, ups, downs = groups_of
 
         positions = (ep_index * row_count + jnp.arange(row_count, dtype=jnp.int32)).astype(
@@ -450,20 +452,34 @@
         key_value = to_everyone(sequenced(own_pack, arrived), "ep", z_groups, z_count)
         hidden = hidden_units(arrived, gates, ups)
         query_all = to_everyone(sequenced(query, key_value, hidden), "ep", x_groups, x_count)
-        partial_all = attend(query_all, key_value, (PLAIN_HEAD_DIM + ROPE) ** (-0.5))
-        partials = lax.all_to_all(
-            partial_all, "ep", 0, 0, tiled=True, axis_index_groups=x_groups
-        )
-
-        partial_out = project_down(hidden, downs, y_count, partials)
+
+        partial_out = project_down(hidden, downs, y_count, query_all)
         groups = lax.all_to_all(
             partial_out, "tp", 0, 0, tiled=True, axis_index_groups=y_groups
         )
+
+        partial_all = attend(
+            (ep_index % x_count).reshape(1),
+            query_all,
+            key_value,
+            (PLAIN_HEAD_DIM + ROPE) ** (-0.5),
+            partial_out,
+        )
+        partials = [partial_all[0]] + [
+            lax.ppermute(
+                partial_all[i],
+                "ep",
+                [
+                    (x_count * z + x, x_count * z + (x + i) % x_count)
+                    for z in range(z_count)
+                    for x in range(x_count)
+                ],
+            )
+            for i in range(1, x_count)
+        ]
         attended = merge(partials)
-        everyone = lax.all_gather(
-            sequenced(attended, partial_out), "tp", axis=0, tiled=True
-        )
-        summed = add_up(groups, ep_count, everyone)
+        summed = add_up(groups, ep_count, attended)
+        everyone = lax.all_gather(sequenced(attended, summed), "tp", axis=0, tiled=True)
         attention_out = lax.dot_general(
             everyone, out_proj, (((0,), (0,)), ((), ())), preferred_element_type=jnp.float32
         ).astype(jnp.bfloat16)

time: 199 us -> 182 us (0.915)
  blocking collectives: 42.8 us -> 16.8 us
  starting transfers between devices: 72.4 us -> 79.3 us
  waiting for transfers between devices: 48.9 us -> 51.7 us
    all_gather x1, blocking collectives: 32.5 us -> 16.8 us  [local(): lax.all_gather(sequenced(attended, summed), 'tp', axis=0, tiled=True)]
    all_to_all x1, waiting for transfers between devices: 10.5 us -> 0.01 us  [local(): returned = lax.all_to_all(summed, 'ep', 0, 0, tiled=True)]
    all_to_all x1 -> x0, blocking collectives: 10.3 us -> none  [to_everyone(): lax.all_to_all(jnp.broadcast_to(array[None], (count, *array.shape)), axis...]
    ppermute x6 -> x9, starting transfers between devices: 21.5 us -> 29.9 us  [the longest x6 21.5 us: local(): group.append(lax.ppermute(weight, 'tp', partner))]
    all_to_all x1, waiting for transfers between devices: 0.01 us -> 6.44 us  [local(): lax.all_to_all(partial_out, 'tp', 0, 0, tiled=True, axis_index_groups=y_g...]
    all_to_all x1 -> x2, waiting for transfers between devices: 0.01 us -> 6.18 us  [to_everyone(): lax.all_to_all(jnp.broadcast_to(array[None], (count, *array.shape)), axis...]
    all_to_all x1 -> x0, waiting for transfers between devices: 5.3 us -> none  [local(): lax.all_to_all(partial_all, 'ep', 0, 0, tiled=True, axis_index_groups=x_g...]
    ppermute x6 -> x9, waiting for transfers between devices: 0.02 us -> 4.59 us  [the longest x3 4.57 us: local(): lax.ppermute(partial_all[i], 'ep', [(x_count * z + x, x_count * z + (x +...]
  transfers between devices with their start and end apart: 15 -> 18, of which waited for: 5 -> 7; matrix products, arithmetic and copies ran while one was open for 2% -> 3% of each run, Pallas kernels for 6% -> 6%
where the time goes in v5:
time: 182 us; the launch traced here: 181 us
  starting transfers between devices  79.3 us (44%)
  waiting for transfers between devices  51.7 us (28%)
  Pallas kernels  20.9 us (11%)
  blocking collectives  16.8 us (9%)
  local copies, waits for them, and re-layouts  7.46 us (4%)
  other arithmetic  2.18 us (1%)
    ppermute x3, waiting for transfers between devices, local(): group.append(lax.ppermute(group[0], 'tp', neighbour))  34.3 us
    ppermute x6, starting transfers between devices, local(): group.append(lax.ppermute(weight, 'tp', partner))  21.5 us
    all_gather x1, blocking collectives, local(): lax.all_gather(sequenced(attended, summed), 'tp', axis=0, tiled=True)  16.8 us
    all_to_all x1, starting transfers between devices, local(): arrived = lax.all_to_all(outgoing, 'ep', 0, 0, tiled=True)  13.8 us
    all_to_all x2, starting transfers between devices, to_everyone(): lax.all_to_all(jnp.broadcast_to(array[None], (count, *array.shape)), axis...  10.7 us
    ppermute x3, starting transfers between devices, local(): group.append(lax.ppermute(group[0], 'tp', neighbour))  8.49 us
    ppermute x3, starting transfers between devices, local(): lax.ppermute(partial_all[i], 'ep', [(x_count * z + x, x_count * z + (x +...  8.41 us
    all_to_all x1, starting transfers between devices, local(): returned = lax.all_to_all(summed, 'ep', 0, 0, tiled=True)  7.47 us
  transfers between devices with their start and end apart: 18, of which 7 were waited for; matrix products, arithmetic and copies ran while one was open for 3% of the time, Pallas kernels for 6%

profile of v5, /device:TPU:1, one launch (start us, length us, event | category | flops | bytes accessed | tf_op | source)
XLA Modules:
  0.0 180.7 jit_solution(13994307021312287672)
XLA Ops:
  3.5 4.0 %shard_map.140 = (bf16[32,4,24,128]{3,2,1,0:T(8,128)(2,1)}, s32[256,4]{1,0:T(8,128)S(1)}) custom-call(s32[2]{0:T(128)S(1)} %pad_add_fusion.index_ref, bf16[256,2048]{1,0:T(8,128)(2,1)S(1)} %copy-done.2, f32[1,2048]{1,0:T(1,128)S(1)} %bitcast.19, s32[256,2]{1,0:T(8,128)S(1)} %copy.34.routes_ref), custom_call_target="tpu_custom_call" | custom-call | flops 805306368 | tf_op jit(solution)/shard_map/pallas_call | solution.py:147
  7.5 13.8 %all-to-all-start = ((bf16[32,4,24,128]{3,2,1,0:T(8,128)(2,1)}), bf16[32,4,24,128]{3,2,1,0:T(8,128)(2,1)S(1)}, u32[]{:S(2)}, u32[]{:S(2)}) async-start(bf16[32,4,24,128]{3,2,1,0:T(8,128)(2,1)} %get-tuple-element.10), calls=%async_computation | async-start | bytes 1572864 | tf_op jit(solution)/shard_map/all_to_all | solution.py:412
  21.4 3.2 %collective-permute-start = (bf16[2048,256]{1,0:T(8,128)(2,1)S(1)}, bf16[2048,256]{1,0:T(8,128)(2,1)}, u32[]{:S(2)}, u32[]{:S(2)}) collective-permute-start(bf16[2048,256]{1,0:T(8,128)(2,1)S(1)} %bitcast.15), channel_id=1, source_target_pairs={{0,2},{1,3},{2,0},{3,1},{4,6},{5,7},{6,4},{7,5},{8,10},{9,11},{10,... | collective-permute-start | bytes 3145736 | tf_op jit(solution)/shard_map/ppermute | solution.py:407
  24.6 3.1 %collective-permute-start.1 = (bf16[2048,256]{1,0:T(8,128)(2,1)S(1)}, bf16[2048,256]{1,0:T(8,128)(2,1)}, u32[]{:S(2)}, u32[]{:S(2)}) collective-permute-start(bf16[2048,256]{1,0:T(8,128)(2,1)S(1)} %bitcast.16), channel_id=1, source_target_pairs={{0,1},{1,0},{2,3},{3,2},{4,5},{5,4},{6,7},{7,6},{8,9},{9,8},{10,11... | collective-permute-start | bytes 3145736 | tf_op jit(solution)/shard_map/ppermute | solution.py:416
  32.0 3.2 %collective-permute-start.6 = (bf16[256,2048]{1,0:T(8,128)(2,1)}, bf16[256,2048]{1,0:T(8,128)(2,1)}, u32[]{:S(2)}, u32[]{:S(2)}) collective-permute-start(bf16[256,2048]{1,0:T(8,128)(2,1)} %bitcast.8.refs_0_), channel_id=1, source_target_pairs={{0,2},{1,3},{2,0},{3,1},{4,6},{5,7},{6,4},{7,5},{8,10},{9,11},{10,... | collective-permute-start | bytes 3145736 | tf_op jit(solution)/shard_map/ppermute | solution.py:407
  37.6 9.5 %collective-permute-done.refs_1_ = bf16[2048,256]{1,0:T(8,128)(2,1)} collective-permute-done((bf16[2048,256]{1,0:T(8,128)(2,1)S(1)}, bf16[2048,256]{1,0:T(8,128)(2,1)}, u32[]{:S(2)}, u32[]{:S(2)}) %collective-permute-start) | collective-permute-done | bytes 1048608 | tf_op jit(solution)/shard_map/ppermute | solution.py:407
  47.1 5.1 %collective-permute-start.2 = (bf16[2048,256]{1,0:T(8,128)(2,1)}, bf16[2048,256]{1,0:T(8,128)(2,1)}, u32[]{:S(2)}, u32[]{:S(2)}) collective-permute-start(bf16[2048,256]{1,0:T(8,128)(2,1)} %collective-permute-done.refs_1_), channel_id=1, source_target_pairs={{0,1},{1,0},{2,3},{3,2},{4,5},{5,4},{6,7},{7,6},{8,9},{9,8},{10,11... | collective-permute-start | bytes 3145736 | tf_op jit(solution)/shard_map/ppermute | solution.py:416
  52.2 17.3 %collective-permute-done.3.refs_5_ = bf16[2048,256]{1,0:T(8,128)(2,1)} collective-permute-done((bf16[2048,256]{1,0:T(8,128)(2,1)}, bf16[2048,256]{1,0:T(8,128)(2,1)}, u32[]{:S(2)}, u32[]{:S(2)}) %collective-permute-start.3) | collective-permute-done | bytes 1048608 | tf_op jit(solution)/shard_map/ppermute | solution.py:407
  69.6 5.1 %collective-permute-start.5 = (bf16[2048,256]{1,0:T(8,128)(2,1)}, bf16[2048,256]{1,0:T(8,128)(2,1)}, u32[]{:S(2)}, u32[]{:S(2)}) collective-permute-start(bf16[2048,256]{1,0:T(8,128)(2,1)} %collective-permute-done.3.refs_5_), channel_id=1, source_target_pairs={{0,1},{1,0},{2,3},{3,2},{4,5},{5,4},{6,7},{7,6},{8,9},{9,8},{10,11... | collective-permute-start | bytes 3145736 | tf_op jit(solution)/shard_map/ppermute | solution.py:416
  75.7 6.7 %all-to-all-start.1 = ((bf16[8,160,256]{2,1,0:T(8,128)(2,1)}), bf16[8,160,256]{2,1,0:T(8,128)(2,1)S(1)}, u32[]{:S(2)}, u32[]{:S(2)}) async-start(bf16[8,160,256]{2,1,0:T(8,128)(2,1)} %broadcast_in_dim.7), calls=%async_computation.1 | async-start | bytes 1310720 | tf_op jit(solution)/shard_map/all_to_all | solution.py:46
  84.6 7.5 %collective-permute-done.6.refs_1_ = bf16[256,2048]{1,0:T(8,128)(2,1)} collective-permute-done((bf16[256,2048]{1,0:T(8,128)(2,1)}, bf16[256,2048]{1,0:T(8,128)(2,1)}, u32[]{:S(2)}, u32[]{:S(2)}) %collective-permute-start.6) | collective-permute-done | bytes 1048608 | tf_op jit(solution)/shard_map/ppermute | solution.py:407
  92.1 3.7 %collective-permute-start.8 = (bf16[256,2048]{1,0:T(8,128)(2,1)}, bf16[256,2048]{1,0:T(8,128)(2,1)}, u32[]{:S(2)}, u32[]{:S(2)}) collective-permute-start(bf16[256,2048]{1,0:T(8,128)(2,1)} %collective-permute-done.6.refs_1_), channel_id=1, source_target_pairs={{0,1},{1,0},{2,3},{3,2},{4,5},{5,4},{6,7},{7,6},{8,9},{9,8},{10,11... | collective-permute-start | bytes 3145736 | tf_op jit(solution)/shard_map/ppermute | solution.py:416
  98.3 6.2 %shard_map.142.refs_1_.hidden_ref = bf16[4,192,256]{2,1,0:T(8,128)(2,1)S(1)} custom-call(bf16[32,4,24,128]{3,2,1,0:T(8,128)(2,1)S(1)} %all-to-all-done.refs_0_.rows_ref, bf16[2048,256]{1,0:T(8,128)(2,1)S(1)} %bitcast.17, bf16[2048,256]{1,0:T(8,128)(2,1)} %collective-permute-done.refs_1_, bf16[2048,256]{1,0:T(8,128)(2,1)} %collective-permute-done.1.refs_2_, ...), custom_call_target="tpu_custom_call" | custom-call | flops 1610612736 | tf_op jit(solution)/shard_map/pallas_call | solution.py:308
  105.3 4.0 %all-to-all-start.2 = ((bf16[4,256,128]{2,1,0:T(8,128)(2,1)}), bf16[4,256,128]{2,1,0:T(8,128)(2,1)S(1)}, u32[]{:S(2)}, u32[]{:S(2)}) async-start(bf16[4,256,128]{2,1,0:T(8,128)(2,1)} %broadcast_in_dim.8), calls=%async_computation.2 | async-start | bytes 524288 | tf_op jit(solution)/shard_map/all_to_all | solution.py:46
  109.3 6.2 %all-to-all-done.2.refs_4_.query_ref = bf16[4,256,128]{2,1,0:T(8,128)(2,1)S(1)} async-done(((bf16[4,256,128]{2,1,0:T(8,128)(2,1)}), bf16[4,256,128]{2,1,0:T(8,128)(2,1)S(1)}, u32[]{:S(2)}, u32[]{:S(2)}) %all-to-all-start.2) | async-done | bytes 262176 | tf_op jit(solution)/shard_map/all_to_all | solution.py:46
  115.5 4.1 %shard_map.144.refs_0_ = bf16[8,192,256]{2,1,0:T(8,128)(2,1)} custom-call(bf16[4,192,256]{2,1,0:T(8,128)(2,1)S(1)} %shard_map.142.refs_1_.hidden_ref, bf16[256,2048]{1,0:T(8,128)(2,1)} %bitcast.8.refs_0_, bf16[256,2048]{1,0:T(8,128)(2,1)} %collective-permute-done.6.refs_1_, bf16[256,2048]{1,0:T(8,128)(2,1)} %collective-permute-done.7.refs_2_, ...), custom_call_target="tpu_custom_call" | custom-call | flops 805306368 | tf_op jit(solution)/shard_map/pallas_call | solution.py:333
  119.6 6.8 %all-to-all-start.3 = ((bf16[8,192,256]{2,1,0:T(8,128)(2,1)}), bf16[8,192,256]{2,1,0:T(8,128)(2,1)S(1)}, u32[]{:S(2)}, u32[]{:S(2)}) async-start(bf16[8,192,256]{2,1,0:T(8,128)(2,1)} %shard_map.144.refs_0_), calls=%async_computation.3 | async-start | bytes 1572864 | tf_op jit(solution)/shard_map/all_to_all | solution.py:457
  126.4 3.5 %shard_map.145 = (bf16[256,128]{1,0:T(8,128)(2,1)S(1)}, bf16[256,128]{1,0:T(8,128)(2,1)S(1)}, bf16[256,128]{1,0:T(8,128)(2,1)S(1)}, bf16[256,128]{1,0:T(8,128)(2,1)S(1)}) custom-call(s32[1]{0:T(128)} %bitcast.index_ref, bf16[4,256,128]{2,1,0:T(8,128)(2,1)S(1)} %all-to-all-done.2.refs_4_.query_ref, bf16[8,160,256]{2,1,0:T(8,128)(2,1)S(1)} %all-to-all-done.1.refs_0_.key_ref, ...), custom_call_target="tpu_custom_call" | custom-call | flops 2147483648 | tf_op jit(solution)/shard_map/pallas_call | solution.py:233
  129.9 2.5 %collective-permute-start.10 = (bf16[256,128]{1,0:T(8,128)(2,1)S(1)}, bf16[256,128]{1,0:T(8,128)(2,1)S(1)}, u32[]{:S(2)}, u32[]{:S(2)}) collective-permute-start(bf16[256,128]{1,0:T(8,128)(2,1)S(1)} %get-tuple-element.13), channel_id=1, source_target_pairs={{0,32},{16,48},{32,0},{48,16},{64,96},{80,112},{96,64},{112,80},{1... | collective-permute-start | bytes 196616 | tf_op jit(solution)/shard_map/ppermute | solution.py:469
  132.4 4.0 %collective-permute-start.11 = (bf16[256,128]{1,0:T(8,128)(2,1)S(1)}, bf16[256,128]{1,0:T(8,128)(2,1)S(1)}, u32[]{:S(2)}, u32[]{:S(2)}) collective-permute-start(bf16[256,128]{1,0:T(8,128)(2,1)S(1)} %get-tuple-element.14), channel_id=1, source_target_pairs={{0,48},{16,0},{32,16},{48,32},{64,112},{80,64},{96,80},{112,96},{1... | collective-permute-start | bytes 196616 | tf_op jit(solution)/shard_map/ppermute | solution.py:469
  138.4 4.6 %collective-permute-done.9.refs_1_ = bf16[256,128]{1,0:T(8,128)(2,1)S(1)} collective-permute-done((bf16[256,128]{1,0:T(8,128)(2,1)S(1)}, bf16[256,128]{1,0:T(8,128)(2,1)S(1)}, u32[]{:S(2)}, u32[]{:S(2)}) %collective-permute-start.9) | collective-permute-done | bytes 65568 | tf_op jit(solution)/shard_map/ppermute | solution.py:469
  143.5 6.4 %all-to-all-done.3.in_ref = bf16[8,192,256]{2,1,0:T(8,128)(2,1)S(1)} async-done(((bf16[8,192,256]{2,1,0:T(8,128)(2,1)}), bf16[8,192,256]{2,1,0:T(8,128)(2,1)S(1)}, u32[]{:S(2)}, u32[]{:S(2)}) %all-to-all-start.3) | async-done | bytes 786464 | tf_op jit(solution)/shard_map/all_to_all | solution.py:457
  151.2 7.5 %all-to-all-start.4 = ((bf16[32,24,128]{2,1,0:T(8,128)(2,1)}), bf16[32,24,128]{2,1,0:T(8,128)(2,1)S(1)}, u32[]{:S(2)}, u32[]{:S(2)}) async-start(bf16[32,24,128]{2,1,0:T(8,128)(2,1)} %shard_map.147.refs_0_), calls=%async_computation.4 | async-start | bytes 393216 | tf_op jit(solution)/shard_map/all_to_all | solution.py:487
  158.9 16.8 %all_gather.3 = bf16[1024,256]{1,0:T(8,128)(2,1)S(1)} all-gather(bf16[64,256]{1,0:T(8,128)(2,1)S(1)} %shard_map.148), channel_id=1, replica_groups=mesh['ep'=32,'tp'=16] {'tp'}, dimensions={0}, use_global_device_ids=true | all-gather | bytes 557056 | tf_op jit(solution)/shard_map/all_gather | solution.py:482
  (74 shorter events, 24.6 us)
Async XLA Ops:
  0.6 178.3 %copy-start = (bf16[1024,128]{1,0:T(8,128)(2,1)S(1)}, bf16[1024,128]{1,0:T(8,128)(2,1)}, u32[]{:S(2)}) copy-start(bf16[1024,128]{1,0:T(8,128)(2,1)} %param.18) | copy-start | bytes 786436
  2.2 1.2 copy-start.2
  7.5 13.9 %copy-start.1 = (bf16[1,2048,256]{2,1,0:T(8,128)(2,1)S(1)}, bf16[1,2048,256]{2,1,0:T(8,128)(2,1)}, u32[]{:S(2)}) copy-start(bf16[1,2048,256]{2,1,0:T(8,128)(2,1)} %param.23) | copy-start | bytes 3145732
  7.5 27.7 %copy-start.5 = (bf16[256,32]{0,1:T(8,128)(2,1)S(1)}, bf16[256,32]{0,1:T(8,128)(2,1)}, u32[]{:S(2)}) copy-start(bf16[256,32]{0,1:T(8,128)(2,1)} %param.15) | copy-start | bytes 49156
  7.5 67.2 %all-to-all-start = ((bf16[32,4,24,128]{3,2,1,0:T(8,128)(2,1)}), bf16[32,4,24,128]{3,2,1,0:T(8,128)(2,1)S(1)}, u32[]{:S(2)}, u32[]{:S(2)}) async-start(bf16[32,4,24,128]{3,2,1,0:T(8,128)(2,1)} %get-tuple-element.10), calls=%async_computation | async-start | bytes 1572864 | tf_op jit(solution)/shard_map/all_to_all | solution.py:412
  21.4 25.8 %collective-permute-start = (bf16[2048,256]{1,0:T(8,128)(2,1)S(1)}, bf16[2048,256]{1,0:T(8,128)(2,1)}, u32[]{:S(2)}, u32[]{:S(2)}) collective-permute-start(bf16[2048,256]{1,0:T(8,128)(2,1)S(1)} %bitcast.15), channel_id=1, source_target_pairs={{0,2},{1,3},{2,0},{3,1},{4,6},{5,7},{6,4},{7,5},{8,10},{9,11},{10,... | collective-permute-start | bytes 3145736 | tf_op jit(solution)/shard_map/ppermute | solution.py:407
  24.6 57.8 %collective-permute-start.1 = (bf16[2048,256]{1,0:T(8,128)(2,1)S(1)}, bf16[2048,256]{1,0:T(8,128)(2,1)}, u32[]{:S(2)}, u32[]{:S(2)}) collective-permute-start(bf16[2048,256]{1,0:T(8,128)(2,1)S(1)} %bitcast.16), channel_id=1, source_target_pairs={{0,1},{1,0},{2,3},{3,2},{4,5},{5,4},{6,7},{7,6},{8,9},{9,8},{10,11... | collective-permute-start | bytes 3145736 | tf_op jit(solution)/shard_map/ppermute | solution.py:416
  27.7 41.9 %collective-permute-start.3 = (bf16[2048,256]{1,0:T(8,128)(2,1)}, bf16[2048,256]{1,0:T(8,128)(2,1)}, u32[]{:S(2)}, u32[]{:S(2)}) collective-permute-start(bf16[2048,256]{1,0:T(8,128)(2,1)} %bitcast.7.refs_4_), channel_id=1, source_target_pairs={{0,2},{1,3},{2,0},{3,1},{4,6},{5,7},{6,4},{7,5},{8,10},{9,11},{10,... | collective-permute-start | bytes 3145736 | tf_op jit(solution)/shard_map/ppermute | solution.py:407
  29.8 68.5 %collective-permute-start.4 = (bf16[2048,256]{1,0:T(8,128)(2,1)}, bf16[2048,256]{1,0:T(8,128)(2,1)}, u32[]{:S(2)}, u32[]{:S(2)}) collective-permute-start(bf16[2048,256]{1,0:T(8,128)(2,1)} %bitcast.7.refs_4_), channel_id=1, source_target_pairs={{0,1},{1,0},{2,3},{3,2},{4,5},{5,4},{6,7},{7,6},{8,9},{9,8},{10,11... | collective-permute-start | bytes 3145736 | tf_op jit(solution)/shard_map/ppermute | solution.py:416
  32.0 60.0 %collective-permute-start.6 = (bf16[256,2048]{1,0:T(8,128)(2,1)}, bf16[256,2048]{1,0:T(8,128)(2,1)}, u32[]{:S(2)}, u32[]{:S(2)}) collective-permute-start(bf16[256,2048]{1,0:T(8,128)(2,1)} %bitcast.8.refs_0_), channel_id=1, source_target_pairs={{0,2},{1,3},{2,0},{3,1},{4,6},{5,7},{6,4},{7,5},{8,10},{9,11},{10,... | collective-permute-start | bytes 3145736 | tf_op jit(solution)/shard_map/ppermute | solution.py:407
  35.4 1.0 copy-start.4
  47.1 51.2 %collective-permute-start.2 = (bf16[2048,256]{1,0:T(8,128)(2,1)}, bf16[2048,256]{1,0:T(8,128)(2,1)}, u32[]{:S(2)}, u32[]{:S(2)}) collective-permute-start(bf16[2048,256]{1,0:T(8,128)(2,1)} %collective-permute-done.refs_1_), channel_id=1, source_target_pairs={{0,1},{1,0},{2,3},{3,2},{4,5},{5,4},{6,7},{7,6},{8,9},{9,8},{10,11... | collective-permute-start | bytes 3145736 | tf_op jit(solution)/shard_map/ppermute | solution.py:416
  69.6 28.7 %collective-permute-start.5 = (bf16[2048,256]{1,0:T(8,128)(2,1)}, bf16[2048,256]{1,0:T(8,128)(2,1)}, u32[]{:S(2)}, u32[]{:S(2)}) collective-permute-start(bf16[2048,256]{1,0:T(8,128)(2,1)} %collective-permute-done.3.refs_5_), channel_id=1, source_target_pairs={{0,1},{1,0},{2,3},{3,2},{4,5},{5,4},{6,7},{7,6},{8,9},{9,8},{10,11... | collective-permute-start | bytes 3145736 | tf_op jit(solution)/shard_map/ppermute | solution.py:416
  75.7 28.9 %all-to-all-start.1 = ((bf16[8,160,256]{2,1,0:T(8,128)(2,1)}), bf16[8,160,256]{2,1,0:T(8,128)(2,1)S(1)}, u32[]{:S(2)}, u32[]{:S(2)}) async-start(bf16[8,160,256]{2,1,0:T(8,128)(2,1)} %broadcast_in_dim.7), calls=%async_computation.1 | async-start | bytes 1310720 | tf_op jit(solution)/shard_map/all_to_all | solution.py:46
  82.4 26.9 %collective-permute-start.7 = (bf16[256,2048]{1,0:T(8,128)(2,1)}, bf16[256,2048]{1,0:T(8,128)(2,1)}, u32[]{:S(2)}, u32[]{:S(2)}) collective-permute-start(bf16[256,2048]{1,0:T(8,128)(2,1)} %bitcast.8.refs_0_), channel_id=1, source_target_pairs={{0,1},{1,0},{2,3},{3,2},{4,5},{5,4},{6,7},{7,6},{8,9},{9,8},{10,11... | collective-permute-start | bytes 3145736 | tf_op jit(solution)/shard_map/ppermute | solution.py:416
  92.1 17.2 %collective-permute-start.8 = (bf16[256,2048]{1,0:T(8,128)(2,1)}, bf16[256,2048]{1,0:T(8,128)(2,1)}, u32[]{:S(2)}, u32[]{:S(2)}) collective-permute-start(bf16[256,2048]{1,0:T(8,128)(2,1)} %collective-permute-done.6.refs_1_), channel_id=1, source_target_pairs={{0,1},{1,0},{2,3},{3,2},{4,5},{5,4},{6,7},{7,6},{8,9},{9,8},{10,11... | collective-permute-start | bytes 3145736 | tf_op jit(solution)/shard_map/ppermute | solution.py:416
  105.3 10.2 %all-to-all-start.2 = ((bf16[4,256,128]{2,1,0:T(8,128)(2,1)}), bf16[4,256,128]{2,1,0:T(8,128)(2,1)S(1)}, u32[]{:S(2)}, u32[]{:S(2)}) async-start(bf16[4,256,128]{2,1,0:T(8,128)(2,1)} %broadcast_in_dim.8), calls=%async_computation.2 | async-start | bytes 524288 | tf_op jit(solution)/shard_map/all_to_all | solution.py:46
  119.6 30.4 %all-to-all-start.3 = ((bf16[8,192,256]{2,1,0:T(8,128)(2,1)}), bf16[8,192,256]{2,1,0:T(8,128)(2,1)S(1)}, u32[]{:S(2)}, u32[]{:S(2)}) async-start(bf16[8,192,256]{2,1,0:T(8,128)(2,1)} %shard_map.144.refs_0_), calls=%async_computation.3 | async-start | bytes 1572864 | tf_op jit(solution)/shard_map/all_to_all | solution.py:457
  129.9 8.4 %collective-permute-start.10 = (bf16[256,128]{1,0:T(8,128)(2,1)S(1)}, bf16[256,128]{1,0:T(8,128)(2,1)S(1)}, u32[]{:S(2)}, u32[]{:S(2)}) collective-permute-start(bf16[256,128]{1,0:T(8,128)(2,1)S(1)} %get-tuple-element.13), channel_id=1, source_target_pairs={{0,32},{16,48},{32,0},{48,16},{64,96},{80,112},{96,64},{112,80},{1... | collective-permute-start | bytes 196616 | tf_op jit(solution)/shard_map/ppermute | solution.py:469
  132.4 6.0 %collective-permute-start.11 = (bf16[256,128]{1,0:T(8,128)(2,1)S(1)}, bf16[256,128]{1,0:T(8,128)(2,1)S(1)}, u32[]{:S(2)}, u32[]{:S(2)}) collective-permute-start(bf16[256,128]{1,0:T(8,128)(2,1)S(1)} %get-tuple-element.14), channel_id=1, source_target_pairs={{0,48},{16,0},{32,16},{48,32},{64,112},{80,64},{96,80},{112,96},{1... | collective-permute-start | bytes 196616 | tf_op jit(solution)/shard_map/ppermute | solution.py:469
  136.4 6.5 %collective-permute-start.9 = (bf16[256,128]{1,0:T(8,128)(2,1)S(1)}, bf16[256,128]{1,0:T(8,128)(2,1)S(1)}, u32[]{:S(2)}, u32[]{:S(2)}) collective-permute-start(bf16[256,128]{1,0:T(8,128)(2,1)S(1)} %get-tuple-element.12), channel_id=1, source_target_pairs={{0,16},{16,32},{32,48},{48,0},{64,80},{80,96},{96,112},{112,64},{1... | collective-permute-start | bytes 196616 | tf_op jit(solution)/shard_map/ppermute | solution.py:469
  151.2 7.5 %copy-start.7 = (f32[256,2]{0,1:T(2,128)S(1)}, f32[256,2]{0,1:T(2,128)}, u32[]{:S(2)}) copy-start(f32[256,2]{0,1:T(2,128)} %param.22) | copy-start | bytes 6148
  151.2 24.4 %all-to-all-start.4 = ((bf16[32,24,128]{2,1,0:T(8,128)(2,1)}), bf16[32,24,128]{2,1,0:T(8,128)(2,1)S(1)}, u32[]{:S(2)}, u32[]{:S(2)}) async-start(bf16[32,24,128]{2,1,0:T(8,128)(2,1)} %shard_map.147.refs_0_), calls=%async_computation.4 | async-start | bytes 393216 | tf_op jit(solution)/shard_map/all_to_all | solution.py:487
  176.8 3.2 %collective-permute-start.12 = (f32[256,128]{1,0:T(8,128)S(1)}, f32[256,128]{1,0:T(8,128)S(1)}, u32[]{:S(2)}, u32[]{:S(2)}) collective-permute-start(f32[256,128]{1,0:T(8,128)S(1)} %get-tuple-element.17), channel_id=1, source_target_pairs={{0,1},{1,0},{2,3},{3,2},{4,5},{5,4},{6,7},{7,6},{8,9},{9,8},{10,11... | collective-permute-start | bytes 393224 | tf_op jit(solution)/shard_map/ppermute | solution.py:491
  (6 other events, 4.7 us)

commit v6 on v5

--- a/solution.py
+++ b/solution.py
@@ -133,22 +133,15 @@
                 total = piece if total is None else total + piece
             out_ref[:, b] = total.reshape(expert_total, capacity, LANES).astype(jnp.bfloat16)
 
-        low_slot, low_valid = within(index_ref[1])
-        high_slot, high_valid = within(index_ref[1] + 2)
-        value = jnp.where(low_valid, low_slot, high_slot + 2.0 * share) + first_row
+        anywhere = earlier >= 0.0
         for k in range(top):
-            start = pick(k, value, low_valid | high_valid)
-            for side in range(2):
-                column = side * top + k
-                place_ref[:, column : column + 1] = jnp.where(
-                    start < 0, -1, start + side * SHARE
-                )
+            place_ref[:, k : k + 1] = pick(k, earlier + first_row, anywhere)
 
     return kernel_call(
         body,
         (
             jax.ShapeDtypeStruct((expert_total, width // wide, capacity, LANES), jnp.bfloat16),
-            jax.ShapeDtypeStruct((rows, 2 * top), jnp.int32),
+            jax.ShapeDtypeStruct((rows, top), jnp.int32),
         ),
         [SMEM, VMEM, VMEM, VMEM],
         (VMEM, VMEM),
@@ -165,20 +158,15 @@
         targets = message_rows((blocks * capacity, rows), 1)
         lines = lax.broadcasted_iota(jnp.int32, (blocks * capacity, rows), 0)
         total = None
-        for parity in range(2):
-            added = in_ref[parity].astype(jnp.float32)
-            for i in range(parity + 2, count, 2):
+        for part in range(PARTS):
+            added = in_ref[part].astype(jnp.float32)
+            for i in range(part + PARTS, count, PARTS):
                 added += in_ref[i].astype(jnp.float32)
-            added = added.astype(jnp.bfloat16)
-            for side in range(2):
-                offset = (2 * parity + side) * SHARE
-                select = jnp.where(lines == targets + offset, 1.0, 0.0).astype(jnp.bfloat16)
-                part = jnp.dot(
-                    select,
-                    added[:, side * LANES : (side + 1) * LANES],
-                    preferred_element_type=jnp.float32,
-                )
-                total = part if total is None else total + part
+            select = jnp.where(lines == targets + part * SHARE, 1.0, 0.0).astype(jnp.bfloat16)
+            piece = jnp.dot(
+                select, added.astype(jnp.bfloat16), preferred_element_type=jnp.float32
+            )
+            total = piece if total is None else total + piece
         out_ref[...] = total.reshape(blocks, capacity, LANES).astype(jnp.bfloat16)
 
     return kernel_call(
@@ -190,15 +178,16 @@
     )(parts, *earlier)
 
 
-def attend(index, query, key_value, score_scale, *earlier):
-    blocks, rows, _ = query.shape
+def attend(queries, key_value, score_scale, *earlier):
+    blocks = len(queries)
+    rows = queries[0].shape[0]
     pieces, _, length = key_value.shape
     factor = score_scale * math.log2(math.e)
     first_value = PLAIN_HEAD_DIM + ROPE
 
-    def body(index_ref, query_ref, key_ref, *refs):
-        for i, out_ref in enumerate(refs[-blocks:]):
-            q = query_ref[(index_ref[0] + i) % blocks]
+    def body(key_ref, *refs):
+        for query_ref, out_ref in zip(refs[:blocks], refs[-blocks:]):
+            q = query_ref[...]
             scores = [
                 jnp.dot(q, key_ref[j, :LANES, :], preferred_element_type=jnp.float32)
                 for j in range(pieces)
@@ -233,10 +222,10 @@
     return kernel_call(
         body,
         tuple(jax.ShapeDtypeStruct((rows, LANES), jnp.bfloat16) for _ in range(blocks)),
-        [SMEM, VMEM, VMEM] + [ANY] * len(earlier),
+        [VMEM] * (1 + blocks) + [ANY] * len(earlier),
         (VMEM,) * blocks,
         4 * blocks * rows * pieces * length * 2 * LANES,
-    )(index, query, key_value, *earlier)
+    )(key_value, *queries, *earlier)
 
 
 def merge(partials):
@@ -314,9 +303,10 @@
     )(messages, *gates, *ups)
 
 
-def project_down(hidden, downs, blocks, *earlier):
+def project_down(hidden, downs, *earlier):
     count, rows, units = hidden.shape
-    wide = downs[0].shape[1] // blocks
+    wide = 2 * LANES
+    blocks = downs[0].shape[1] // wide
 
     def body(hidden_ref, *refs):
         out_ref = refs[-1]
@@ -328,56 +318,54 @@
                     hidden_ref[g], refs[g][:, span], preferred_element_type=jnp.float32
                 )
                 total = part if total is None else total + part
-            out_ref[b] = total.astype(jnp.bfloat16)
-
-    return kernel_call(
-        body,
-        jax.ShapeDtypeStruct((blocks, rows, wide), jnp.bfloat16),
+            total = total.astype(jnp.bfloat16)
+            for side in range(2):
+                out_ref[2 * b + side] = total[:, side * LANES : (side + 1) * LANES]
+
+    return kernel_call(
+        body,
+        jax.ShapeDtypeStruct((2 * blocks, rows, LANES), jnp.bfloat16),
         [VMEM] * (1 + count) + [ANY] * len(earlier),
         VMEM,
         2 * rows * units * count * wide * blocks,
     )(hidden, *downs, *earlier)
 
 
-def combine(index, returned, places, route_weight):
+def combine(returned, places, route_weight):
     total, width = returned.shape
     rows, top = route_weight.shape
 
-    def body(index_ref, rows_ref, place_ref, weight_ref, own_ref, other_ref):
+    def body(rows_ref, place_ref, weight_ref, out_ref):
         slots = lax.broadcasted_iota(jnp.int32, (rows, total), 1)
-        sides = []
-        for side in range(2):
-            result = None
-            for k in range(top):
-                column = side * top + k
-                select = jnp.where(slots == place_ref[:, column : column + 1], 1.0, 0.0)
-                picked = jnp.dot(
-                    select.astype(jnp.bfloat16), rows_ref[...], preferred_element_type=jnp.float32
-                )
-                part = picked * weight_ref[:, k : k + 1]
-                result = part if result is None else result + part
-            sides.append(result)
-        first = index_ref[1] == 0
-        own_ref[...] = jnp.where(first, sides[0], sides[1])
-        other_ref[...] = jnp.where(first, sides[1], sides[0])
-
-    shape = jax.ShapeDtypeStruct((rows, width), jnp.float32)
-    return kernel_call(
-        body,
-        (shape, shape),
-        [SMEM, VMEM, VMEM, VMEM],
-        (VMEM, VMEM),
-        4 * rows * total * width * top,
-    )(index, returned, places, route_weight)
+        result = None
+        for k in range(top):
+            select = jnp.where(slots == place_ref[:, k : k + 1], 1.0, 0.0).astype(jnp.bfloat16)
+            picked = jnp.dot(select, rows_ref[...], preferred_element_type=jnp.float32)
+            part = picked * weight_ref[:, k : k + 1]
+            result = part if result is None else result + part
+        out_ref[...] = result.astype(jnp.bfloat16)
+
+    return kernel_call(
+        body,
+        jax.ShapeDtypeStruct((rows, width), jnp.bfloat16),
+        [VMEM, VMEM, VMEM],
+        VMEM,
+        2 * rows * total * width * top,
+    )(returned, places, route_weight)
 
 
 def make_local(z_count, x_count, tp_count):
     cores = 2
-    y_count = tp_count // cores
     ep_count = z_count * x_count
-    x_groups = [[x_count * z + x for x in range(x_count)] for z in range(z_count)]
     z_groups = [[x_count * z + x for z in range(z_count)] for x in range(x_count)]
-    y_groups = [[cores * y + c for y in range(y_count)] for c in range(cores)]
+    x_shifts = [
+        [
+            (x_count * z + x, x_count * z + (x + i) % x_count)
+            for z in range(z_count)
+            for x in range(x_count)
+        ]
+        for i in range(x_count)
+    ]
     partner = [(i, i ^ 1) for i in range(tp_count)]
     neighbour = [(i, i ^ cores) for i in range(tp_count)]
 
@@ -400,7 +388,7 @@
         capacity = 3 * row_count // ep_count
         tp_index = lax.axis_index("tp").astype(jnp.int32)
         ep_index = lax.axis_index("ep").astype(jnp.int32)
-        place_index = jnp.stack([tp_index % PARTS, tp_index % cores])
+        place_index = (tp_index % PARTS).reshape(1)
 
         groups_of = [[gate_weight[0]], [up_weight[0]], [down_weight[0]]]
         for group in groups_of:
@@ -449,33 +437,20 @@
         own_pack = jnp.concatenate(
             [own_keys[:PLAIN_HEAD_DIM], own_rope, own_keys[PLAIN_HEAD_DIM:]], axis=0
         )
-        key_value = to_everyone(sequenced(own_pack, arrived), "ep", z_groups, z_count)
+        query_all = [query]
+        for i in range(1, x_count):
+            query_all.append(lax.ppermute(query, "ep", x_shifts[x_count - i]))
+        key_value = to_everyone(sequenced(own_pack, arrived, *query_all), "ep", z_groups, z_count)
         hidden = hidden_units(arrived, gates, ups)
-        query_all = to_everyone(sequenced(query, key_value, hidden), "ep", x_groups, x_count)
-
-        partial_out = project_down(hidden, downs, y_count, query_all)
-        groups = lax.all_to_all(
-            partial_out, "tp", 0, 0, tiled=True, axis_index_groups=y_groups
-        )
+
+        partial_out = project_down(hidden, downs, key_value)
+        groups = lax.all_to_all(partial_out, "tp", 0, 0, tiled=True)
 
         partial_all = attend(
-            (ep_index % x_count).reshape(1),
-            query_all,
-            key_value,
-            (PLAIN_HEAD_DIM + ROPE) ** (-0.5),
-            partial_out,
+            query_all, key_value, (PLAIN_HEAD_DIM + ROPE) ** (-0.5), partial_out
         )
         partials = [partial_all[0]] + [
-            lax.ppermute(
-                partial_all[i],
-                "ep",
-                [
-                    (x_count * z + x, x_count * z + (x + i) % x_count)
-                    for z in range(z_count)
-                    for x in range(x_count)
-                ],
-            )
-            for i in range(1, x_count)
+            lax.ppermute(partial_all[i], "ep", x_shifts[i]) for i in range(1, x_count)
         ]
         attended = merge(partials)
         summed = add_up(groups, ep_count, attended)
@@ -485,10 +460,9 @@
         ).astype(jnp.bfloat16)
 
         returned = lax.all_to_all(summed, "ep", 0, 0, tiled=True)
-        own, other = combine(
-            place_index, returned.reshape(ep_count * capacity, LANES), places, route_weight
-        )
-        expert_out = (own + lax.ppermute(other, "tp", partner)).astype(jnp.bfloat16)
+        expert_out = combine(
+            returned.reshape(ep_count * capacity, LANES), places, route_weight
+        )
         return (attention_out, expert_out)
 
     return local

time: 182 us -> 154 us (0.85)
  waiting for transfers between devices: 51.7 us -> 26.9 us
  starting transfers between devices: 79.3 us -> 76 us
  local copies, waits for them, and re-layouts: 7.46 us -> 10.3 us
    ppermute x3, waiting for transfers between devices: 34.3 us -> 3.18 us  [local(): group.append(lax.ppermute(group[0], 'tp', neighbour))]
    ppermute x4 -> x6, waiting for transfers between devices: 4.76 us -> 12.4 us  [the longest x3 9.4 us: local(): query_all.append(lax.ppermute(query, 'ep', x_shifts[x_count - i]))]
    ppermute x4 -> x6, starting transfers between devices: 10.5 us -> 17.2 us  [the longest x3 8.74 us: local(): query_all.append(lax.ppermute(query, 'ep', x_shifts[x_count - i]))]
    all_to_all x1, starting transfers between devices: 13.8 us -> 9.1 us  [local(): arrived = lax.all_to_all(outgoing, 'ep', 0, 0, tiled=True)]
    all_to_all x2 -> x1, starting transfers between devices: 10.7 us -> 5.98 us  [to_everyone(): lax.all_to_all(jnp.broadcast_to(array[None], (count, *array.shape)), axis...]
    unnamed x25 -> x33, local copies, waits for them, and re-layouts: 4.15 us -> 8.26 us
    all_to_all x2 -> x1, waiting for transfers between devices: 6.18 us -> 4.1 us  [to_everyone(): lax.all_to_all(jnp.broadcast_to(array[None], (count, *array.shape)), axis...]
  transfers between devices with their start and end apart: 18 -> 19, of which waited for: 7 -> 7; matrix products, arithmetic and copies ran while one was open for 3% -> 3% of each run, Pallas kernels for 6% -> 9%
where the time goes in v6:
time: 154 us; the launch traced here: 152 us
  starting transfers between devices  76 us (49%)
  waiting for transfers between devices  26.9 us (17%)
  Pallas kernels  19.5 us (13%)
  blocking collectives  15.9 us (10%)
  local copies, waits for them, and re-layouts  10.3 us (7%)
    ppermute x6, starting transfers between devices, local(): group.append(lax.ppermute(weight, 'tp', partner))  21 us
    all_gather x1, blocking collectives, local(): lax.all_gather(sequenced(attended, summed), 'tp', axis=0, tiled=True)  15.9 us
    ppermute x3, starting transfers between devices, local(): group.append(lax.ppermute(group[0], 'tp', neighbour))  9.45 us
    ppermute x3, waiting for transfers between devices, local(): query_all.append(lax.ppermute(query, 'ep', x_shifts[x_count - i]))  9.4 us
    all_to_all x1, starting transfers between devices, local(): arrived = lax.all_to_all(outgoing, 'ep', 0, 0, tiled=True)  9.1 us
    ppermute x3, starting transfers between devices, local(): query_all.append(lax.ppermute(query, 'ep', x_shifts[x_count - i]))  8.74 us
    ppermute x3, starting transfers between devices, local(): lax.ppermute(partial_all[i], 'ep', x_shifts[i])  8.41 us
    unnamed x33, local copies, waits for them, and re-layouts  8.26 us
  transfers between devices with their start and end apart: 19, of which 7 were waited for; matrix products, arithmetic and copies ran while one was open for 3% of the time, Pallas kernels for 9%

profile of v6, /device:TPU:1, one launch (start us, length us, event | category | flops | bytes accessed | tf_op | source)
XLA Modules:
  0.0 152.5 jit_solution(11471818079247256576)
XLA Ops:
  0.6 4.2 %collective-permute-start.3 = (bf16[2048,256]{1,0:T(8,128)(2,1)}, bf16[2048,256]{1,0:T(8,128)(2,1)}, u32[]{:S(2)}, u32[]{:S(2)}) collective-permute-start(bf16[2048,256]{1,0:T(8,128)(2,1)} %bitcast.13), channel_id=1, source_target_pairs={{0,2},{1,3},{2,0},{3,1},{4,6},{5,7},{6,4},{7,5},{8,10},{9,11},{10,... | collective-permute-start | bytes 3145736 | tf_op jit(solution)/shard_map/ppermute | solution.py:395
  4.8 6.6 %collective-permute-start.4 = (bf16[2048,256]{1,0:T(8,128)(2,1)}, bf16[2048,256]{1,0:T(8,128)(2,1)}, u32[]{:S(2)}, u32[]{:S(2)}) collective-permute-start(bf16[2048,256]{1,0:T(8,128)(2,1)} %bitcast.14), channel_id=1, source_target_pairs={{0,1},{1,0},{2,3},{3,2},{4,5},{5,4},{6,7},{7,6},{8,9},{9,8},{10,11... | collective-permute-start | bytes 3145736 | tf_op jit(solution)/shard_map/ppermute | solution.py:404
  14.1 3.6 %shard_map.140 = (bf16[32,4,24,128]{3,2,1,0:T(8,128)(2,1)}, s32[256,2]{1,0:T(8,128)S(1)}) custom-call(s32[1]{0:T(128)} %bitcast.2.index_ref, bf16[256,2048]{1,0:T(8,128)(2,1)S(1)} %copy-done.6, f32[1,2048]{1,0:T(1,128)S(1)} %bitcast.17, s32[256,2]{1,0:T(8,128)S(1)} %copy.32.routes_ref), custom_call_target="tpu_custom_call" | custom-call | flops 805306368 | tf_op jit(solution)/shard_map/pallas_call | solution.py:140
  17.7 9.1 %all-to-all-start = ((bf16[32,4,24,128]{3,2,1,0:T(8,128)(2,1)}), bf16[32,4,24,128]{3,2,1,0:T(8,128)(2,1)S(1)}, u32[]{:S(2)}, u32[]{:S(2)}) async-start(bf16[32,4,24,128]{3,2,1,0:T(8,128)(2,1)} %get-tuple-element.8), calls=%async_computation | async-start | bytes 1572864 | tf_op jit(solution)/shard_map/all_to_all | solution.py:400
  30.8 4.3 %collective-permute-start = (bf16[256,128]{1,0:T(8,128)(2,1)S(1)}, bf16[256,128]{1,0:T(8,128)(2,1)S(1)}, u32[]{:S(2)}, u32[]{:S(2)}) collective-permute-start(bf16[256,128]{1,0:T(8,128)(2,1)S(1)} %maximum_maximum_fusion.refs_1_.refs_0_), channel_id=1, source_target_pairs={{0,48},{16,0},{32,16},{48,32},{64,112},{80,64},{96,80},{112,96},{1... | collective-permute-start | bytes 196616 | tf_op jit(solution)/shard_map/ppermute | solution.py:442
  35.2 3.2 %collective-permute-start.9 = (bf16[256,2048]{1,0:T(8,128)(2,1)}, bf16[256,2048]{1,0:T(8,128)(2,1)}, u32[]{:S(2)}, u32[]{:S(2)}) collective-permute-start(bf16[256,2048]{1,0:T(8,128)(2,1)} %bitcast.6.refs_0_), channel_id=1, source_target_pairs={{0,2},{1,3},{2,0},{3,1},{4,6},{5,7},{6,4},{7,5},{8,10},{9,11},{10,... | collective-permute-start | bytes 3145736 | tf_op jit(solution)/shard_map/ppermute | solution.py:395
  40.4 2.5 %collective-permute-start.1 = (bf16[256,128]{1,0:T(8,128)(2,1)S(1)}, bf16[256,128]{1,0:T(8,128)(2,1)S(1)}, u32[]{:S(2)}, u32[]{:S(2)}) collective-permute-start(bf16[256,128]{1,0:T(8,128)(2,1)S(1)} %maximum_maximum_fusion.refs_1_.refs_0_), channel_id=1, source_target_pairs={{0,32},{16,48},{32,0},{48,16},{64,96},{80,112},{96,64},{112,80},{1... | collective-permute-start | bytes 196616 | tf_op jit(solution)/shard_map/ppermute | solution.py:442
  43.0 5.1 %collective-permute-done.1.refs_3_.refs_2_ = bf16[256,128]{1,0:T(8,128)(2,1)S(1)} collective-permute-done((bf16[256,128]{1,0:T(8,128)(2,1)S(1)}, bf16[256,128]{1,0:T(8,128)(2,1)S(1)}, u32[]{:S(2)}, u32[]{:S(2)}) %collective-permute-start.1) | collective-permute-done | bytes 65568 | tf_op jit(solution)/shard_map/ppermute | solution.py:442
  50.1 4.3 %collective-permute-done.2.refs_4_.refs_3_ = bf16[256,128]{1,0:T(8,128)(2,1)S(1)} collective-permute-done((bf16[256,128]{1,0:T(8,128)(2,1)S(1)}, bf16[256,128]{1,0:T(8,128)(2,1)S(1)}, u32[]{:S(2)}, u32[]{:S(2)}) %collective-permute-start.2) | collective-permute-done | bytes 65568 | tf_op jit(solution)/shard_map/ppermute | solution.py:442
  54.4 4.8 %collective-permute-start.7 = (bf16[2048,256]{1,0:T(8,128)(2,1)}, bf16[2048,256]{1,0:T(8,128)(2,1)}, u32[]{:S(2)}, u32[]{:S(2)}) collective-permute-start(bf16[2048,256]{1,0:T(8,128)(2,1)} %bitcast.5.refs_4_), channel_id=1, source_target_pairs={{0,1},{1,0},{2,3},{3,2},{4,5},{5,4},{6,7},{7,6},{8,9},{9,8},{10,11... | collective-permute-start | bytes 3145736 | tf_op jit(solution)/shard_map/ppermute | solution.py:404
  61.1 2.4 %collective-permute-start.8 = (bf16[2048,256]{1,0:T(8,128)(2,1)}, bf16[2048,256]{1,0:T(8,128)(2,1)}, u32[]{:S(2)}, u32[]{:S(2)}) collective-permute-start(bf16[2048,256]{1,0:T(8,128)(2,1)} %collective-permute-done.6.refs_5_), channel_id=1, source_target_pairs={{0,1},{1,0},{2,3},{3,2},{4,5},{5,4},{6,7},{7,6},{8,9},{9,8},{10,11... | collective-permute-start | bytes 3145736 | tf_op jit(solution)/shard_map/ppermute | solution.py:404
  64.5 6.0 %all-to-all-start.1 = ((bf16[8,160,256]{2,1,0:T(8,128)(2,1)}), bf16[8,160,256]{2,1,0:T(8,128)(2,1)S(1)}, u32[]{:S(2)}, u32[]{:S(2)}) async-start(bf16[8,160,256]{2,1,0:T(8,128)(2,1)} %broadcast_in_dim.5), calls=%async_computation.1 | async-start | bytes 1310720 | tf_op jit(solution)/shard_map/all_to_all | solution.py:46
  72.7 3.2 %collective-permute-done.9.refs_1_ = bf16[256,2048]{1,0:T(8,128)(2,1)} collective-permute-done((bf16[256,2048]{1,0:T(8,128)(2,1)}, bf16[256,2048]{1,0:T(8,128)(2,1)}, u32[]{:S(2)}, u32[]{:S(2)}) %collective-permute-start.9) | collective-permute-done | bytes 1048608 | tf_op jit(solution)/shard_map/ppermute | solution.py:395
  75.9 3.1 %collective-permute-start.11 = (bf16[256,2048]{1,0:T(8,128)(2,1)}, bf16[256,2048]{1,0:T(8,128)(2,1)S(1)}, u32[]{:S(2)}, u32[]{:S(2)}) collective-permute-start(bf16[256,2048]{1,0:T(8,128)(2,1)} %collective-permute-done.9.refs_1_), channel_id=1, source_target_pairs={{0,1},{1,0},{2,3},{3,2},{4,5},{5,4},{6,7},{7,6},{8,9},{9,8},{10,11... | collective-permute-start | bytes 3145736 | tf_op jit(solution)/shard_map/ppermute | solution.py:404
  79.0 6.2 %shard_map.142.hidden_ref = bf16[4,192,256]{2,1,0:T(8,128)(2,1)S(1)} custom-call(bf16[32,4,24,128]{3,2,1,0:T(8,128)(2,1)S(1)} %all-to-all-done.refs_0_.rows_ref, bf16[2048,256]{1,0:T(8,128)(2,1)S(1)} %bitcast.15, bf16[2048,256]{1,0:T(8,128)(2,1)} %collective-permute-done.3.refs_1_, bf16[2048,256]{1,0:T(8,128)(2,1)} %collective-permute-done.4.refs_2_, ...), custom_call_target="tpu_custom_call" | custom-call | flops 1610612736 | tf_op jit(solution)/shard_map/pallas_call | solution.py:297
  87.2 4.1 %all-to-all-done.1.refs_4_.key_ref = bf16[8,160,256]{2,1,0:T(8,128)(2,1)S(1)} async-done(((bf16[8,160,256]{2,1,0:T(8,128)(2,1)}), bf16[8,160,256]{2,1,0:T(8,128)(2,1)S(1)}, u32[]{:S(2)}, u32[]{:S(2)}) %all-to-all-start.1) | async-done | bytes 655392 | tf_op jit(solution)/shard_map/all_to_all | solution.py:46
  93.7 3.4 %shard_map.143.refs_4_ = bf16[16,192,128]{2,1,0:T(8,128)(2,1)} custom-call(bf16[4,192,256]{2,1,0:T(8,128)(2,1)S(1)} %shard_map.142.hidden_ref, bf16[256,2048]{1,0:T(8,128)(2,1)} %bitcast.6.refs_0_, bf16[256,2048]{1,0:T(8,128)(2,1)} %collective-permute-done.9.refs_1_, bf16[256,2048]{1,0:T(8,128)(2,1)S(1)} %copy-done.3, bf16[256,2048]{1,0:T(8,128)(2,1)S(1)} %copy-done.5, ...), custom_call_target="tpu_custom_call" | custom-call | flops 805306368 | tf_op jit(solution)/shard_map/pallas_call | solution.py:325
  97.1 6.7 %all-to-all-start.2 = ((bf16[16,192,128]{2,1,0:T(8,128)(2,1)}), bf16[16,192,128]{2,1,0:T(8,128)(2,1)S(1)}, u32[]{:S(2)}, u32[]{:S(2)}) async-start(bf16[16,192,128]{2,1,0:T(8,128)(2,1)} %shard_map.143.refs_4_), calls=%async_computation.2 | async-start | bytes 1572864 | tf_op jit(solution)/shard_map/all_to_all | solution.py:447
  103.8 3.4 %shard_map.144 = (bf16[256,128]{1,0:T(8,128)(2,1)S(1)}, bf16[256,128]{1,0:T(8,128)(2,1)S(1)}, bf16[256,128]{1,0:T(8,128)(2,1)S(1)}, bf16[256,128]{1,0:T(8,128)(2,1)S(1)}) custom-call(bf16[8,160,256]{2,1,0:T(8,128)(2,1)S(1)} %all-to-all-done.1.refs_4_.key_ref, bf16[256,128]{1,0:T(8,128)(2,1)S(1)} %maximum_maximum_fusion.refs_1_.refs_0_, ...), custom_call_target="tpu_custom_call" | custom-call | flops 2147483648 | tf_op jit(solution)/shard_map/pallas_call | solution.py:222
  109.2 4.4 %collective-permute-start.13 = (bf16[256,128]{1,0:T(8,128)(2,1)S(1)}, bf16[256,128]{1,0:T(8,128)(2,1)S(1)}, u32[]{:S(2)}, u32[]{:S(2)}) collective-permute-start(bf16[256,128]{1,0:T(8,128)(2,1)S(1)} %get-tuple-element.11), channel_id=1, source_target_pairs={{0,32},{16,48},{32,0},{48,16},{64,96},{80,112},{96,64},{112,80},{1... | collective-permute-start | bytes 196616 | tf_op jit(solution)/shard_map/ppermute | solution.py:453
  116.1 2.8 %collective-permute-done.14.refs_3_ = bf16[256,128]{1,0:T(8,128)(2,1)S(1)} collective-permute-done((bf16[256,128]{1,0:T(8,128)(2,1)S(1)}, bf16[256,128]{1,0:T(8,128)(2,1)S(1)}, u32[]{:S(2)}, u32[]{:S(2)}) %collective-permute-start.14) | collective-permute-done | bytes 65568 | tf_op jit(solution)/shard_map/ppermute | solution.py:453
  119.4 7.1 %all-to-all-done.2.in_ref = bf16[16,192,128]{2,1,0:T(8,128)(2,1)S(1)} async-done(((bf16[16,192,128]{2,1,0:T(8,128)(2,1)}), bf16[16,192,128]{2,1,0:T(8,128)(2,1)S(1)}, u32[]{:S(2)}, u32[]{:S(2)}) %all-to-all-start.2) | async-done | bytes 786464 | tf_op jit(solution)/shard_map/all_to_all | solution.py:447
  127.8 6.6 %all-to-all-start.3 = ((bf16[32,24,128]{2,1,0:T(8,128)(2,1)}), bf16[32,24,128]{2,1,0:T(8,128)(2,1)S(1)}, u32[]{:S(2)}, u32[]{:S(2)}) async-start(bf16[32,24,128]{2,1,0:T(8,128)(2,1)} %shard_map.146.refs_0_), calls=%async_computation.3 | async-start | bytes 393216 | tf_op jit(solution)/shard_map/all_to_all | solution.py:462
  134.5 15.9 %all_gather.3 = bf16[1024,256]{1,0:T(8,128)(2,1)S(1)} all-gather(bf16[64,256]{1,0:T(8,128)(2,1)S(1)} %shard_map.147), channel_id=1, replica_groups=mesh['ep'=32,'tp'=16] {'tp'}, dimensions={0}, use_global_device_ids=true | all-gather | bytes 557056 | tf_op jit(solution)/shard_map/all_gather | solution.py:457
  (80 shorter events, 28.4 us)
Async XLA Ops:
  0.6 149.8 %copy-start = (bf16[1024,128]{1,0:T(8,128)(2,1)S(1)}, bf16[1024,128]{1,0:T(8,128)(2,1)}, u32[]{:S(2)}) copy-start(bf16[1024,128]{1,0:T(8,128)(2,1)} %param.18) | copy-start | bytes 786436
  0.6 58.5 %collective-permute-start.3 = (bf16[2048,256]{1,0:T(8,128)(2,1)}, bf16[2048,256]{1,0:T(8,128)(2,1)}, u32[]{:S(2)}, u32[]{:S(2)}) collective-permute-start(bf16[2048,256]{1,0:T(8,128)(2,1)} %bitcast.13), channel_id=1, source_target_pairs={{0,2},{1,3},{2,0},{3,1},{4,6},{5,7},{6,4},{7,5},{8,10},{9,11},{10,... | collective-permute-start | bytes 3145736 | tf_op jit(solution)/shard_map/ppermute | solution.py:395
  4.8 65.7 %collective-permute-start.4 = (bf16[2048,256]{1,0:T(8,128)(2,1)}, bf16[2048,256]{1,0:T(8,128)(2,1)}, u32[]{:S(2)}, u32[]{:S(2)}) collective-permute-start(bf16[2048,256]{1,0:T(8,128)(2,1)} %bitcast.14), channel_id=1, source_target_pairs={{0,1},{1,0},{2,3},{3,2},{4,5},{5,4},{6,7},{7,6},{8,9},{9,8},{10,11... | collective-permute-start | bytes 3145736 | tf_op jit(solution)/shard_map/ppermute | solution.py:404
  17.7 45.9 %all-to-all-start = ((bf16[32,4,24,128]{3,2,1,0:T(8,128)(2,1)}), bf16[32,4,24,128]{3,2,1,0:T(8,128)(2,1)S(1)}, u32[]{:S(2)}, u32[]{:S(2)}) async-start(bf16[32,4,24,128]{3,2,1,0:T(8,128)(2,1)} %get-tuple-element.8), calls=%async_computation | async-start | bytes 1572864 | tf_op jit(solution)/shard_map/all_to_all | solution.py:400
  26.8 34.3 %collective-permute-start.6 = (bf16[2048,256]{1,0:T(8,128)(2,1)}, bf16[2048,256]{1,0:T(8,128)(2,1)}, u32[]{:S(2)}, u32[]{:S(2)}) collective-permute-start(bf16[2048,256]{1,0:T(8,128)(2,1)} %bitcast.5.refs_4_), channel_id=1, source_target_pairs={{0,2},{1,3},{2,0},{3,1},{4,6},{5,7},{6,4},{7,5},{8,10},{9,11},{10,... | collective-permute-start | bytes 3145736 | tf_op jit(solution)/shard_map/ppermute | solution.py:395
  30.3 8.1 %copy-start.8 = (bf16[256,512]{1,0:T(8,128)(2,1)S(1)}, bf16[256,512]{1,0:T(8,128)(2,1)}, u32[]{:S(2)}) copy-start(bf16[256,512]{1,0:T(8,128)(2,1)} %param.14) | copy-start | bytes 786436
  30.8 9.5 %collective-permute-start = (bf16[256,128]{1,0:T(8,128)(2,1)S(1)}, bf16[256,128]{1,0:T(8,128)(2,1)S(1)}, u32[]{:S(2)}, u32[]{:S(2)}) collective-permute-start(bf16[256,128]{1,0:T(8,128)(2,1)S(1)} %maximum_maximum_fusion.refs_1_.refs_0_), channel_id=1, source_target_pairs={{0,48},{16,0},{32,16},{48,32},{64,112},{80,64},{96,80},{112,96},{1... | collective-permute-start | bytes 196616 | tf_op jit(solution)/shard_map/ppermute | solution.py:442
  35.2 3.4 %copy-start.9 = (bf16[256,32]{0,1:T(8,128)(2,1)S(1)}, bf16[256,32]{0,1:T(8,128)(2,1)}, u32[]{:S(2)}) copy-start(bf16[256,32]{0,1:T(8,128)(2,1)} %param.15) | copy-start | bytes 49156
  35.2 40.7 %collective-permute-start.9 = (bf16[256,2048]{1,0:T(8,128)(2,1)}, bf16[256,2048]{1,0:T(8,128)(2,1)}, u32[]{:S(2)}, u32[]{:S(2)}) collective-permute-start(bf16[256,2048]{1,0:T(8,128)(2,1)} %bitcast.6.refs_0_), channel_id=1, source_target_pairs={{0,2},{1,3},{2,0},{3,1},{4,6},{5,7},{6,4},{7,5},{8,10},{9,11},{10,... | collective-permute-start | bytes 3145736 | tf_op jit(solution)/shard_map/ppermute | solution.py:395
  40.4 7.8 %collective-permute-start.1 = (bf16[256,128]{1,0:T(8,128)(2,1)S(1)}, bf16[256,128]{1,0:T(8,128)(2,1)S(1)}, u32[]{:S(2)}, u32[]{:S(2)}) collective-permute-start(bf16[256,128]{1,0:T(8,128)(2,1)S(1)} %maximum_maximum_fusion.refs_1_.refs_0_), channel_id=1, source_target_pairs={{0,32},{16,48},{32,0},{48,16},{64,96},{80,112},{96,64},{112,80},{1... | collective-permute-start | bytes 196616 | tf_op jit(solution)/shard_map/ppermute | solution.py:442
  48.1 6.2 %collective-permute-start.2 = (bf16[256,128]{1,0:T(8,128)(2,1)S(1)}, bf16[256,128]{1,0:T(8,128)(2,1)S(1)}, u32[]{:S(2)}, u32[]{:S(2)}) collective-permute-start(bf16[256,128]{1,0:T(8,128)(2,1)S(1)} %maximum_maximum_fusion.refs_1_.refs_0_), channel_id=1, source_target_pairs={{0,16},{16,32},{32,48},{48,0},{64,80},{80,96},{96,112},{112,64},{1... | collective-permute-start | bytes 196616 | tf_op jit(solution)/shard_map/ppermute | solution.py:442
  54.4 24.6 %collective-permute-start.7 = (bf16[2048,256]{1,0:T(8,128)(2,1)}, bf16[2048,256]{1,0:T(8,128)(2,1)}, u32[]{:S(2)}, u32[]{:S(2)}) collective-permute-start(bf16[2048,256]{1,0:T(8,128)(2,1)} %bitcast.5.refs_4_), channel_id=1, source_target_pairs={{0,1},{1,0},{2,3},{3,2},{4,5},{5,4},{6,7},{7,6},{8,9},{9,8},{10,11... | collective-permute-start | bytes 3145736 | tf_op jit(solution)/shard_map/ppermute | solution.py:404
  59.1 19.8 %collective-permute-start.5 = (bf16[2048,256]{1,0:T(8,128)(2,1)}, bf16[2048,256]{1,0:T(8,128)(2,1)}, u32[]{:S(2)}, u32[]{:S(2)}) collective-permute-start(bf16[2048,256]{1,0:T(8,128)(2,1)} %collective-permute-done.3.refs_1_), channel_id=1, source_target_pairs={{0,1},{1,0},{2,3},{3,2},{4,5},{5,4},{6,7},{7,6},{8,9},{9,8},{10,11... | collective-permute-start | bytes 3145736 | tf_op jit(solution)/shard_map/ppermute | solution.py:404
  61.1 17.9 %collective-permute-start.8 = (bf16[2048,256]{1,0:T(8,128)(2,1)}, bf16[2048,256]{1,0:T(8,128)(2,1)}, u32[]{:S(2)}, u32[]{:S(2)}) collective-permute-start(bf16[2048,256]{1,0:T(8,128)(2,1)} %collective-permute-done.6.refs_5_), channel_id=1, source_target_pairs={{0,1},{1,0},{2,3},{3,2},{4,5},{5,4},{6,7},{7,6},{8,9},{9,8},{10,11... | collective-permute-start | bytes 3145736 | tf_op jit(solution)/shard_map/ppermute | solution.py:404
  63.5 15.4 %copy-start.1 = (bf16[1,2048,256]{2,1,0:T(8,128)(2,1)S(1)}, bf16[1,2048,256]{2,1,0:T(8,128)(2,1)}, u32[]{:S(2)}) copy-start(bf16[1,2048,256]{2,1,0:T(8,128)(2,1)} %param.23) | copy-start | bytes 3145732
  64.5 26.8 %all-to-all-start.1 = ((bf16[8,160,256]{2,1,0:T(8,128)(2,1)}), bf16[8,160,256]{2,1,0:T(8,128)(2,1)S(1)}, u32[]{:S(2)}, u32[]{:S(2)}) async-start(bf16[8,160,256]{2,1,0:T(8,128)(2,1)} %broadcast_in_dim.5), calls=%async_computation.1 | async-start | bytes 1310720 | tf_op jit(solution)/shard_map/all_to_all | solution.py:46
  70.5 14.7 %collective-permute-start.10 = (bf16[256,2048]{1,0:T(8,128)(2,1)}, bf16[256,2048]{1,0:T(8,128)(2,1)S(1)}, u32[]{:S(2)}, u32[]{:S(2)}) collective-permute-start(bf16[256,2048]{1,0:T(8,128)(2,1)} %bitcast.6.refs_0_), channel_id=1, source_target_pairs={{0,1},{1,0},{2,3},{3,2},{4,5},{5,4},{6,7},{7,6},{8,9},{9,8},{10,11... | collective-permute-start | bytes 3145736 | tf_op jit(solution)/shard_map/ppermute | solution.py:404
  75.9 10.3 %collective-permute-start.11 = (bf16[256,2048]{1,0:T(8,128)(2,1)}, bf16[256,2048]{1,0:T(8,128)(2,1)S(1)}, u32[]{:S(2)}, u32[]{:S(2)}) collective-permute-start(bf16[256,2048]{1,0:T(8,128)(2,1)} %collective-permute-done.9.refs_1_), channel_id=1, source_target_pairs={{0,1},{1,0},{2,3},{3,2},{4,5},{5,4},{6,7},{7,6},{8,9},{9,8},{10,11... | collective-permute-start | bytes 3145736 | tf_op jit(solution)/shard_map/ppermute | solution.py:404
  97.1 29.4 %all-to-all-start.2 = ((bf16[16,192,128]{2,1,0:T(8,128)(2,1)}), bf16[16,192,128]{2,1,0:T(8,128)(2,1)S(1)}, u32[]{:S(2)}, u32[]{:S(2)}) async-start(bf16[16,192,128]{2,1,0:T(8,128)(2,1)} %shard_map.143.refs_4_), calls=%async_computation.2 | async-start | bytes 1572864 | tf_op jit(solution)/shard_map/all_to_all | solution.py:447
  107.2 8.5 %copy-start.11 = (f32[256,2]{0,1:T(2,128)S(1)}, f32[256,2]{0,1:T(2,128)}, u32[]{:S(2)}) copy-start(f32[256,2]{0,1:T(2,128)} %param.22) | copy-start | bytes 6148
  107.2 8.6 %collective-permute-start.12 = (bf16[256,128]{1,0:T(8,128)(2,1)S(1)}, bf16[256,128]{1,0:T(8,128)(2,1)S(1)}, u32[]{:S(2)}, u32[]{:S(2)}) collective-permute-start(bf16[256,128]{1,0:T(8,128)(2,1)S(1)} %get-tuple-element.10), channel_id=1, source_target_pairs={{0,16},{16,32},{32,48},{48,0},{64,80},{80,96},{96,112},{112,64},{1... | collective-permute-start | bytes 196616 | tf_op jit(solution)/shard_map/ppermute | solution.py:453
  109.2 6.9 %collective-permute-start.13 = (bf16[256,128]{1,0:T(8,128)(2,1)S(1)}, bf16[256,128]{1,0:T(8,128)(2,1)S(1)}, u32[]{:S(2)}, u32[]{:S(2)}) collective-permute-start(bf16[256,128]{1,0:T(8,128)(2,1)S(1)} %get-tuple-element.11), channel_id=1, source_target_pairs={{0,32},{16,48},{32,0},{48,16},{64,96},{80,112},{96,64},{112,80},{1... | collective-permute-start | bytes 196616 | tf_op jit(solution)/shard_map/ppermute | solution.py:453
  113.5 5.3 %collective-permute-start.14 = (bf16[256,128]{1,0:T(8,128)(2,1)S(1)}, bf16[256,128]{1,0:T(8,128)(2,1)S(1)}, u32[]{:S(2)}, u32[]{:S(2)}) collective-permute-start(bf16[256,128]{1,0:T(8,128)(2,1)S(1)} %get-tuple-element.12), channel_id=1, source_target_pairs={{0,48},{16,0},{32,16},{48,32},{64,112},{80,64},{96,80},{112,96},{1... | collective-permute-start | bytes 196616 | tf_op jit(solution)/shard_map/ppermute | solution.py:453
  127.8 23.6 %all-to-all-start.3 = ((bf16[32,24,128]{2,1,0:T(8,128)(2,1)}), bf16[32,24,128]{2,1,0:T(8,128)(2,1)S(1)}, u32[]{:S(2)}, u32[]{:S(2)}) async-start(bf16[32,24,128]{2,1,0:T(8,128)(2,1)} %shard_map.146.refs_0_), calls=%async_computation.3 | async-start | bytes 393216 | tf_op jit(solution)/shard_map/all_to_all | solution.py:462
  (11 other events, 10.2 us)

commit v7 on v6

--- a/solution.py
+++ b/solution.py
@@ -20,9 +20,10 @@
 VMEM = pl.BlockSpec(memory_space=pltpu.VMEM)
 SMEM = pl.BlockSpec(memory_space=pltpu.SMEM)
 ANY = pl.BlockSpec(memory_space=pl.ANY)
-
-
-def kernel_call(body, out_shape, in_specs, out_specs, flops, limit=48):
+HBM = pl.BlockSpec(memory_space=pltpu.HBM)
+
+
+def kernel_call(body, out_shape, in_specs, out_specs, flops, limit=16):
     return pl.pallas_call(
         body,
         out_shape=out_shape,
@@ -259,15 +260,26 @@
     )(*partials)
 
 
-def hidden_units(messages, gates, ups):
+def experts(messages, gate_ups, downs, *earlier):
     sources, blocks, capacity, _ = messages.shape
     rows = sources * SHARE
-    units = gates[0].shape[1]
-    count = len(gates)
+    _, width, units = gate_ups[0].shape
+    count = len(gate_ups)
     wide = 2 * LANES
 
     def body(rows_ref, *refs):
-        gate_refs, up_refs, out_ref = refs[:count], refs[count : 2 * count], refs[-1]
+        gate_up_in, down_in = refs[:count], refs[count : 2 * count]
+        out_ref, gate_up_ref, down_ref, sems = refs[-4:]
+        gate_up_copies = [
+            pltpu.make_async_copy(gate_up_in[g], gate_up_ref.at[g], sems.at[g])
+            for g in range(count)
+        ]
+        down_copies = [
+            pltpu.make_async_copy(down_in[g], down_ref.at[g], sems.at[count + g])
+            for g in range(count)
+        ]
+        for copy in gate_up_copies + down_copies:
+            copy.start()
         targets = message_rows((rows, sources * capacity), 0)
         lines = lax.broadcasted_iota(jnp.int32, (rows, sources * capacity), 1)
         selects = [
@@ -284,51 +296,50 @@
             ]
             for part in range(0, PARTS, 2):
                 parts.append(jnp.concatenate(columns[part : part + 2], axis=1))
-        for g, (gate_ref, up_ref) in enumerate(zip(gate_refs, up_refs)):
+        hidden = []
+        for g in range(count):
+            gate_up_copies[g].wait()
             gate_value = jnp.zeros((rows, units), jnp.float32)
             up_value = jnp.zeros((rows, units), jnp.float32)
             for b, part in enumerate(parts):
                 span = slice(b * wide, (b + 1) * wide)
-                gate_value += jnp.dot(part, gate_ref[span, :], preferred_element_type=jnp.float32)
-                up_value += jnp.dot(part, up_ref[span, :], preferred_element_type=jnp.float32)
+                gate_value += jnp.dot(
+                    part, gate_up_ref[g, 0, span, :], preferred_element_type=jnp.float32
+                )
+                up_value += jnp.dot(
+                    part, gate_up_ref[g, 1, span, :], preferred_element_type=jnp.float32
+                )
             silu = gate_value / (1.0 + jnp.exp(-gate_value))
-            out_ref[g] = (silu * up_value).astype(jnp.bfloat16)
-
-    return kernel_call(
-        body,
-        jax.ShapeDtypeStruct((count, rows, units), jnp.bfloat16),
-        [VMEM] * (1 + 2 * count),
-        VMEM,
-        4 * rows * gates[0].shape[0] * units * count,
-    )(messages, *gates, *ups)
-
-
-def project_down(hidden, downs, *earlier):
-    count, rows, units = hidden.shape
-    wide = 2 * LANES
-    blocks = downs[0].shape[1] // wide
-
-    def body(hidden_ref, *refs):
-        out_ref = refs[-1]
-        for b in range(blocks):
+            hidden.append((silu * up_value).astype(jnp.bfloat16))
+        for copy in down_copies:
+            copy.wait()
+        for b in range(width // wide):
             span = slice(b * wide, (b + 1) * wide)
             total = None
             for g in range(count):
                 part = jnp.dot(
-                    hidden_ref[g], refs[g][:, span], preferred_element_type=jnp.float32
+                    hidden[g], down_ref[g, :, span], preferred_element_type=jnp.float32
                 )
                 total = part if total is None else total + part
             total = total.astype(jnp.bfloat16)
             for side in range(2):
                 out_ref[2 * b + side] = total[:, side * LANES : (side + 1) * LANES]
 
-    return kernel_call(
-        body,
-        jax.ShapeDtypeStruct((2 * blocks, rows, LANES), jnp.bfloat16),
-        [VMEM] * (1 + count) + [ANY] * len(earlier),
-        VMEM,
-        2 * rows * units * count * wide * blocks,
-    )(hidden, *downs, *earlier)
+    return pl.pallas_call(
+        body,
+        out_shape=jax.ShapeDtypeStruct((width // LANES, rows, LANES), jnp.bfloat16),
+        in_specs=[VMEM] + [HBM] * (2 * count) + [ANY] * len(earlier),
+        out_specs=VMEM,
+        scratch_shapes=[
+            pltpu.VMEM((count, 2, width, units), jnp.bfloat16),
+            pltpu.VMEM((count, units, width), jnp.bfloat16),
+            pltpu.SemaphoreType.DMA((2 * count,)),
+        ],
+        compiler_params=pltpu.CompilerParams(vmem_limit_bytes=36 * 1024 * 1024),
+        cost_estimate=pl.CostEstimate(
+            flops=6 * rows * width * units * count, transcendentals=0, bytes_accessed=0
+        ),
+    )(messages, *gate_ups, *downs, *earlier)
 
 
 def combine(returned, places, route_weight):
@@ -367,7 +378,12 @@
         for i in range(x_count)
     ]
     partner = [(i, i ^ 1) for i in range(tp_count)]
-    neighbour = [(i, i ^ cores) for i in range(tp_count)]
+    y_count = tp_count // cores
+    neighbour = [
+        (cores * y + c, cores * ((y + (1 if (y + c) % 2 == 0 else -1)) % y_count) + c)
+        for y in range(y_count)
+        for c in range(cores)
+    ]
 
     def local(
         queries,
@@ -390,7 +406,7 @@
         ep_index = lax.axis_index("ep").astype(jnp.int32)
         place_index = (tp_index % PARTS).reshape(1)
 
-        groups_of = [[gate_weight[0]], [up_weight[0]], [down_weight[0]]]
+        groups_of = [[jnp.stack([gate_weight[0], up_weight[0]])], [down_weight[0]]]
         for group in groups_of:
             group.append(lax.ppermute(group[0], "tp", neighbour))
 
@@ -402,7 +418,7 @@
         for group in groups_of:
             for weight in group[:2]:
                 group.append(lax.ppermute(weight, "tp", partner))
-        gates, ups, downs = groups_of
+        gate_ups, downs = groups_of
 
         positions = (ep_index * row_count + jnp.arange(row_count, dtype=jnp.int32)).astype(
             jnp.float32
@@ -441,9 +457,8 @@
         for i in range(1, x_count):
             query_all.append(lax.ppermute(query, "ep", x_shifts[x_count - i]))
         key_value = to_everyone(sequenced(own_pack, arrived, *query_all), "ep", z_groups, z_count)
-        hidden = hidden_units(arrived, gates, ups)
-
-        partial_out = project_down(hidden, downs, key_value)
+
+        partial_out = experts(arrived, gate_ups, downs)
         groups = lax.all_to_all(partial_out, "tp", 0, 0, tiled=True)
 
         partial_all = attend(

time: 154 us -> 143 us (0.929)
  starting transfers between devices: 76 us -> 64.3 us
  Pallas kernels: 19.5 us -> 16.5 us
  other arithmetic: 1.46 us -> 3.18 us
    all_to_all x1, waiting for transfers between devices: 4.1 us -> 11.1 us  [to_everyone(): lax.all_to_all(jnp.broadcast_to(array[None], (count, *array.shape)), axis...]
    ppermute x6 -> x4, starting transfers between devices: 21 us -> 14.1 us  [local(): group.append(lax.ppermute(weight, 'tp', partner))]
    ppermute x3 -> x2, waiting for transfers between devices: 3.18 us -> 0.01 us  [local(): group.append(lax.ppermute(group[0], 'tp', neighbour))]
    pallas_call x2 -> x1, Pallas kernels: 9.6 us -> 6.45 us  [experts(): pl.pallas_call(body, out_shape=jax.ShapeDtypeStruct((width // LANES, rows...]
    all_to_all x1, starting transfers between devices: 6.65 us -> 3.86 us  [local(): returned = lax.all_to_all(summed, 'ep', 0, 0, tiled=True)]
    ppermute x3, waiting for transfers between devices: 9.4 us -> 7.2 us  [local(): query_all.append(lax.ppermute(query, 'ep', x_shifts[x_count - i]))]
    all_to_all x1, waiting for transfers between devices: 7.13 us -> 5.15 us  [local(): groups = lax.all_to_all(partial_out, 'tp', 0, 0, tiled=True)]
    ppermute x3 -> x2, starting transfers between devices: 9.45 us -> 7.84 us  [local(): group.append(lax.ppermute(group[0], 'tp', neighbour))]
  transfers between devices with their start and end apart: 19 -> 16, of which waited for: 7 -> 5; matrix products, arithmetic and copies ran while one was open for 3% -> 7% of each run, Pallas kernels for 9% -> 10%
where the time goes in v7:
time: 143 us; the launch traced here: 142 us
  starting transfers between devices  64.3 us (45%)
  waiting for transfers between devices  27.5 us (19%)
  Pallas kernels  16.5 us (12%)
  blocking collectives  15.9 us (11%)
  local copies, waits for them, and re-layouts  11.1 us (8%)
  other arithmetic  3.18 us (2%)
  matrix products  2.27 us (2%)
    all_gather x1, blocking collectives, local(): lax.all_gather(sequenced(attended, summed), 'tp', axis=0, tiled=True)  15.9 us
    ppermute x4, starting transfers between devices, local(): group.append(lax.ppermute(weight, 'tp', partner))  14.1 us
    all_to_all x1, waiting for transfers between devices, to_everyone(): lax.all_to_all(jnp.broadcast_to(array[None], (count, *array.shape)), axis...  11.1 us
    all_to_all x1, starting transfers between devices, local(): arrived = lax.all_to_all(outgoing, 'ep', 0, 0, tiled=True)  10 us
    ppermute x3, starting transfers between devices, local(): query_all.append(lax.ppermute(query, 'ep', x_shifts[x_count - i]))  8.76 us
    unnamed x30, local copies, waits for them, and re-layouts  8.54 us
    ppermute x2, starting transfers between devices, local(): group.append(lax.ppermute(group[0], 'tp', neighbour))  7.84 us
    all_to_all x1, starting transfers between devices, local(): groups = lax.all_to_all(partial_out, 'tp', 0, 0, tiled=True)  7.47 us
  transfers between devices with their start and end apart: 16, of which 5 were waited for; matrix products, arithmetic and copies ran while one was open for 7% of the time, Pallas kernels for 10%

profile of v7, /device:TPU:1, one launch (start us, length us, event | category | flops | bytes accessed | tf_op | source)
XLA Modules:
  0.0 141.8 jit_solution(13926527315979691080)
XLA Ops:
  2.3 5.9 %collective-permute-start.3 = (bf16[2,2048,256]{2,1,0:T(8,128)(2,1)S(1)}, bf16[2,2048,256]{2,1,0:T(8,128)(2,1)}, u32[]{:S(2)}, u32[]{:S(2)}) collective-permute-start(bf16[2,2048,256]{2,1,0:T(8,128)(2,1)S(1)} %constant_dynamic-update-slice_fusion.refs_0_), channel_id=1, source_target_pairs={{0,2},{1,15},{2,0},{3,5},{4,6},{5,3},{6,4},{7,9},{8,10},{9,7},{10,... | collective-permute-start | bytes 6291464 | tf_op jit(solution)/shard_map/ppermute | solution.py:411
  8.2 4.8 %collective-permute-start.4 = (bf16[2,2048,256]{2,1,0:T(8,128)(2,1)S(1)}, bf16[2,2048,256]{2,1,0:T(8,128)(2,1)}, u32[]{:S(2)}, u32[]{:S(2)}) collective-permute-start(bf16[2,2048,256]{2,1,0:T(8,128)(2,1)S(1)} %constant_dynamic-update-slice_fusion.refs_0_), channel_id=1, source_target_pairs={{0,1},{1,0},{2,3},{3,2},{4,5},{5,4},{6,7},{7,6},{8,9},{9,8},{10,11... | collective-permute-start | bytes 6291464 | tf_op jit(solution)/shard_map/ppermute | solution.py:420
  13.0 1.9 %collective-permute-start.6 = (bf16[256,2048]{1,0:T(8,128)(2,1)}, bf16[256,2048]{1,0:T(8,128)(2,1)}, u32[]{:S(2)}, u32[]{:S(2)}) collective-permute-start(bf16[256,2048]{1,0:T(8,128)(2,1)} %bitcast.4.refs_4_), channel_id=1, source_target_pairs={{0,2},{1,15},{2,0},{3,5},{4,6},{5,3},{6,4},{7,9},{8,10},{9,7},{10,... | collective-permute-start | bytes 3145736 | tf_op jit(solution)/shard_map/ppermute | solution.py:411
  14.9 3.9 %collective-permute-start.7 = (bf16[256,2048]{1,0:T(8,128)(2,1)}, bf16[256,2048]{1,0:T(8,128)(2,1)}, u32[]{:S(2)}, u32[]{:S(2)}) collective-permute-start(bf16[256,2048]{1,0:T(8,128)(2,1)} %bitcast.4.refs_4_), channel_id=1, source_target_pairs={{0,1},{1,0},{2,3},{3,2},{4,5},{5,4},{6,7},{7,6},{8,9},{9,8},{10,11... | collective-permute-start | bytes 3145736 | tf_op jit(solution)/shard_map/ppermute | solution.py:420
  20.3 2.6 %shard_map.140 = (bf16[32,4,24,128]{3,2,1,0:T(8,128)(2,1)S(1)}, s32[256,2]{1,0:T(8,128)S(1)}) custom-call(s32[1]{0:T(128)} %bitcast.2.index_ref, bf16[256,2048]{1,0:T(8,128)(2,1)S(1)} %copy-done.7, f32[1,2048]{1,0:T(1,128)S(1)} %bitcast.12, s32[256,2]{1,0:T(8,128)S(1)} %copy.32.routes_ref), custom_call_target="tpu_custom_call" | custom-call | flops 805306368 | tf_op jit(solution)/shard_map/pallas_call | solution.py:141
  23.8 10.0 %all-to-all-start = ((bf16[32,4,24,128]{3,2,1,0:T(8,128)(2,1)}), bf16[32,4,24,128]{3,2,1,0:T(8,128)(2,1)S(1)}, u32[]{:S(2)}, u32[]{:S(2)}) async-start(bf16[32,4,24,128]{3,2,1,0:T(8,128)(2,1)} %copy-done.3), calls=%async_computation | async-start | bytes 1572864 | tf_op jit(solution)/shard_map/all_to_all | solution.py:416
  35.7 4.3 %collective-permute-start = (bf16[256,128]{1,0:T(8,128)(2,1)S(1)}, bf16[256,128]{1,0:T(8,128)(2,1)S(1)}, u32[]{:S(2)}, u32[]{:S(2)}) collective-permute-start(bf16[256,128]{1,0:T(8,128)(2,1)S(1)} %maximum_maximum_fusion.refs_1_.refs_0_), channel_id=1, source_target_pairs={{0,48},{16,0},{32,16},{48,32},{64,112},{80,64},{96,80},{112,96},{1... | collective-permute-start | bytes 196616 | tf_op jit(solution)/shard_map/ppermute | solution.py:458
  40.0 3.2 %collective-permute-start.5 = (bf16[2,2048,256]{2,1,0:T(8,128)(2,1)}, bf16[2,2048,256]{2,1,0:T(8,128)(2,1)}, u32[]{:S(2)}, u32[]{:S(2)}) collective-permute-start(bf16[2,2048,256]{2,1,0:T(8,128)(2,1)} %collective-permute-done.3.refs_1_), channel_id=1, source_target_pairs={{0,1},{1,0},{2,3},{3,2},{4,5},{5,4},{6,7},{7,6},{8,9},{9,8},{10,11... | collective-permute-start | bytes 6291464 | tf_op jit(solution)/shard_map/ppermute | solution.py:420
  47.9 2.5 %collective-permute-start.1 = (bf16[256,128]{1,0:T(8,128)(2,1)S(1)}, bf16[256,128]{1,0:T(8,128)(2,1)S(1)}, u32[]{:S(2)}, u32[]{:S(2)}) collective-permute-start(bf16[256,128]{1,0:T(8,128)(2,1)S(1)} %maximum_maximum_fusion.refs_1_.refs_0_), channel_id=1, source_target_pairs={{0,32},{16,48},{32,0},{48,16},{64,96},{80,112},{96,64},{112,80},{1... | collective-permute-start | bytes 196616 | tf_op jit(solution)/shard_map/ppermute | solution.py:458
  50.4 2.2 %collective-permute-start.8 = (bf16[256,2048]{1,0:T(8,128)(2,1)}, bf16[256,2048]{1,0:T(8,128)(2,1)}, u32[]{:S(2)}, u32[]{:S(2)}) collective-permute-start(bf16[256,2048]{1,0:T(8,128)(2,1)} %collective-permute-done.6.refs_5_), channel_id=1, source_target_pairs={{0,1},{1,0},{2,3},{3,2},{4,5},{5,4},{6,7},{7,6},{8,9},{9,8},{10,11... | collective-permute-start | bytes 3145736 | tf_op jit(solution)/shard_map/ppermute | solution.py:420
  52.6 3.7 %collective-permute-done.1.refs_3_.refs_2_ = bf16[256,128]{1,0:T(8,128)(2,1)S(1)} collective-permute-done((bf16[256,128]{1,0:T(8,128)(2,1)S(1)}, bf16[256,128]{1,0:T(8,128)(2,1)S(1)}, u32[]{:S(2)}, u32[]{:S(2)}) %collective-permute-start.1) | collective-permute-done | bytes 65568 | tf_op jit(solution)/shard_map/ppermute | solution.py:458
  59.0 3.5 %collective-permute-done.2.refs_4_.refs_3_ = bf16[256,128]{1,0:T(8,128)(2,1)S(1)} collective-permute-done((bf16[256,128]{1,0:T(8,128)(2,1)S(1)}, bf16[256,128]{1,0:T(8,128)(2,1)S(1)}, u32[]{:S(2)}, u32[]{:S(2)}) %collective-permute-start.2) | collective-permute-done | bytes 65568 | tf_op jit(solution)/shard_map/ppermute | solution.py:458
  64.9 5.0 %all-to-all-start.1 = ((bf16[8,160,256]{2,1,0:T(8,128)(2,1)}), bf16[8,160,256]{2,1,0:T(8,128)(2,1)}, u32[]{:S(2)}, u32[]{:S(2)}) async-start(bf16[8,160,256]{2,1,0:T(8,128)(2,1)} %broadcast_in_dim.5), calls=%async_computation.1 | async-start | bytes 1310720 | tf_op jit(solution)/shard_map/all_to_all | solution.py:47
  69.9 6.5 %shard_map.142.refs_4_ = bf16[16,192,128]{2,1,0:T(8,128)(2,1)S(1)} custom-call(bf16[32,4,24,128]{3,2,1,0:T(8,128)(2,1)S(1)} %all-to-all-done.refs_0_.rows_ref, bf16[2,2048,256]{2,1,0:T(8,128)(2,1)S(1)} %constant_dynamic-update-slice_fusion.refs_0_, bf16[2,2048,256]{2,1,0:T(8,128)(2,1)} %collective-permute-done.3.refs_1_, ...), custom_call_target="tpu_custom_call" | custom-call | flops 2415919104 | tf_op jit(solution)/shard_map/pallas_call | solution.py:328
  77.3 11.1 %all-to-all-done.1.key_ref = bf16[8,160,256]{2,1,0:T(8,128)(2,1)} async-done(((bf16[8,160,256]{2,1,0:T(8,128)(2,1)}), bf16[8,160,256]{2,1,0:T(8,128)(2,1)}, u32[]{:S(2)}, u32[]{:S(2)}) %all-to-all-start.1) | async-done | bytes 655392 | tf_op jit(solution)/shard_map/all_to_all | solution.py:47
  88.4 7.5 %all-to-all-start.2 = ((bf16[16,192,128]{2,1,0:T(8,128)(2,1)}), bf16[16,192,128]{2,1,0:T(8,128)(2,1)S(1)}, u32[]{:S(2)}, u32[]{:S(2)}) async-start(bf16[16,192,128]{2,1,0:T(8,128)(2,1)} %copy-done.1), calls=%async_computation.2 | async-start | bytes 1572864 | tf_op jit(solution)/shard_map/all_to_all | solution.py:462
  97.1 4.5 %shard_map.143 = (bf16[256,128]{1,0:T(8,128)(2,1)S(1)}, bf16[256,128]{1,0:T(8,128)(2,1)S(1)}, bf16[256,128]{1,0:T(8,128)(2,1)S(1)}, bf16[256,128]{1,0:T(8,128)(2,1)S(1)}) custom-call(bf16[8,160,256]{2,1,0:T(8,128)(2,1)} %all-to-all-done.1.key_ref, bf16[256,128]{1,0:T(8,128)(2,1)S(1)} %maximum_maximum_fusion.refs_1_.refs_0_, ...), custom_call_target="tpu_custom_call" | custom-call | flops 2147483648 | tf_op jit(solution)/shard_map/pallas_call | solution.py:223
  101.6 1.9 %collective-permute-start.10 = (bf16[256,128]{1,0:T(8,128)(2,1)S(1)}, bf16[256,128]{1,0:T(8,128)(2,1)S(1)}, u32[]{:S(2)}, u32[]{:S(2)}) collective-permute-start(bf16[256,128]{1,0:T(8,128)(2,1)S(1)} %get-tuple-element.11), channel_id=1, source_target_pairs={{0,32},{16,48},{32,0},{48,16},{64,96},{80,112},{96,64},{112,80},{1... | collective-permute-start | bytes 196616 | tf_op jit(solution)/shard_map/ppermute | solution.py:468
  103.5 3.0 %collective-permute-start.11 = (bf16[256,128]{1,0:T(8,128)(2,1)S(1)}, bf16[256,128]{1,0:T(8,128)(2,1)S(1)}, u32[]{:S(2)}, u32[]{:S(2)}) collective-permute-start(bf16[256,128]{1,0:T(8,128)(2,1)S(1)} %get-tuple-element.12), channel_id=1, source_target_pairs={{0,48},{16,0},{32,16},{48,32},{64,112},{80,64},{96,80},{112,96},{1... | collective-permute-start | bytes 196616 | tf_op jit(solution)/shard_map/ppermute | solution.py:468
  106.6 2.2 %collective-permute-start.9 = (bf16[256,128]{1,0:T(8,128)(2,1)S(1)}, bf16[256,128]{1,0:T(8,128)(2,1)S(1)}, u32[]{:S(2)}, u32[]{:S(2)}) collective-permute-start(bf16[256,128]{1,0:T(8,128)(2,1)S(1)} %get-tuple-element.10), channel_id=1, source_target_pairs={{0,16},{16,32},{32,48},{48,0},{64,80},{80,96},{96,112},{112,64},{1... | collective-permute-start | bytes 196616 | tf_op jit(solution)/shard_map/ppermute | solution.py:468
  109.0 3.9 %collective-permute-done.9.refs_1_ = bf16[256,128]{1,0:T(8,128)(2,1)S(1)} collective-permute-done((bf16[256,128]{1,0:T(8,128)(2,1)S(1)}, bf16[256,128]{1,0:T(8,128)(2,1)S(1)}, u32[]{:S(2)}, u32[]{:S(2)}) %collective-permute-start.9) | collective-permute-done | bytes 65568 | tf_op jit(solution)/shard_map/ppermute | solution.py:468
  113.5 5.2 %all-to-all-done.2.in_ref = bf16[16,192,128]{2,1,0:T(8,128)(2,1)S(1)} async-done(((bf16[16,192,128]{2,1,0:T(8,128)(2,1)}), bf16[16,192,128]{2,1,0:T(8,128)(2,1)S(1)}, u32[]{:S(2)}, u32[]{:S(2)}) %all-to-all-start.2) | async-done | bytes 786464 | tf_op jit(solution)/shard_map/all_to_all | solution.py:462
  119.9 3.9 %all-to-all-start.3 = ((bf16[32,24,128]{2,1,0:T(8,128)(2,1)}), bf16[32,24,128]{2,1,0:T(8,128)(2,1)S(1)}, u32[]{:S(2)}, u32[]{:S(2)}) async-start(bf16[32,24,128]{2,1,0:T(8,128)(2,1)} %shard_map.145.refs_0_), calls=%async_computation.3 | async-start | bytes 393216 | tf_op jit(solution)/shard_map/all_to_all | solution.py:477
  123.8 15.9 %all_gather.3 = bf16[1024,256]{1,0:T(8,128)(2,1)S(1)} all-gather(bf16[64,256]{1,0:T(8,128)(2,1)S(1)} %shard_map.146), channel_id=1, replica_groups=mesh['ep'=32,'tp'=16] {'tp'}, dimensions={0}, use_global_device_ids=true | all-gather | bytes 557056 | tf_op jit(solution)/shard_map/all_gather | solution.py:472
  (70 shorter events, 21.5 us)
Async XLA Ops:
  0.6 139.1 %copy-start = (bf16[1024,128]{1,0:T(8,128)(2,1)S(1)}, bf16[1024,128]{1,0:T(8,128)(2,1)}, u32[]{:S(2)}) copy-start(bf16[1024,128]{1,0:T(8,128)(2,1)} %param.18) | copy-start | bytes 786436
  0.6 1.6 %copy-start.9 = (bf16[1,2048,256]{2,1,0:T(8,128)(2,1)S(1)}, bf16[1,2048,256]{2,1,0:T(8,128)(2,1)}, u32[]{:S(2)}) copy-start(bf16[1,2048,256]{2,1,0:T(8,128)(2,1)} %param.24) | copy-start | bytes 3145732
  0.7 18.2 %copy-start.10 = (s32[256,2]{0,1:T(2,128)S(1)}, s32[256,2]{0,1:T(2,128)}, u32[]{:S(2)}) copy-start(s32[256,2]{0,1:T(2,128)} %param.21) | copy-start | bytes 6148
  0.7 18.4 %copy-start.8 = (f32[2048]{0:T(1024)S(1)}, f32[2048]{0:T(1024)}, u32[]{:S(2)}) copy-start(f32[2048]{0:T(1024)} %param.20) | copy-start | bytes 24580
  2.3 37.7 %collective-permute-start.3 = (bf16[2,2048,256]{2,1,0:T(8,128)(2,1)S(1)}, bf16[2,2048,256]{2,1,0:T(8,128)(2,1)}, u32[]{:S(2)}, u32[]{:S(2)}) collective-permute-start(bf16[2,2048,256]{2,1,0:T(8,128)(2,1)S(1)} %constant_dynamic-update-slice_fusion.refs_0_), channel_id=1, source_target_pairs={{0,2},{1,15},{2,0},{3,5},{4,6},{5,3},{6,4},{7,9},{8,10},{9,7},{10,... | collective-permute-start | bytes 6291464 | tf_op jit(solution)/shard_map/ppermute | solution.py:411
  8.2 61.7 %collective-permute-start.4 = (bf16[2,2048,256]{2,1,0:T(8,128)(2,1)S(1)}, bf16[2,2048,256]{2,1,0:T(8,128)(2,1)}, u32[]{:S(2)}, u32[]{:S(2)}) collective-permute-start(bf16[2,2048,256]{2,1,0:T(8,128)(2,1)S(1)} %constant_dynamic-update-slice_fusion.refs_0_), channel_id=1, source_target_pairs={{0,1},{1,0},{2,3},{3,2},{4,5},{5,4},{6,7},{7,6},{8,9},{9,8},{10,11... | collective-permute-start | bytes 6291464 | tf_op jit(solution)/shard_map/ppermute | solution.py:420
  13.0 37.4 %collective-permute-start.6 = (bf16[256,2048]{1,0:T(8,128)(2,1)}, bf16[256,2048]{1,0:T(8,128)(2,1)}, u32[]{:S(2)}, u32[]{:S(2)}) collective-permute-start(bf16[256,2048]{1,0:T(8,128)(2,1)} %bitcast.4.refs_4_), channel_id=1, source_target_pairs={{0,2},{1,15},{2,0},{3,5},{4,6},{5,3},{6,4},{7,9},{8,10},{9,7},{10,... | collective-permute-start | bytes 3145736 | tf_op jit(solution)/shard_map/ppermute | solution.py:411
  14.9 55.0 %collective-permute-start.7 = (bf16[256,2048]{1,0:T(8,128)(2,1)}, bf16[256,2048]{1,0:T(8,128)(2,1)}, u32[]{:S(2)}, u32[]{:S(2)}) collective-permute-start(bf16[256,2048]{1,0:T(8,128)(2,1)} %bitcast.4.refs_4_), channel_id=1, source_target_pairs={{0,1},{1,0},{2,3},{3,2},{4,5},{5,4},{6,7},{7,6},{8,9},{9,8},{10,11... | collective-permute-start | bytes 3145736 | tf_op jit(solution)/shard_map/ppermute | solution.py:420
  19.0 1.2 copy-start.7
  20.3 13.6 %slice-start = ((bf16[256,96]{0,1:T(8,128)(2,1)}), bf16[256,32]{0,1:T(8,128)(2,1)S(1)}, s32[]{:S(2)}) async-start(bf16[256,96]{0,1:T(8,128)(2,1)} %param.13), calls=%async_computation.4 | async-start | bytes 32768 | tf_op jit(solution)/shard_map/slice | solution.py:440
  23.8 39.4 %all-to-all-start = ((bf16[32,4,24,128]{3,2,1,0:T(8,128)(2,1)}), bf16[32,4,24,128]{3,2,1,0:T(8,128)(2,1)S(1)}, u32[]{:S(2)}, u32[]{:S(2)}) async-start(bf16[32,4,24,128]{3,2,1,0:T(8,128)(2,1)} %copy-done.3), calls=%async_computation | async-start | bytes 1572864 | tf_op jit(solution)/shard_map/all_to_all | solution.py:416
  35.7 12.2 %collective-permute-start = (bf16[256,128]{1,0:T(8,128)(2,1)S(1)}, bf16[256,128]{1,0:T(8,128)(2,1)S(1)}, u32[]{:S(2)}, u32[]{:S(2)}) collective-permute-start(bf16[256,128]{1,0:T(8,128)(2,1)S(1)} %maximum_maximum_fusion.refs_1_.refs_0_), channel_id=1, source_target_pairs={{0,48},{16,0},{32,16},{48,32},{64,112},{80,64},{96,80},{112,96},{1... | collective-permute-start | bytes 196616 | tf_op jit(solution)/shard_map/ppermute | solution.py:458
  40.0 29.9 %collective-permute-start.5 = (bf16[2,2048,256]{2,1,0:T(8,128)(2,1)}, bf16[2,2048,256]{2,1,0:T(8,128)(2,1)}, u32[]{:S(2)}, u32[]{:S(2)}) collective-permute-start(bf16[2,2048,256]{2,1,0:T(8,128)(2,1)} %collective-permute-done.3.refs_1_), channel_id=1, source_target_pairs={{0,1},{1,0},{2,3},{3,2},{4,5},{5,4},{6,7},{7,6},{8,9},{9,8},{10,11... | collective-permute-start | bytes 6291464 | tf_op jit(solution)/shard_map/ppermute | solution.py:420
  47.9 8.4 %collective-permute-start.1 = (bf16[256,128]{1,0:T(8,128)(2,1)S(1)}, bf16[256,128]{1,0:T(8,128)(2,1)S(1)}, u32[]{:S(2)}, u32[]{:S(2)}) collective-permute-start(bf16[256,128]{1,0:T(8,128)(2,1)S(1)} %maximum_maximum_fusion.refs_1_.refs_0_), channel_id=1, source_target_pairs={{0,32},{16,48},{32,0},{48,16},{64,96},{80,112},{96,64},{112,80},{1... | collective-permute-start | bytes 196616 | tf_op jit(solution)/shard_map/ppermute | solution.py:458
  50.4 19.5 %collective-permute-start.8 = (bf16[256,2048]{1,0:T(8,128)(2,1)}, bf16[256,2048]{1,0:T(8,128)(2,1)}, u32[]{:S(2)}, u32[]{:S(2)}) collective-permute-start(bf16[256,2048]{1,0:T(8,128)(2,1)} %collective-permute-done.6.refs_5_), channel_id=1, source_target_pairs={{0,1},{1,0},{2,3},{3,2},{4,5},{5,4},{6,7},{7,6},{8,9},{9,8},{10,11... | collective-permute-start | bytes 3145736 | tf_op jit(solution)/shard_map/ppermute | solution.py:420
  56.3 6.2 %collective-permute-start.2 = (bf16[256,128]{1,0:T(8,128)(2,1)S(1)}, bf16[256,128]{1,0:T(8,128)(2,1)S(1)}, u32[]{:S(2)}, u32[]{:S(2)}) collective-permute-start(bf16[256,128]{1,0:T(8,128)(2,1)S(1)} %maximum_maximum_fusion.refs_1_.refs_0_), channel_id=1, source_target_pairs={{0,16},{16,32},{32,48},{48,0},{64,80},{80,96},{96,112},{112,64},{1... | collective-permute-start | bytes 196616 | tf_op jit(solution)/shard_map/ppermute | solution.py:458
  64.9 23.5 %all-to-all-start.1 = ((bf16[8,160,256]{2,1,0:T(8,128)(2,1)}), bf16[8,160,256]{2,1,0:T(8,128)(2,1)}, u32[]{:S(2)}, u32[]{:S(2)}) async-start(bf16[8,160,256]{2,1,0:T(8,128)(2,1)} %broadcast_in_dim.5), calls=%async_computation.1 | async-start | bytes 1310720 | tf_op jit(solution)/shard_map/all_to_all | solution.py:47
  69.9 26.0 %copy-start.6 = (bf16[256,128]{1,0:T(8,128)(2,1)S(1)}, bf16[256,128]{1,0:T(8,128)(2,1)}, u32[]{:S(2)}) copy-start(bf16[256,128]{1,0:T(8,128)(2,1)} %copy-done.4) | copy-start | bytes 196612
  88.4 30.2 %all-to-all-start.2 = ((bf16[16,192,128]{2,1,0:T(8,128)(2,1)}), bf16[16,192,128]{2,1,0:T(8,128)(2,1)S(1)}, u32[]{:S(2)}, u32[]{:S(2)}) async-start(bf16[16,192,128]{2,1,0:T(8,128)(2,1)} %copy-done.1), calls=%async_computation.2 | async-start | bytes 1572864 | tf_op jit(solution)/shard_map/all_to_all | solution.py:462
  97.1 11.7 %copy-start.11 = (f32[256,2]{0,1:T(2,128)S(1)}, f32[256,2]{0,1:T(2,128)}, u32[]{:S(2)}) copy-start(f32[256,2]{0,1:T(2,128)} %param.22) | copy-start | bytes 6148
  101.6 7.4 %collective-permute-start.10 = (bf16[256,128]{1,0:T(8,128)(2,1)S(1)}, bf16[256,128]{1,0:T(8,128)(2,1)S(1)}, u32[]{:S(2)}, u32[]{:S(2)}) collective-permute-start(bf16[256,128]{1,0:T(8,128)(2,1)S(1)} %get-tuple-element.11), channel_id=1, source_target_pairs={{0,32},{16,48},{32,0},{48,16},{64,96},{80,112},{96,64},{112,80},{1... | collective-permute-start | bytes 196616 | tf_op jit(solution)/shard_map/ppermute | solution.py:468
  103.5 5.5 %collective-permute-start.11 = (bf16[256,128]{1,0:T(8,128)(2,1)S(1)}, bf16[256,128]{1,0:T(8,128)(2,1)S(1)}, u32[]{:S(2)}, u32[]{:S(2)}) collective-permute-start(bf16[256,128]{1,0:T(8,128)(2,1)S(1)} %get-tuple-element.12), channel_id=1, source_target_pairs={{0,48},{16,0},{32,16},{48,32},{64,112},{80,64},{96,80},{112,96},{1... | collective-permute-start | bytes 196616 | tf_op jit(solution)/shard_map/ppermute | solution.py:468
  106.6 6.4 %collective-permute-start.9 = (bf16[256,128]{1,0:T(8,128)(2,1)S(1)}, bf16[256,128]{1,0:T(8,128)(2,1)S(1)}, u32[]{:S(2)}, u32[]{:S(2)}) collective-permute-start(bf16[256,128]{1,0:T(8,128)(2,1)S(1)} %get-tuple-element.10), channel_id=1, source_target_pairs={{0,16},{16,32},{32,48},{48,0},{64,80},{80,96},{96,112},{112,64},{1... | collective-permute-start | bytes 196616 | tf_op jit(solution)/shard_map/ppermute | solution.py:468
  119.9 20.8 %all-to-all-start.3 = ((bf16[32,24,128]{2,1,0:T(8,128)(2,1)}), bf16[32,24,128]{2,1,0:T(8,128)(2,1)S(1)}, u32[]{:S(2)}, u32[]{:S(2)}) async-start(bf16[32,24,128]{2,1,0:T(8,128)(2,1)} %shard_map.145.refs_0_), calls=%async_computation.3 | async-start | bytes 393216 | tf_op jit(solution)/shard_map/all_to_all | solution.py:477
  (5 other events, 4.4 us)

commit v8 on v7

--- a/solution.py
+++ b/solution.py
@@ -2,6 +2,7 @@
 
 import jax
 import jax.numpy as jnp
+import numpy as np
 from jax import lax
 from jax.experimental import pallas as pl
 from jax.experimental.pallas import tpu as pltpu
@@ -34,24 +35,70 @@
     )
 
 
-def rms_scale(values, gain_vector):
-    floats = values.astype(jnp.float32)
-    return (
-        floats
-        * lax.rsqrt(jnp.mean(floats * floats, axis=-1, keepdims=True) + EPSILON)
-        * gain_vector
-    )
-
-
-def to_everyone(array, axis, groups, count):
-    return lax.all_to_all(
-        jnp.broadcast_to(array[None], (count, *array.shape)),
-        axis,
-        0,
-        0,
-        tiled=True,
-        axis_index_groups=groups,
-    )
+def angle_tables(blocks, rows):
+    half = ROPE // 2
+    frequency = ROPE_BASE_VALUE ** (-np.arange(half) * 2.0 / ROPE)
+    tables = []
+    for positions in (np.arange(blocks) * rows, np.arange(rows)):
+        angles = np.zeros((len(positions), LANES))
+        angles[:, PLAIN_HEAD_DIM : PLAIN_HEAD_DIM + ROPE] = np.tile(
+            positions[:, None] * frequency, (1, 2)
+        )
+        tables += [np.cos(angles).astype(np.float32), np.sin(angles).astype(np.float32)]
+    return tables
+
+
+def prepare(index, queries, latents, rope_key, gain, weight, tables, copies):
+    rows = queries.shape[0]
+    first, last = PLAIN_HEAD_DIM, PLAIN_HEAD_DIM + ROPE
+    half = ROPE // 2
+
+    def body(index_ref, query_ref, latent_ref, rope_ref, gain_ref, weight_ref, *refs):
+        block_cos, block_sin, place_cos, place_sin = refs[:4]
+        query_out, key_out, padded_ref = refs[4:]
+        base_cos = block_cos[pl.ds(index_ref[0], 1), :]
+        base_sin = block_sin[pl.ds(index_ref[0], 1), :]
+        cosine = base_cos * place_cos[...] - base_sin * place_sin[...]
+        sine = base_sin * place_cos[...] + base_cos * place_sin[...]
+        lane = lax.broadcasted_iota(jnp.int32, (rows, LANES), 1)
+        early = lane < first + half
+        sine = jnp.where(early, -sine, sine)
+
+        def rotated(values):
+            other = jnp.where(
+                early, pltpu.roll(values, LANES - half, 1), pltpu.roll(values, half, 1)
+            )
+            return values * cosine + other * sine
+
+        padded_ref[...] = jnp.zeros((rows, LANES), jnp.float32)
+        padded_ref[:, :last] = query_ref[...].astype(jnp.float32)
+        query_out[...] = rotated(padded_ref[...]).astype(jnp.bfloat16)
+        padded_ref[:, first:last] = rope_ref[...].astype(jnp.float32)
+        turned = rotated(padded_ref[...]).T[first:last].astype(jnp.bfloat16)
+        floats = latent_ref[...].astype(jnp.float32)
+        scale = lax.rsqrt(jnp.mean(floats * floats, axis=-1, keepdims=True) + EPSILON)
+        normed = (floats * scale * gain_ref[...]).astype(jnp.bfloat16)
+        expanded = jnp.dot(normed, weight_ref[...], preferred_element_type=jnp.float32).T
+        expanded = expanded.astype(jnp.bfloat16)
+        for i in range(copies):
+            key_out[i, :first, :] = expanded[:first]
+            key_out[i, first:last, :] = turned
+            key_out[i, last:, :] = expanded[first:]
+
+    return pl.pallas_call(
+        body,
+        out_shape=(
+            jax.ShapeDtypeStruct((rows, LANES), jnp.bfloat16),
+            jax.ShapeDtypeStruct((copies, LANES + ROPE, rows), jnp.bfloat16),
+        ),
+        in_specs=[SMEM] + [VMEM] * 9,
+        out_specs=(VMEM, VMEM),
+        scratch_shapes=[pltpu.VMEM((rows, LANES), jnp.float32)],
+        compiler_params=pltpu.CompilerParams(vmem_limit_bytes=16 * 1024 * 1024),
+        cost_estimate=pl.CostEstimate(
+            flops=2 * latents.size * weight.shape[1], transcendentals=0, bytes_accessed=0
+        ),
+    )(index, queries, latents, rope_key, gain, weight, *tables)
 
 
 def sequenced(array, *earlier):
@@ -420,50 +467,27 @@
                 group.append(lax.ppermute(weight, "tp", partner))
         gate_ups, downs = groups_of
 
-        positions = (ep_index * row_count + jnp.arange(row_count, dtype=jnp.int32)).astype(
-            jnp.float32
-        )
-        half = ROPE // 2
-        frequency = ROPE_BASE_VALUE ** (-jnp.arange(half, dtype=jnp.float32) * 2.0 / ROPE)
-        angles = positions[:, None] * frequency
-        cosine, sine = jnp.cos(angles), jnp.sin(angles)
-
-        def rotated(values):
-            first, second = values[:, :half], values[:, half:]
-            return jnp.concatenate(
-                [first * cosine - second * sine, second * cosine + first * sine], axis=1
-            ).astype(jnp.bfloat16)
-
-        query = jnp.concatenate(
-            [
-                queries[:, :PLAIN_HEAD_DIM],
-                rotated(queries[:, PLAIN_HEAD_DIM:].astype(jnp.float32)),
-                jnp.zeros((row_count, LANES - PLAIN_HEAD_DIM - ROPE), jnp.bfloat16),
-            ],
-            axis=1,
-        )
-        latent_normed = rms_scale(compressed_key_value, latent_norm_gain).astype(jnp.bfloat16)
-        own_keys = lax.dot_general(
+        query, own_keys = prepare(
+            ep_index.reshape(1),
+            queries,
+            compressed_key_value,
+            rope_key,
+            latent_norm_gain.reshape(1, -1),
             latent_to_key_value,
-            latent_normed,
-            (((0,), (1,)), ((), ())),
-            preferred_element_type=jnp.float32,
-        ).astype(jnp.bfloat16)
-        own_rope = rotated(rope_key.astype(jnp.float32)).T
-        own_pack = jnp.concatenate(
-            [own_keys[:PLAIN_HEAD_DIM], own_rope, own_keys[PLAIN_HEAD_DIM:]], axis=0
+            angle_tables(ep_count, row_count),
+            z_count,
         )
         query_all = [query]
         for i in range(1, x_count):
             query_all.append(lax.ppermute(query, "ep", x_shifts[x_count - i]))
-        key_value = to_everyone(sequenced(own_pack, arrived, *query_all), "ep", z_groups, z_count)
+        key_value = lax.all_to_all(
+            own_keys, "ep", 0, 0, tiled=True, axis_index_groups=z_groups
+        )
 
         partial_out = experts(arrived, gate_ups, downs)
         groups = lax.all_to_all(partial_out, "tp", 0, 0, tiled=True)
 
-        partial_all = attend(
-            query_all, key_value, (PLAIN_HEAD_DIM + ROPE) ** (-0.5), partial_out
-        )
+        partial_all = attend(query_all, key_value, (PLAIN_HEAD_DIM + ROPE) ** (-0.5))
         partials = [partial_all[0]] + [
             lax.ppermute(partial_all[i], "ep", x_shifts[i]) for i in range(1, x_count)
         ]

time: 143 us -> 151 us (1.056)
  starting transfers between devices: 64.3 us -> 74.1 us
  blocking collectives: 15.9 us -> 21.3 us
  waiting for transfers between devices: 27.5 us -> 23.5 us
  other arithmetic: 3.18 us -> 0 us
    all_gather x1, blocking collectives: 15.9 us -> 21.3 us  [local(): lax.all_gather(sequenced(attended, summed), 'tp', axis=0, tiled=True)]
    all_to_all x1, waiting for transfers between devices: 5.15 us -> 0.01 us  [local(): groups = lax.all_to_all(partial_out, 'tp', 0, 0, tiled=True)]
    ppermute x2, waiting for transfers between devices: 0.01 us -> 4.16 us  [local(): group.append(lax.ppermute(group[0], 'tp', neighbour))]
    unnamed x30 -> x47, local copies, waits for them, and re-layouts: 8.54 us -> 12.4 us
    ppermute x4, starting transfers between devices: 14.1 us -> 17.5 us  [local(): group.append(lax.ppermute(weight, 'tp', partner))]
    ppermute x3, waiting for transfers between devices: 7.2 us -> 3.98 us  [local(): query_all.append(lax.ppermute(query, 'ep', x_shifts[x_count - i]))]
    all_to_all x1, starting transfers between devices: 10 us -> 12.9 us  [local(): arrived = lax.all_to_all(outgoing, 'ep', 0, 0, tiled=True)]
    all_to_all x1, waiting for transfers between devices: 11.1 us -> 13.5 us  [local(): lax.all_to_all(own_keys, 'ep', 0, 0, tiled=True, axis_index_groups=z_groups)]
  transfers between devices with their start and end apart: 16 -> 16, of which waited for: 5 -> 6; matrix products, arithmetic and copies ran while one was open for 7% -> 1% of each run, Pallas kernels for 10% -> 9%
where the time goes in v8:
time: 151 us; the launch traced here: 150 us
  starting transfers between devices  74.1 us (49%)
  waiting for transfers between devices  23.5 us (16%)
  blocking collectives  21.3 us (14%)
  Pallas kernels  16.6 us (11%)
  local copies, waits for them, and re-layouts  12.4 us (8%)
    all_gather x1, blocking collectives, local(): lax.all_gather(sequenced(attended, summed), 'tp', axis=0, tiled=True)  21.3 us
    ppermute x4, starting transfers between devices, local(): group.append(lax.ppermute(weight, 'tp', partner))  17.5 us
    all_to_all x1, waiting for transfers between devices, local(): lax.all_to_all(own_keys, 'ep', 0, 0, tiled=True, axis_index_groups=z_groups)  13.5 us
    all_to_all x1, starting transfers between devices, local(): arrived = lax.all_to_all(outgoing, 'ep', 0, 0, tiled=True)  12.9 us
    unnamed x47, local copies, waits for them, and re-layouts  12.4 us
    ppermute x3, starting transfers between devices, local(): lax.ppermute(partial_all[i], 'ep', x_shifts[i])  9.35 us
    ppermute x3, starting transfers between devices, local(): query_all.append(lax.ppermute(query, 'ep', x_shifts[x_count - i]))  9.33 us
    ppermute x2, starting transfers between devices, local(): group.append(lax.ppermute(group[0], 'tp', neighbour))  7.85 us
  transfers between devices with their start and end apart: 16, of which 6 were waited for; matrix products, arithmetic and copies ran while one was open for 1% of the time, Pallas kernels for 9%

profile of v8, /device:TPU:1, one launch (start us, length us, event | category | flops | bytes accessed | tf_op | source)
XLA Modules:
  0.0 149.9 jit_solution(14462325684438922710)
XLA Ops:
  2.3 5.9 %collective-permute-start.6 = (bf16[2,2048,256]{2,1,0:T(8,128)(2,1)S(1)}, bf16[2,2048,256]{2,1,0:T(8,128)(2,1)}, u32[]{:S(2)}, u32[]{:S(2)}) collective-permute-start(bf16[2,2048,256]{2,1,0:T(8,128)(2,1)S(1)} %constant_dynamic-update-slice_fusion.refs_0_), channel_id=1, source_target_pairs={{0,2},{1,15},{2,0},{3,5},{4,6},{5,3},{6,4},{7,9},{8,10},{9,7},{10,... | collective-permute-start | bytes 6291464 | tf_op jit(solution)/shard_map/ppermute | solution.py:458
  9.6 2.6 %shard_map.179 = (bf16[32,4,24,128]{3,2,1,0:T(8,128)(2,1)S(1)}, s32[256,2]{1,0:T(8,128)S(1)}) custom-call(s32[1]{0:T(128)} %bitcast.2.index_ref, bf16[256,2048]{1,0:T(8,128)(2,1)S(1)} %copy-done.13, f32[1,2048]{1,0:T(1,128)S(1)} %bitcast.13, s32[256,2]{1,0:T(8,128)S(1)} %copy.21.routes_ref), custom_call_target="tpu_custom_call" | custom-call | flops 805306368 | tf_op jit(solution)/shard_map/pallas_call | solution.py:188
  13.8 12.9 %all-to-all-start.1 = ((bf16[32,4,24,128]{3,2,1,0:T(8,128)(2,1)}), bf16[32,4,24,128]{3,2,1,0:T(8,128)(2,1)S(1)}, u32[]{:S(2)}, u32[]{:S(2)}) async-start(bf16[32,4,24,128]{3,2,1,0:T(8,128)(2,1)} %copy-done.2), calls=%async_computation.1 | async-start | bytes 1572864 | tf_op jit(solution)/shard_map/all_to_all | solution.py:463
  26.7 1.9 %collective-permute-start.9 = (bf16[256,2048]{1,0:T(8,128)(2,1)}, bf16[256,2048]{1,0:T(8,128)(2,1)}, u32[]{:S(2)}, u32[]{:S(2)}) collective-permute-start(bf16[256,2048]{1,0:T(8,128)(2,1)} %bitcast.8), channel_id=1, source_target_pairs={{0,2},{1,15},{2,0},{3,5},{4,6},{5,3},{6,4},{7,9},{8,10},{9,7},{10,... | collective-permute-start | bytes 3145736 | tf_op jit(solution)/shard_map/ppermute | solution.py:458
  28.6 1.9 %collective-permute-start.7 = (bf16[2,2048,256]{2,1,0:T(8,128)(2,1)S(1)}, bf16[2,2048,256]{2,1,0:T(8,128)(2,1)}, u32[]{:S(2)}, u32[]{:S(2)}) collective-permute-start(bf16[2,2048,256]{2,1,0:T(8,128)(2,1)S(1)} %constant_dynamic-update-slice_fusion.refs_0_), channel_id=1, source_target_pairs={{0,1},{1,0},{2,3},{3,2},{4,5},{5,4},{6,7},{7,6},{8,9},{9,8},{10,11... | collective-permute-start | bytes 6291464 | tf_op jit(solution)/shard_map/ppermute | solution.py:467
  31.8 7.3 %collective-permute-start.8 = (bf16[2,2048,256]{2,1,0:T(8,128)(2,1)}, bf16[2,2048,256]{2,1,0:T(8,128)(2,1)}, u32[]{:S(2)}, u32[]{:S(2)}) collective-permute-start(bf16[2,2048,256]{2,1,0:T(8,128)(2,1)} %collective-permute-done.6.refs_1_), channel_id=1, source_target_pairs={{0,1},{1,0},{2,3},{3,2},{4,5},{5,4},{6,7},{7,6},{8,9},{9,8},{10,11... | collective-permute-start | bytes 6291464 | tf_op jit(solution)/shard_map/ppermute | solution.py:467
  39.1 1.9 %collective-permute-start.10 = (bf16[256,2048]{1,0:T(8,128)(2,1)}, bf16[256,2048]{1,0:T(8,128)(2,1)}, u32[]{:S(2)}, u32[]{:S(2)}) collective-permute-start(bf16[256,2048]{1,0:T(8,128)(2,1)} %bitcast.9), channel_id=1, source_target_pairs={{0,1},{1,0},{2,3},{3,2},{4,5},{5,4},{6,7},{7,6},{8,9},{9,8},{10,11... | collective-permute-start | bytes 3145736 | tf_op jit(solution)/shard_map/ppermute | solution.py:467
  41.0 2.9 %collective-permute-done.9.refs_5_ = bf16[256,2048]{1,0:T(8,128)(2,1)} collective-permute-done((bf16[256,2048]{1,0:T(8,128)(2,1)}, bf16[256,2048]{1,0:T(8,128)(2,1)}, u32[]{:S(2)}, u32[]{:S(2)}) %collective-permute-start.9) | collective-permute-done | bytes 1048608 | tf_op jit(solution)/shard_map/ppermute | solution.py:458
  43.9 6.4 %collective-permute-start.11 = (bf16[256,2048]{1,0:T(8,128)(2,1)}, bf16[256,2048]{1,0:T(8,128)(2,1)}, u32[]{:S(2)}, u32[]{:S(2)}) collective-permute-start(bf16[256,2048]{1,0:T(8,128)(2,1)} %collective-permute-done.9.refs_5_), channel_id=1, source_target_pairs={{0,1},{1,0},{2,3},{3,2},{4,5},{5,4},{6,7},{7,6},{8,9},{9,8},{10,11... | collective-permute-start | bytes 3145736 | tf_op jit(solution)/shard_map/ppermute | solution.py:467
  57.4 4.8 %all-to-all-start = ((bf16[8,160,256]{2,1,0:T(8,128)(2,1)}), bf16[8,160,256]{2,1,0:T(8,128)(2,1)}, u32[]{:S(2)}, u32[]{:S(2)}) async-start(bf16[8,160,256]{2,1,0:T(8,128)(2,1)} %copy-done.3), calls=%async_computation | async-start | bytes 1310720 | tf_op jit(solution)/shard_map/all_to_all | solution.py:483
  63.5 6.1 %shard_map.180 = bf16[16,192,128]{2,1,0:T(8,128)(2,1)} custom-call(bf16[32,4,24,128]{3,2,1,0:T(8,128)(2,1)S(1)} %all-to-all-done.1.rows_ref, bf16[2,2048,256]{2,1,0:T(8,128)(2,1)S(1)} %constant_dynamic-update-slice_fusion.refs_0_, bf16[2,2048,256]{2,1,0:T(8,128)(2,1)} %collective-permute-done.6.refs_1_, ...), custom_call_target="tpu_custom_call" | custom-call | flops 2415919104 | tf_op jit(solution)/shard_map/pallas_call | solution.py:375
  69.5 13.5 %all-to-all-done.key_ref = bf16[8,160,256]{2,1,0:T(8,128)(2,1)} async-done(((bf16[8,160,256]{2,1,0:T(8,128)(2,1)}), bf16[8,160,256]{2,1,0:T(8,128)(2,1)}, u32[]{:S(2)}, u32[]{:S(2)}) %all-to-all-start) | async-done | bytes 655392 | tf_op jit(solution)/shard_map/all_to_all | solution.py:483
  83.1 7.6 %all-to-all-start.2 = ((bf16[16,192,128]{2,1,0:T(8,128)(2,1)}), bf16[16,192,128]{2,1,0:T(8,128)(2,1)S(1)}, u32[]{:S(2)}, u32[]{:S(2)}) async-start(bf16[16,192,128]{2,1,0:T(8,128)(2,1)} %shard_map.180), calls=%async_computation.2 | async-start | bytes 1572864 | tf_op jit(solution)/shard_map/all_to_all | solution.py:488
  90.7 4.4 %collective-permute-start = (bf16[256,128]{1,0:T(8,128)(2,1)S(1)}, bf16[256,128]{1,0:T(8,128)(2,1)S(1)}, u32[]{:S(2)}, u32[]{:S(2)}) collective-permute-start(bf16[256,128]{1,0:T(8,128)(2,1)S(1)} %copy-done.15), channel_id=1, source_target_pairs={{0,48},{16,0},{32,16},{48,32},{64,112},{80,64},{96,80},{112,96},{1... | collective-permute-start | bytes 196616 | tf_op jit(solution)/shard_map/ppermute | solution.py:482
  95.1 2.4 %collective-permute-start.1 = (bf16[256,128]{1,0:T(8,128)(2,1)S(1)}, bf16[256,128]{1,0:T(8,128)(2,1)S(1)}, u32[]{:S(2)}, u32[]{:S(2)}) collective-permute-start(bf16[256,128]{1,0:T(8,128)(2,1)S(1)} %copy-done.15), channel_id=1, source_target_pairs={{0,32},{16,48},{32,0},{48,16},{64,96},{80,112},{96,64},{112,80},{1... | collective-permute-start | bytes 196616 | tf_op jit(solution)/shard_map/ppermute | solution.py:482
  97.5 2.5 %collective-permute-start.2 = (bf16[256,128]{1,0:T(8,128)(2,1)S(1)}, bf16[256,128]{1,0:T(8,128)(2,1)S(1)}, u32[]{:S(2)}, u32[]{:S(2)}) collective-permute-start(bf16[256,128]{1,0:T(8,128)(2,1)S(1)} %copy-done.15), channel_id=1, source_target_pairs={{0,16},{16,32},{32,48},{48,0},{64,80},{80,96},{96,112},{112,64},{1... | collective-permute-start | bytes 196616 | tf_op jit(solution)/shard_map/ppermute | solution.py:482
  100.1 1.8 %collective-permute-done.1.refs_2_ = bf16[256,128]{1,0:T(8,128)(2,1)S(1)} collective-permute-done((bf16[256,128]{1,0:T(8,128)(2,1)S(1)}, bf16[256,128]{1,0:T(8,128)(2,1)S(1)}, u32[]{:S(2)}, u32[]{:S(2)}) %collective-permute-start.1) | collective-permute-done | bytes 65568 | tf_op jit(solution)/shard_map/ppermute | solution.py:482
  101.9 2.1 %collective-permute-done.2.refs_3_ = bf16[256,128]{1,0:T(8,128)(2,1)S(1)} collective-permute-done((bf16[256,128]{1,0:T(8,128)(2,1)S(1)}, bf16[256,128]{1,0:T(8,128)(2,1)S(1)}, u32[]{:S(2)}, u32[]{:S(2)}) %collective-permute-start.2) | collective-permute-done | bytes 65568 | tf_op jit(solution)/shard_map/ppermute | solution.py:482
  104.1 4.5 %shard_map.177 = (bf16[256,128]{1,0:T(8,128)(2,1)S(1)}, bf16[256,128]{1,0:T(8,128)(2,1)S(1)}, bf16[256,128]{1,0:T(8,128)(2,1)S(1)}, bf16[256,128]{1,0:T(8,128)(2,1)S(1)}) custom-call(bf16[8,160,256]{2,1,0:T(8,128)(2,1)} %all-to-all-done.key_ref, bf16[256,128]{1,0:T(8,128)(2,1)S(1)} %copy-done.15, bf16[256,128]{1,0:T(8,128)(2,1)S(1)} %collective-permute-done.refs_1_, ...), custom_call_target="tpu_custom_call" | custom-call | flops 2147483648 | tf_op jit(solution)/shard_map/pallas_call | solution.py:270
  108.6 2.2 %collective-permute-start.3 = (bf16[256,128]{1,0:T(8,128)(2,1)S(1)}, bf16[256,128]{1,0:T(8,128)(2,1)S(1)}, u32[]{:S(2)}, u32[]{:S(2)}) collective-permute-start(bf16[256,128]{1,0:T(8,128)(2,1)S(1)} %get-tuple-element.13), channel_id=1, source_target_pairs={{0,16},{16,32},{32,48},{48,0},{64,80},{80,96},{96,112},{112,64},{1... | collective-permute-start | bytes 196616 | tf_op jit(solution)/shard_map/ppermute | solution.py:492
  110.8 3.1 %collective-permute-start.4 = (bf16[256,128]{1,0:T(8,128)(2,1)S(1)}, bf16[256,128]{1,0:T(8,128)(2,1)S(1)}, u32[]{:S(2)}, u32[]{:S(2)}) collective-permute-start(bf16[256,128]{1,0:T(8,128)(2,1)S(1)} %get-tuple-element.14), channel_id=1, source_target_pairs={{0,32},{16,48},{32,0},{48,16},{64,96},{80,112},{96,64},{112,80},{1... | collective-permute-start | bytes 196616 | tf_op jit(solution)/shard_map/ppermute | solution.py:492
  114.0 4.0 %collective-permute-start.5 = (bf16[256,128]{1,0:T(8,128)(2,1)S(1)}, bf16[256,128]{1,0:T(8,128)(2,1)S(1)}, u32[]{:S(2)}, u32[]{:S(2)}) collective-permute-start(bf16[256,128]{1,0:T(8,128)(2,1)S(1)} %get-tuple-element.15), channel_id=1, source_target_pairs={{0,48},{16,0},{32,16},{48,32},{64,112},{80,64},{96,80},{112,96},{1... | collective-permute-start | bytes 196616 | tf_op jit(solution)/shard_map/ppermute | solution.py:492
  121.7 4.7 %all-to-all-start.3 = ((bf16[32,24,128]{2,1,0:T(8,128)(2,1)}), bf16[32,24,128]{2,1,0:T(8,128)(2,1)S(1)}, u32[]{:S(2)}, u32[]{:S(2)}) async-start(bf16[32,24,128]{2,1,0:T(8,128)(2,1)} %shard_map.181.refs_0_), calls=%async_computation.3 | async-start | bytes 393216 | tf_op jit(solution)/shard_map/all_to_all | solution.py:501
  126.5 21.3 %all_gather.3 = bf16[1024,256]{1,0:T(8,128)(2,1)S(1)} all-gather(bf16[64,256]{1,0:T(8,128)(2,1)S(1)} %shard_map.182), channel_id=1, replica_groups=mesh['ep'=32,'tp'=16] {'tp'}, dimensions={0}, use_global_device_ids=true | all-gather | bytes 557056 | tf_op jit(solution)/shard_map/all_gather | solution.py:496
  (66 shorter events, 19.9 us)
Async XLA Ops:
  0.6 147.2 %copy-start = (bf16[1024,128]{1,0:T(8,128)(2,1)S(1)}, bf16[1024,128]{1,0:T(8,128)(2,1)}, u32[]{:S(2)}) copy-start(bf16[1024,128]{1,0:T(8,128)(2,1)} %param.22) | copy-start | bytes 786436
  0.7 7.7 %copy-start.16 = (f32[2048]{0:T(1024)S(1)}, f32[2048]{0:T(1024)}, u32[]{:S(2)}) copy-start(f32[2048]{0:T(1024)} %param.24) | copy-start | bytes 24580
  2.3 29.5 %collective-permute-start.6 = (bf16[2,2048,256]{2,1,0:T(8,128)(2,1)S(1)}, bf16[2,2048,256]{2,1,0:T(8,128)(2,1)}, u32[]{:S(2)}, u32[]{:S(2)}) collective-permute-start(bf16[2,2048,256]{2,1,0:T(8,128)(2,1)S(1)} %constant_dynamic-update-slice_fusion.refs_0_), channel_id=1, source_target_pairs={{0,2},{1,15},{2,0},{3,5},{4,6},{5,3},{6,4},{7,9},{8,10},{9,7},{10,... | collective-permute-start | bytes 6291464 | tf_op jit(solution)/shard_map/ppermute | solution.py:458
  9.6 40.7 %copy-start.18 = (bf16[256,96]{0,1:T(8,128)(2,1)S(1)}, bf16[256,96]{0,1:T(8,128)(2,1)}, u32[]{:S(2)}) copy-start(bf16[256,96]{0,1:T(8,128)(2,1)} %param.17) | copy-start | bytes 147460
  9.6 41.7 %copy-start.4 = (bf16[256,512]{1,0:T(8,128)(2,1)S(1)}, bf16[256,512]{1,0:T(8,128)(2,1)}, u32[]{:S(2)}) copy-start(bf16[256,512]{1,0:T(8,128)(2,1)} %latent_ref.1) | copy-start | bytes 786436
  9.6 41.7 %copy-start.10 = (f32[32,128]{1,0:T(8,128)S(1)}, f32[32,128]{1,0:T(8,128)}, u32[]{:S(2)}) copy-start(f32[32,128]{1,0:T(8,128)} %constant.30.clone.refs_0_) | copy-start | bytes 49156
  13.8 43.6 %all-to-all-start.1 = ((bf16[32,4,24,128]{3,2,1,0:T(8,128)(2,1)}), bf16[32,4,24,128]{3,2,1,0:T(8,128)(2,1)S(1)}, u32[]{:S(2)}, u32[]{:S(2)}) async-start(bf16[32,4,24,128]{3,2,1,0:T(8,128)(2,1)} %copy-done.2), calls=%async_computation.1 | async-start | bytes 1572864 | tf_op jit(solution)/shard_map/all_to_all | solution.py:463
  26.7 17.3 %collective-permute-start.9 = (bf16[256,2048]{1,0:T(8,128)(2,1)}, bf16[256,2048]{1,0:T(8,128)(2,1)}, u32[]{:S(2)}, u32[]{:S(2)}) collective-permute-start(bf16[256,2048]{1,0:T(8,128)(2,1)} %bitcast.8), channel_id=1, source_target_pairs={{0,2},{1,15},{2,0},{3,5},{4,6},{5,3},{6,4},{7,9},{8,10},{9,7},{10,... | collective-permute-start | bytes 3145736 | tf_op jit(solution)/shard_map/ppermute | solution.py:458
  28.6 33.6 %collective-permute-start.7 = (bf16[2,2048,256]{2,1,0:T(8,128)(2,1)S(1)}, bf16[2,2048,256]{2,1,0:T(8,128)(2,1)}, u32[]{:S(2)}, u32[]{:S(2)}) collective-permute-start(bf16[2,2048,256]{2,1,0:T(8,128)(2,1)S(1)} %constant_dynamic-update-slice_fusion.refs_0_), channel_id=1, source_target_pairs={{0,1},{1,0},{2,3},{3,2},{4,5},{5,4},{6,7},{7,6},{8,9},{9,8},{10,11... | collective-permute-start | bytes 6291464 | tf_op jit(solution)/shard_map/ppermute | solution.py:467
  31.8 30.5 %collective-permute-start.8 = (bf16[2,2048,256]{2,1,0:T(8,128)(2,1)}, bf16[2,2048,256]{2,1,0:T(8,128)(2,1)}, u32[]{:S(2)}, u32[]{:S(2)}) collective-permute-start(bf16[2,2048,256]{2,1,0:T(8,128)(2,1)} %collective-permute-done.6.refs_1_), channel_id=1, source_target_pairs={{0,1},{1,0},{2,3},{3,2},{4,5},{5,4},{6,7},{7,6},{8,9},{9,8},{10,11... | collective-permute-start | bytes 6291464 | tf_op jit(solution)/shard_map/ppermute | solution.py:467
  39.1 23.1 %collective-permute-start.10 = (bf16[256,2048]{1,0:T(8,128)(2,1)}, bf16[256,2048]{1,0:T(8,128)(2,1)}, u32[]{:S(2)}, u32[]{:S(2)}) collective-permute-start(bf16[256,2048]{1,0:T(8,128)(2,1)} %bitcast.9), channel_id=1, source_target_pairs={{0,1},{1,0},{2,3},{3,2},{4,5},{5,4},{6,7},{7,6},{8,9},{9,8},{10,11... | collective-permute-start | bytes 3145736 | tf_op jit(solution)/shard_map/ppermute | solution.py:467
  43.9 18.3 %collective-permute-start.11 = (bf16[256,2048]{1,0:T(8,128)(2,1)}, bf16[256,2048]{1,0:T(8,128)(2,1)}, u32[]{:S(2)}, u32[]{:S(2)}) collective-permute-start(bf16[256,2048]{1,0:T(8,128)(2,1)} %collective-permute-done.9.refs_5_), channel_id=1, source_target_pairs={{0,1},{1,0},{2,3},{3,2},{4,5},{5,4},{6,7},{7,6},{8,9},{9,8},{10,11... | collective-permute-start | bytes 3145736 | tf_op jit(solution)/shard_map/ppermute | solution.py:467
  57.4 33.3 %copy-start.15 = (bf16[256,128]{1,0:T(8,128)(2,1)S(1)}, bf16[256,128]{1,0:T(8,128)(2,1)}, u32[]{:S(2)}) copy-start(bf16[256,128]{1,0:T(8,128)(2,1)} %copy-done.14) | copy-start | bytes 196612
  57.4 25.7 %all-to-all-start = ((bf16[8,160,256]{2,1,0:T(8,128)(2,1)}), bf16[8,160,256]{2,1,0:T(8,128)(2,1)}, u32[]{:S(2)}, u32[]{:S(2)}) async-start(bf16[8,160,256]{2,1,0:T(8,128)(2,1)} %copy-done.3), calls=%async_computation | async-start | bytes 1310720 | tf_op jit(solution)/shard_map/all_to_all | solution.py:483
  83.1 37.4 %all-to-all-start.2 = ((bf16[16,192,128]{2,1,0:T(8,128)(2,1)}), bf16[16,192,128]{2,1,0:T(8,128)(2,1)S(1)}, u32[]{:S(2)}, u32[]{:S(2)}) async-start(bf16[16,192,128]{2,1,0:T(8,128)(2,1)} %shard_map.180), calls=%async_computation.2 | async-start | bytes 1572864 | tf_op jit(solution)/shard_map/all_to_all | solution.py:488
  90.7 27.2 %copy-start.20 = (f32[256,2]{0,1:T(2,128)S(1)}, f32[256,2]{0,1:T(2,128)}, u32[]{:S(2)}) copy-start(f32[256,2]{0,1:T(2,128)} %param.26) | copy-start | bytes 6148
  90.7 9.4 %collective-permute-start = (bf16[256,128]{1,0:T(8,128)(2,1)S(1)}, bf16[256,128]{1,0:T(8,128)(2,1)S(1)}, u32[]{:S(2)}, u32[]{:S(2)}) collective-permute-start(bf16[256,128]{1,0:T(8,128)(2,1)S(1)} %copy-done.15), channel_id=1, source_target_pairs={{0,48},{16,0},{32,16},{48,32},{64,112},{80,64},{96,80},{112,96},{1... | collective-permute-start | bytes 196616 | tf_op jit(solution)/shard_map/ppermute | solution.py:482
  95.1 6.8 %collective-permute-start.1 = (bf16[256,128]{1,0:T(8,128)(2,1)S(1)}, bf16[256,128]{1,0:T(8,128)(2,1)S(1)}, u32[]{:S(2)}, u32[]{:S(2)}) collective-permute-start(bf16[256,128]{1,0:T(8,128)(2,1)S(1)} %copy-done.15), channel_id=1, source_target_pairs={{0,32},{16,48},{32,0},{48,16},{64,96},{80,112},{96,64},{112,80},{1... | collective-permute-start | bytes 196616 | tf_op jit(solution)/shard_map/ppermute | solution.py:482
  97.5 6.5 %collective-permute-start.2 = (bf16[256,128]{1,0:T(8,128)(2,1)S(1)}, bf16[256,128]{1,0:T(8,128)(2,1)S(1)}, u32[]{:S(2)}, u32[]{:S(2)}) collective-permute-start(bf16[256,128]{1,0:T(8,128)(2,1)S(1)} %copy-done.15), channel_id=1, source_target_pairs={{0,16},{16,32},{32,48},{48,0},{64,80},{80,96},{96,112},{112,64},{1... | collective-permute-start | bytes 196616 | tf_op jit(solution)/shard_map/ppermute | solution.py:482
  108.6 40.2 %copy-start.7 = (s32[256,2]{1,0:T(8,128)S(1)}, s32[256,2]{1,0:T(8,128)}, u32[]{:S(2)}) copy-start(s32[256,2]{1,0:T(8,128)} %copy-done.6) | copy-start | bytes 6148
  108.6 9.5 %collective-permute-start.3 = (bf16[256,128]{1,0:T(8,128)(2,1)S(1)}, bf16[256,128]{1,0:T(8,128)(2,1)S(1)}, u32[]{:S(2)}, u32[]{:S(2)}) collective-permute-start(bf16[256,128]{1,0:T(8,128)(2,1)S(1)} %get-tuple-element.13), channel_id=1, source_target_pairs={{0,16},{16,32},{32,48},{48,0},{64,80},{80,96},{96,112},{112,64},{1... | collective-permute-start | bytes 196616 | tf_op jit(solution)/shard_map/ppermute | solution.py:492
  110.8 7.3 %collective-permute-start.4 = (bf16[256,128]{1,0:T(8,128)(2,1)S(1)}, bf16[256,128]{1,0:T(8,128)(2,1)S(1)}, u32[]{:S(2)}, u32[]{:S(2)}) collective-permute-start(bf16[256,128]{1,0:T(8,128)(2,1)S(1)} %get-tuple-element.14), channel_id=1, source_target_pairs={{0,32},{16,48},{32,0},{48,16},{64,96},{80,112},{96,64},{112,80},{1... | collective-permute-start | bytes 196616 | tf_op jit(solution)/shard_map/ppermute | solution.py:492
  114.0 5.9 %collective-permute-start.5 = (bf16[256,128]{1,0:T(8,128)(2,1)S(1)}, bf16[256,128]{1,0:T(8,128)(2,1)S(1)}, u32[]{:S(2)}, u32[]{:S(2)}) collective-permute-start(bf16[256,128]{1,0:T(8,128)(2,1)S(1)} %get-tuple-element.15), channel_id=1, source_target_pairs={{0,48},{16,0},{32,16},{48,32},{64,112},{80,64},{96,80},{112,96},{1... | collective-permute-start | bytes 196616 | tf_op jit(solution)/shard_map/ppermute | solution.py:492
  121.7 27.1 %all-to-all-start.3 = ((bf16[32,24,128]{2,1,0:T(8,128)(2,1)}), bf16[32,24,128]{2,1,0:T(8,128)(2,1)S(1)}, u32[]{:S(2)}, u32[]{:S(2)}) async-start(bf16[32,24,128]{2,1,0:T(8,128)(2,1)} %shard_map.181.refs_0_), calls=%async_computation.3 | async-start | bytes 393216 | tf_op jit(solution)/shard_map/all_to_all | solution.py:501
  (13 other events, 18.8 us)

commit v9 on v8

--- a/solution.py
+++ b/solution.py
@@ -45,21 +45,23 @@
             positions[:, None] * frequency, (1, 2)
         )
         tables += [np.cos(angles).astype(np.float32), np.sin(angles).astype(np.float32)]
-    return tables
+    return np.concatenate(tables)
 
 
 def prepare(index, queries, latents, rope_key, gain, weight, tables, copies):
     rows = queries.shape[0]
+    blocks = tables.shape[0] // 2 - rows
     first, last = PLAIN_HEAD_DIM, PLAIN_HEAD_DIM + ROPE
     half = ROPE // 2
 
     def body(index_ref, query_ref, latent_ref, rope_ref, gain_ref, weight_ref, *refs):
-        block_cos, block_sin, place_cos, place_sin = refs[:4]
-        query_out, key_out, padded_ref = refs[4:]
-        base_cos = block_cos[pl.ds(index_ref[0], 1), :]
-        base_sin = block_sin[pl.ds(index_ref[0], 1), :]
-        cosine = base_cos * place_cos[...] - base_sin * place_sin[...]
-        sine = base_sin * place_cos[...] + base_cos * place_sin[...]
+        table_ref, query_out, key_out, padded_ref = refs
+        base_cos = table_ref[pl.ds(index_ref[0], 1), :]
+        base_sin = table_ref[pl.ds(index_ref[0] + blocks, 1), :]
+        place_cos = table_ref[2 * blocks : 2 * blocks + rows, :]
+        place_sin = table_ref[2 * blocks + rows :, :]
+        cosine = base_cos * place_cos - base_sin * place_sin
+        sine = base_sin * place_cos + base_cos * place_sin
         lane = lax.broadcasted_iota(jnp.int32, (rows, LANES), 1)
         early = lane < first + half
         sine = jnp.where(early, -sine, sine)
@@ -91,14 +93,14 @@
             jax.ShapeDtypeStruct((rows, LANES), jnp.bfloat16),
             jax.ShapeDtypeStruct((copies, LANES + ROPE, rows), jnp.bfloat16),
         ),
-        in_specs=[SMEM] + [VMEM] * 9,
+        in_specs=[SMEM] + [VMEM] * 6,
         out_specs=(VMEM, VMEM),
         scratch_shapes=[pltpu.VMEM((rows, LANES), jnp.float32)],
-        compiler_params=pltpu.CompilerParams(vmem_limit_bytes=16 * 1024 * 1024),
+        compiler_params=pltpu.CompilerParams(vmem_limit_bytes=60 * 1024 * 1024),
         cost_estimate=pl.CostEstimate(
             flops=2 * latents.size * weight.shape[1], transcendentals=0, bytes_accessed=0
         ),
-    )(index, queries, latents, rope_key, gain, weight, *tables)
+    )(index, queries, latents, rope_key, gain, weight, tables)
 
 
 def sequenced(array, *earlier):

time: 151 us -> 148 us (0.980)
  local copies, waits for them, and re-layouts: 12.4 us -> 6.72 us
  Pallas kernels: 16.6 us -> 18.6 us
    unnamed x47 -> x27, local copies, waits for them, and re-layouts: 12.4 us -> 6.65 us
    pallas_call x1, Pallas kernels: 0.48 us -> 2.51 us  [prepare(): pl.pallas_call(body, out_shape=(jax.ShapeDtypeStruct((rows, LANES), jnp.b...]
  transfers between devices with their start and end apart: 16 -> 16, of which waited for: 6 -> 6; matrix products, arithmetic and copies ran while one was open for 1% -> 2% of each run, Pallas kernels for 9% -> 11%
where the time goes in v9:
time: 148 us; the launch traced here: 147 us
  starting transfers between devices  74.2 us (50%)
  waiting for transfers between devices  23.8 us (16%)
  blocking collectives  21.4 us (14%)
  Pallas kernels  18.6 us (13%)
  local copies, waits for them, and re-layouts  6.72 us (5%)
    all_gather x1, blocking collectives, local(): lax.all_gather(sequenced(attended, summed), 'tp', axis=0, tiled=True)  21.4 us
    ppermute x4, starting transfers between devices, local(): group.append(lax.ppermute(weight, 'tp', partner))  18 us
    all_to_all x1, waiting for transfers between devices, local(): lax.all_to_all(own_keys, 'ep', 0, 0, tiled=True, axis_index_groups=z_groups)  13.5 us
    all_to_all x1, starting transfers between devices, local(): arrived = lax.all_to_all(outgoing, 'ep', 0, 0, tiled=True)  12.9 us
    ppermute x3, starting transfers between devices, local(): query_all.append(lax.ppermute(query, 'ep', x_shifts[x_count - i]))  9.33 us
    ppermute x3, starting transfers between devices, local(): lax.ppermute(partial_all[i], 'ep', x_shifts[i])  9.22 us
    ppermute x2, starting transfers between devices, local(): group.append(lax.ppermute(group[0], 'tp', neighbour))  7.84 us
    all_to_all x1, starting transfers between devices, local(): groups = lax.all_to_all(partial_out, 'tp', 0, 0, tiled=True)  7.61 us
  transfers between devices with their start and end apart: 16, of which 6 were waited for; matrix products, arithmetic and copies ran while one was open for 2% of the time, Pallas kernels for 11%

profile of v9, /device:TPU:1, one launch (start us, length us, event | category | flops | bytes accessed | tf_op | source)
XLA Modules:
  0.0 146.7 jit_solution(5282261356265796275)
XLA Ops:
  2.3 5.9 %collective-permute-start.6 = (bf16[2,2048,256]{2,1,0:T(8,128)(2,1)S(1)}, bf16[2,2048,256]{2,1,0:T(8,128)(2,1)}, u32[]{:S(2)}, u32[]{:S(2)}) collective-permute-start(bf16[2,2048,256]{2,1,0:T(8,128)(2,1)S(1)} %constant_dynamic-update-slice_fusion.refs_0_), channel_id=1, source_target_pairs={{0,2},{1,15},{2,0},{3,5},{4,6},{5,3},{6,4},{7,9},{8,10},{9,7},{10,... | collective-permute-start | bytes 6291464 | tf_op jit(solution)/shard_map/ppermute | solution.py:460
  9.6 2.6 %shard_map.152 = (bf16[32,4,24,128]{3,2,1,0:T(8,128)(2,1)S(1)}, s32[256,2]{1,0:T(8,128)S(1)}) custom-call(s32[1]{0:T(128)} %bitcast.2.index_ref, bf16[256,2048]{1,0:T(8,128)(2,1)S(1)} %copy-done.3, f32[1,2048]{1,0:T(1,128)S(1)} %bitcast.12, s32[256,2]{1,0:T(8,128)S(1)} %copy.18.routes_ref), custom_call_target="tpu_custom_call" | custom-call | flops 805306368 | tf_op jit(solution)/shard_map/pallas_call | solution.py:190
  13.1 12.9 %all-to-all-start.1 = ((bf16[32,4,24,128]{3,2,1,0:T(8,128)(2,1)}), bf16[32,4,24,128]{3,2,1,0:T(8,128)(2,1)S(1)}, u32[]{:S(2)}, u32[]{:S(2)}) async-start(bf16[32,4,24,128]{3,2,1,0:T(8,128)(2,1)} %copy-done.2), calls=%async_computation.1 | async-start | bytes 1572864 | tf_op jit(solution)/shard_map/all_to_all | solution.py:465
  26.0 1.9 %collective-permute-start.9 = (bf16[256,2048]{1,0:T(8,128)(2,1)}, bf16[256,2048]{1,0:T(8,128)(2,1)}, u32[]{:S(2)}, u32[]{:S(2)}) collective-permute-start(bf16[256,2048]{1,0:T(8,128)(2,1)} %bitcast.8), channel_id=1, source_target_pairs={{0,2},{1,15},{2,0},{3,5},{4,6},{5,3},{6,4},{7,9},{8,10},{9,7},{10,... | collective-permute-start | bytes 3145736 | tf_op jit(solution)/shard_map/ppermute | solution.py:460
  29.9 2.1 %collective-permute-done.6.refs_1_ = bf16[2,2048,256]{2,1,0:T(8,128)(2,1)} collective-permute-done((bf16[2,2048,256]{2,1,0:T(8,128)(2,1)S(1)}, bf16[2,2048,256]{2,1,0:T(8,128)(2,1)}, u32[]{:S(2)}, u32[]{:S(2)}) %collective-permute-start.6) | collective-permute-done | bytes 2097184 | tf_op jit(solution)/shard_map/ppermute | solution.py:460
  31.9 7.1 %collective-permute-start.8 = (bf16[2,2048,256]{2,1,0:T(8,128)(2,1)}, bf16[2,2048,256]{2,1,0:T(8,128)(2,1)}, u32[]{:S(2)}, u32[]{:S(2)}) collective-permute-start(bf16[2,2048,256]{2,1,0:T(8,128)(2,1)} %collective-permute-done.6.refs_1_), channel_id=1, source_target_pairs={{0,1},{1,0},{2,3},{3,2},{4,5},{5,4},{6,7},{7,6},{8,9},{9,8},{10,11... | collective-permute-start | bytes 6291464 | tf_op jit(solution)/shard_map/ppermute | solution.py:469
  39.1 1.9 %collective-permute-start.10 = (bf16[256,2048]{1,0:T(8,128)(2,1)}, bf16[256,2048]{1,0:T(8,128)(2,1)}, u32[]{:S(2)}, u32[]{:S(2)}) collective-permute-start(bf16[256,2048]{1,0:T(8,128)(2,1)} %bitcast.9), channel_id=1, source_target_pairs={{0,1},{1,0},{2,3},{3,2},{4,5},{5,4},{6,7},{7,6},{8,9},{9,8},{10,11... | collective-permute-start | bytes 3145736 | tf_op jit(solution)/shard_map/ppermute | solution.py:469
  41.0 2.3 %collective-permute-done.9.refs_5_ = bf16[256,2048]{1,0:T(8,128)(2,1)} collective-permute-done((bf16[256,2048]{1,0:T(8,128)(2,1)}, bf16[256,2048]{1,0:T(8,128)(2,1)}, u32[]{:S(2)}, u32[]{:S(2)}) %collective-permute-start.9) | collective-permute-done | bytes 1048608 | tf_op jit(solution)/shard_map/ppermute | solution.py:460
  43.3 7.0 %collective-permute-start.11 = (bf16[256,2048]{1,0:T(8,128)(2,1)}, bf16[256,2048]{1,0:T(8,128)(2,1)}, u32[]{:S(2)}, u32[]{:S(2)}) collective-permute-start(bf16[256,2048]{1,0:T(8,128)(2,1)} %collective-permute-done.9.refs_5_), channel_id=1, source_target_pairs={{0,1},{1,0},{2,3},{3,2},{4,5},{5,4},{6,7},{7,6},{8,9},{9,8},{10,11... | collective-permute-start | bytes 3145736 | tf_op jit(solution)/shard_map/ppermute | solution.py:469
  51.8 2.5 %shard_map.149 = (bf16[256,128]{1,0:T(8,128)(2,1)}, bf16[8,160,256]{2,1,0:T(8,128)(2,1)}) custom-call(s32[1]{0:T(128)} %bitcast.index_ref, bf16[256,96]{1,0:T(8,128)(2,1)} %copy.16.query_ref, bf16[256,512]{1,0:T(8,128)(2,1)} %latent_ref.1, bf16[256,32]{1,0:T(8,128)(2,1)} %copy.17.rope_ref, f32[1,512]{1,0:T(1,128)} %bitcast.13, bf16[512,128]{1,0:T(8,128)(2,1)} %weight_ref.2, ...), custom_call_target="tpu_custom_call" | custom-call | flops 33554432 | tf_op jit(solution)/shard_map/pallas_call | solution.py:90
  54.3 4.8 %all-to-all-start = ((bf16[8,160,256]{2,1,0:T(8,128)(2,1)}), bf16[8,160,256]{2,1,0:T(8,128)(2,1)}, u32[]{:S(2)}, u32[]{:S(2)}) async-start(bf16[8,160,256]{2,1,0:T(8,128)(2,1)} %get-tuple-element.10), calls=%async_computation | async-start | bytes 1310720 | tf_op jit(solution)/shard_map/all_to_all | solution.py:485
  60.4 6.1 %shard_map.153 = bf16[16,192,128]{2,1,0:T(8,128)(2,1)} custom-call(bf16[32,4,24,128]{3,2,1,0:T(8,128)(2,1)S(1)} %all-to-all-done.1.rows_ref, bf16[2,2048,256]{2,1,0:T(8,128)(2,1)S(1)} %constant_dynamic-update-slice_fusion.refs_0_, bf16[2,2048,256]{2,1,0:T(8,128)(2,1)} %collective-permute-done.6.refs_1_, ...), custom_call_target="tpu_custom_call" | custom-call | flops 2415919104 | tf_op jit(solution)/shard_map/pallas_call | solution.py:377
  66.5 13.5 %all-to-all-done.key_ref = bf16[8,160,256]{2,1,0:T(8,128)(2,1)} async-done(((bf16[8,160,256]{2,1,0:T(8,128)(2,1)}), bf16[8,160,256]{2,1,0:T(8,128)(2,1)}, u32[]{:S(2)}, u32[]{:S(2)}) %all-to-all-start) | async-done | bytes 655392 | tf_op jit(solution)/shard_map/all_to_all | solution.py:485
  80.0 7.6 %all-to-all-start.2 = ((bf16[16,192,128]{2,1,0:T(8,128)(2,1)}), bf16[16,192,128]{2,1,0:T(8,128)(2,1)S(1)}, u32[]{:S(2)}, u32[]{:S(2)}) async-start(bf16[16,192,128]{2,1,0:T(8,128)(2,1)} %shard_map.153), calls=%async_computation.2 | async-start | bytes 1572864 | tf_op jit(solution)/shard_map/all_to_all | solution.py:490
  87.6 4.4 %collective-permute-start = (bf16[256,128]{1,0:T(8,128)(2,1)S(1)}, bf16[256,128]{1,0:T(8,128)(2,1)S(1)}, u32[]{:S(2)}, u32[]{:S(2)}) collective-permute-start(bf16[256,128]{1,0:T(8,128)(2,1)S(1)} %copy-done.4), channel_id=1, source_target_pairs={{0,48},{16,0},{32,16},{48,32},{64,112},{80,64},{96,80},{112,96},{1... | collective-permute-start | bytes 196616 | tf_op jit(solution)/shard_map/ppermute | solution.py:484
  92.0 2.4 %collective-permute-start.1 = (bf16[256,128]{1,0:T(8,128)(2,1)S(1)}, bf16[256,128]{1,0:T(8,128)(2,1)S(1)}, u32[]{:S(2)}, u32[]{:S(2)}) collective-permute-start(bf16[256,128]{1,0:T(8,128)(2,1)S(1)} %copy-done.4), channel_id=1, source_target_pairs={{0,32},{16,48},{32,0},{48,16},{64,96},{80,112},{96,64},{112,80},{1... | collective-permute-start | bytes 196616 | tf_op jit(solution)/shard_map/ppermute | solution.py:484
  94.5 2.5 %collective-permute-start.2 = (bf16[256,128]{1,0:T(8,128)(2,1)S(1)}, bf16[256,128]{1,0:T(8,128)(2,1)S(1)}, u32[]{:S(2)}, u32[]{:S(2)}) collective-permute-start(bf16[256,128]{1,0:T(8,128)(2,1)S(1)} %copy-done.4), channel_id=1, source_target_pairs={{0,16},{16,32},{32,48},{48,0},{64,80},{80,96},{96,112},{112,64},{1... | collective-permute-start | bytes 196616 | tf_op jit(solution)/shard_map/ppermute | solution.py:484
  98.8 2.1 %collective-permute-done.2.refs_3_ = bf16[256,128]{1,0:T(8,128)(2,1)S(1)} collective-permute-done((bf16[256,128]{1,0:T(8,128)(2,1)S(1)}, bf16[256,128]{1,0:T(8,128)(2,1)S(1)}, u32[]{:S(2)}, u32[]{:S(2)}) %collective-permute-start.2) | collective-permute-done | bytes 65568 | tf_op jit(solution)/shard_map/ppermute | solution.py:484
  101.0 4.5 %shard_map.150 = (bf16[256,128]{1,0:T(8,128)(2,1)S(1)}, bf16[256,128]{1,0:T(8,128)(2,1)S(1)}, bf16[256,128]{1,0:T(8,128)(2,1)S(1)}, bf16[256,128]{1,0:T(8,128)(2,1)S(1)}) custom-call(bf16[8,160,256]{2,1,0:T(8,128)(2,1)} %all-to-all-done.key_ref, bf16[256,128]{1,0:T(8,128)(2,1)S(1)} %copy-done.4, bf16[256,128]{1,0:T(8,128)(2,1)S(1)} %collective-permute-done.refs_1_, ...), custom_call_target="tpu_custom_call" | custom-call | flops 2147483648 | tf_op jit(solution)/shard_map/pallas_call | solution.py:272
  107.4 3.1 %collective-permute-start.4 = (bf16[256,128]{1,0:T(8,128)(2,1)S(1)}, bf16[256,128]{1,0:T(8,128)(2,1)S(1)}, u32[]{:S(2)}, u32[]{:S(2)}) collective-permute-start(bf16[256,128]{1,0:T(8,128)(2,1)S(1)} %get-tuple-element.14), channel_id=1, source_target_pairs={{0,32},{16,48},{32,0},{48,16},{64,96},{80,112},{96,64},{112,80},{1... | collective-permute-start | bytes 196616 | tf_op jit(solution)/shard_map/ppermute | solution.py:494
  110.6 4.1 %collective-permute-start.5 = (bf16[256,128]{1,0:T(8,128)(2,1)S(1)}, bf16[256,128]{1,0:T(8,128)(2,1)S(1)}, u32[]{:S(2)}, u32[]{:S(2)}) collective-permute-start(bf16[256,128]{1,0:T(8,128)(2,1)S(1)} %get-tuple-element.15), channel_id=1, source_target_pairs={{0,48},{16,0},{32,16},{48,32},{64,112},{80,64},{96,80},{112,96},{1... | collective-permute-start | bytes 196616 | tf_op jit(solution)/shard_map/ppermute | solution.py:494
  114.9 2.0 %collective-permute-done.5.refs_3_ = bf16[256,128]{1,0:T(8,128)(2,1)S(1)} collective-permute-done((bf16[256,128]{1,0:T(8,128)(2,1)S(1)}, bf16[256,128]{1,0:T(8,128)(2,1)S(1)}, u32[]{:S(2)}, u32[]{:S(2)}) %collective-permute-start.5) | collective-permute-done | bytes 65568 | tf_op jit(solution)/shard_map/ppermute | solution.py:494
  118.7 4.5 %all-to-all-start.3 = ((bf16[32,24,128]{2,1,0:T(8,128)(2,1)}), bf16[32,24,128]{2,1,0:T(8,128)(2,1)S(1)}, u32[]{:S(2)}, u32[]{:S(2)}) async-start(bf16[32,24,128]{2,1,0:T(8,128)(2,1)} %shard_map.154.refs_0_), calls=%async_computation.3 | async-start | bytes 393216 | tf_op jit(solution)/shard_map/all_to_all | solution.py:503
  123.2 21.4 %all_gather.3 = bf16[1024,256]{1,0:T(8,128)(2,1)S(1)} all-gather(bf16[64,256]{1,0:T(8,128)(2,1)S(1)} %shard_map.155), channel_id=1, replica_groups=mesh['ep'=32,'tp'=16] {'tp'}, dimensions={0}, use_global_device_ids=true | all-gather | bytes 557056 | tf_op jit(solution)/shard_map/all_gather | solution.py:498
  (46 shorter events, 16.4 us)
Async XLA Ops:
  0.6 144.0 %copy-start = (bf16[1024,128]{1,0:T(8,128)(2,1)S(1)}, bf16[1024,128]{1,0:T(8,128)(2,1)}, u32[]{:S(2)}) copy-start(bf16[1024,128]{1,0:T(8,128)(2,1)} %param.19) | copy-start | bytes 786436
  0.6 1.6 %copy-start.6 = (bf16[1,2048,256]{2,1,0:T(8,128)(2,1)S(1)}, bf16[1,2048,256]{2,1,0:T(8,128)(2,1)}, u32[]{:S(2)}) copy-start(bf16[1,2048,256]{2,1,0:T(8,128)(2,1)} %param.25) | copy-start | bytes 3145732
  0.7 7.6 %copy-start.9 = (s32[256,2]{0,1:T(2,128)S(1)}, s32[256,2]{0,1:T(2,128)}, u32[]{:S(2)}) copy-start(s32[256,2]{0,1:T(2,128)} %param.22) | copy-start | bytes 6148
  0.7 7.7 %copy-start.5 = (f32[2048]{0:T(1024)S(1)}, f32[2048]{0:T(1024)}, u32[]{:S(2)}) copy-start(f32[2048]{0:T(1024)} %param.21) | copy-start | bytes 24580
  2.3 29.6 %collective-permute-start.6 = (bf16[2,2048,256]{2,1,0:T(8,128)(2,1)S(1)}, bf16[2,2048,256]{2,1,0:T(8,128)(2,1)}, u32[]{:S(2)}, u32[]{:S(2)}) collective-permute-start(bf16[2,2048,256]{2,1,0:T(8,128)(2,1)S(1)} %constant_dynamic-update-slice_fusion.refs_0_), channel_id=1, source_target_pairs={{0,2},{1,15},{2,0},{3,5},{4,6},{5,3},{6,4},{7,9},{8,10},{9,7},{10,... | collective-permute-start | bytes 6291464 | tf_op jit(solution)/shard_map/ppermute | solution.py:460
  9.6 40.7 %copy-start.7 = (bf16[256,96]{0,1:T(8,128)(2,1)S(1)}, bf16[256,96]{0,1:T(8,128)(2,1)}, u32[]{:S(2)}) copy-start(bf16[256,96]{0,1:T(8,128)(2,1)} %param.14) | copy-start | bytes 147460
  9.6 41.4 %copy-start.8 = (bf16[256,32]{0,1:T(8,128)(2,1)S(1)}, bf16[256,32]{0,1:T(8,128)(2,1)}, u32[]{:S(2)}) copy-start(bf16[256,32]{0,1:T(8,128)(2,1)} %param.16) | copy-start | bytes 49156
  13.1 41.2 %all-to-all-start.1 = ((bf16[32,4,24,128]{3,2,1,0:T(8,128)(2,1)}), bf16[32,4,24,128]{3,2,1,0:T(8,128)(2,1)S(1)}, u32[]{:S(2)}, u32[]{:S(2)}) async-start(bf16[32,4,24,128]{3,2,1,0:T(8,128)(2,1)} %copy-done.2), calls=%async_computation.1 | async-start | bytes 1572864 | tf_op jit(solution)/shard_map/all_to_all | solution.py:465
  26.0 17.3 %collective-permute-start.9 = (bf16[256,2048]{1,0:T(8,128)(2,1)}, bf16[256,2048]{1,0:T(8,128)(2,1)}, u32[]{:S(2)}, u32[]{:S(2)}) collective-permute-start(bf16[256,2048]{1,0:T(8,128)(2,1)} %bitcast.8), channel_id=1, source_target_pairs={{0,2},{1,15},{2,0},{3,5},{4,6},{5,3},{6,4},{7,9},{8,10},{9,7},{10,... | collective-permute-start | bytes 3145736 | tf_op jit(solution)/shard_map/ppermute | solution.py:460
  27.9 31.2 %collective-permute-start.7 = (bf16[2,2048,256]{2,1,0:T(8,128)(2,1)S(1)}, bf16[2,2048,256]{2,1,0:T(8,128)(2,1)}, u32[]{:S(2)}, u32[]{:S(2)}) collective-permute-start(bf16[2,2048,256]{2,1,0:T(8,128)(2,1)S(1)} %constant_dynamic-update-slice_fusion.refs_0_), channel_id=1, source_target_pairs={{0,1},{1,0},{2,3},{3,2},{4,5},{5,4},{6,7},{7,6},{8,9},{9,8},{10,11... | collective-permute-start | bytes 6291464 | tf_op jit(solution)/shard_map/ppermute | solution.py:469
  31.9 27.2 %collective-permute-start.8 = (bf16[2,2048,256]{2,1,0:T(8,128)(2,1)}, bf16[2,2048,256]{2,1,0:T(8,128)(2,1)}, u32[]{:S(2)}, u32[]{:S(2)}) collective-permute-start(bf16[2,2048,256]{2,1,0:T(8,128)(2,1)} %collective-permute-done.6.refs_1_), channel_id=1, source_target_pairs={{0,1},{1,0},{2,3},{3,2},{4,5},{5,4},{6,7},{7,6},{8,9},{9,8},{10,11... | collective-permute-start | bytes 6291464 | tf_op jit(solution)/shard_map/ppermute | solution.py:469
  39.1 20.1 %collective-permute-start.10 = (bf16[256,2048]{1,0:T(8,128)(2,1)}, bf16[256,2048]{1,0:T(8,128)(2,1)}, u32[]{:S(2)}, u32[]{:S(2)}) collective-permute-start(bf16[256,2048]{1,0:T(8,128)(2,1)} %bitcast.9), channel_id=1, source_target_pairs={{0,1},{1,0},{2,3},{3,2},{4,5},{5,4},{6,7},{7,6},{8,9},{9,8},{10,11... | collective-permute-start | bytes 3145736 | tf_op jit(solution)/shard_map/ppermute | solution.py:469
  43.3 15.9 %collective-permute-start.11 = (bf16[256,2048]{1,0:T(8,128)(2,1)}, bf16[256,2048]{1,0:T(8,128)(2,1)}, u32[]{:S(2)}, u32[]{:S(2)}) collective-permute-start(bf16[256,2048]{1,0:T(8,128)(2,1)} %collective-permute-done.9.refs_5_), channel_id=1, source_target_pairs={{0,1},{1,0},{2,3},{3,2},{4,5},{5,4},{6,7},{7,6},{8,9},{9,8},{10,11... | collective-permute-start | bytes 3145736 | tf_op jit(solution)/shard_map/ppermute | solution.py:469
  54.3 33.3 %copy-start.4 = (bf16[256,128]{1,0:T(8,128)(2,1)S(1)}, bf16[256,128]{1,0:T(8,128)(2,1)}, u32[]{:S(2)}) copy-start(bf16[256,128]{1,0:T(8,128)(2,1)} %get-tuple-element.11.refs_0_) | copy-start | bytes 196612
  54.3 25.7 %all-to-all-start = ((bf16[8,160,256]{2,1,0:T(8,128)(2,1)}), bf16[8,160,256]{2,1,0:T(8,128)(2,1)}, u32[]{:S(2)}, u32[]{:S(2)}) async-start(bf16[8,160,256]{2,1,0:T(8,128)(2,1)} %get-tuple-element.10), calls=%async_computation | async-start | bytes 1310720 | tf_op jit(solution)/shard_map/all_to_all | solution.py:485
  80.0 37.4 %all-to-all-start.2 = ((bf16[16,192,128]{2,1,0:T(8,128)(2,1)}), bf16[16,192,128]{2,1,0:T(8,128)(2,1)S(1)}, u32[]{:S(2)}, u32[]{:S(2)}) async-start(bf16[16,192,128]{2,1,0:T(8,128)(2,1)} %shard_map.153), calls=%async_computation.2 | async-start | bytes 1572864 | tf_op jit(solution)/shard_map/all_to_all | solution.py:490
  87.6 27.1 %copy-start.10 = (f32[256,2]{0,1:T(2,128)S(1)}, f32[256,2]{0,1:T(2,128)}, u32[]{:S(2)}) copy-start(f32[256,2]{0,1:T(2,128)} %param.23) | copy-start | bytes 6148
  87.6 9.4 %collective-permute-start = (bf16[256,128]{1,0:T(8,128)(2,1)S(1)}, bf16[256,128]{1,0:T(8,128)(2,1)S(1)}, u32[]{:S(2)}, u32[]{:S(2)}) collective-permute-start(bf16[256,128]{1,0:T(8,128)(2,1)S(1)} %copy-done.4), channel_id=1, source_target_pairs={{0,48},{16,0},{32,16},{48,32},{64,112},{80,64},{96,80},{112,96},{1... | collective-permute-start | bytes 196616 | tf_op jit(solution)/shard_map/ppermute | solution.py:484
  92.0 6.8 %collective-permute-start.1 = (bf16[256,128]{1,0:T(8,128)(2,1)S(1)}, bf16[256,128]{1,0:T(8,128)(2,1)S(1)}, u32[]{:S(2)}, u32[]{:S(2)}) collective-permute-start(bf16[256,128]{1,0:T(8,128)(2,1)S(1)} %copy-done.4), channel_id=1, source_target_pairs={{0,32},{16,48},{32,0},{48,16},{64,96},{80,112},{96,64},{112,80},{1... | collective-permute-start | bytes 196616 | tf_op jit(solution)/shard_map/ppermute | solution.py:484
  94.5 6.5 %collective-permute-start.2 = (bf16[256,128]{1,0:T(8,128)(2,1)S(1)}, bf16[256,128]{1,0:T(8,128)(2,1)S(1)}, u32[]{:S(2)}, u32[]{:S(2)}) collective-permute-start(bf16[256,128]{1,0:T(8,128)(2,1)S(1)} %copy-done.4), channel_id=1, source_target_pairs={{0,16},{16,32},{32,48},{48,0},{64,80},{80,96},{96,112},{112,64},{1... | collective-permute-start | bytes 196616 | tf_op jit(solution)/shard_map/ppermute | solution.py:484
  105.5 9.4 %collective-permute-start.3 = (bf16[256,128]{1,0:T(8,128)(2,1)S(1)}, bf16[256,128]{1,0:T(8,128)(2,1)S(1)}, u32[]{:S(2)}, u32[]{:S(2)}) collective-permute-start(bf16[256,128]{1,0:T(8,128)(2,1)S(1)} %get-tuple-element.13), channel_id=1, source_target_pairs={{0,16},{16,32},{32,48},{48,0},{64,80},{80,96},{96,112},{112,64},{1... | collective-permute-start | bytes 196616 | tf_op jit(solution)/shard_map/ppermute | solution.py:494
  107.4 7.5 %collective-permute-start.4 = (bf16[256,128]{1,0:T(8,128)(2,1)S(1)}, bf16[256,128]{1,0:T(8,128)(2,1)S(1)}, u32[]{:S(2)}, u32[]{:S(2)}) collective-permute-start(bf16[256,128]{1,0:T(8,128)(2,1)S(1)} %get-tuple-element.14), channel_id=1, source_target_pairs={{0,32},{16,48},{32,0},{48,16},{64,96},{80,112},{96,64},{112,80},{1... | collective-permute-start | bytes 196616 | tf_op jit(solution)/shard_map/ppermute | solution.py:494
  110.6 6.3 %collective-permute-start.5 = (bf16[256,128]{1,0:T(8,128)(2,1)S(1)}, bf16[256,128]{1,0:T(8,128)(2,1)S(1)}, u32[]{:S(2)}, u32[]{:S(2)}) collective-permute-start(bf16[256,128]{1,0:T(8,128)(2,1)S(1)} %get-tuple-element.15), channel_id=1, source_target_pairs={{0,48},{16,0},{32,16},{48,32},{64,112},{80,64},{96,80},{112,96},{1... | collective-permute-start | bytes 196616 | tf_op jit(solution)/shard_map/ppermute | solution.py:494
  118.7 26.9 %all-to-all-start.3 = ((bf16[32,24,128]{2,1,0:T(8,128)(2,1)}), bf16[32,24,128]{2,1,0:T(8,128)(2,1)S(1)}, u32[]{:S(2)}, u32[]{:S(2)}) async-start(bf16[32,24,128]{2,1,0:T(8,128)(2,1)} %shard_map.154.refs_0_), calls=%async_computation.3 | async-start | bytes 393216 | tf_op jit(solution)/shard_map/all_to_all | solution.py:503
  (3 other events, 3.4 us)

commit v10 on v9

--- a/solution.py
+++ b/solution.py
@@ -126,13 +126,14 @@
     return place + source * (SHARE * (PARTS - 1))
 
 
-def pack_rows(index, moe_input, gain, routes, capacity, expert_total):
+def pack_rows(index, moe_input, gain, routes, capacity, expert_total, *earlier):
     rows, width = moe_input.shape
     places = expert_total * capacity
     top = routes.shape[1]
     wide = PARTS * LANES
 
-    def body(index_ref, input_ref, gain_ref, routes_ref, out_ref, place_ref):
+    def body(index_ref, input_ref, gain_ref, routes_ref, *refs):
+        out_ref, place_ref = refs[-2:]
         floats = input_ref[...].astype(jnp.float32)
         scale = lax.rsqrt(jnp.mean(floats * floats, axis=-1, keepdims=True) + EPSILON)
         normed = (floats * scale * gain_ref[...]).astype(jnp.bfloat16)
@@ -193,10 +194,11 @@
             jax.ShapeDtypeStruct((expert_total, width // wide, capacity, LANES), jnp.bfloat16),
             jax.ShapeDtypeStruct((rows, top), jnp.int32),
         ),
-        [SMEM, VMEM, VMEM, VMEM],
+        [SMEM, VMEM, VMEM, VMEM] + [ANY] * len(earlier),
         (VMEM, VMEM),
         2 * rows * places * width,
-    )(index, moe_input, gain, routes)
+        limit=60,
+    )(index, moe_input, gain, routes, *earlier)
 
 
 def add_up(parts, blocks, *earlier):
@@ -460,7 +462,7 @@
             group.append(lax.ppermute(group[0], "tp", neighbour))
 
         outgoing, places = pack_rows(
-            place_index, moe_input, moe_gain.reshape(1, -1), routes, capacity, ep_count
+            place_index, moe_input, moe_gain.reshape(1, -1), routes, capacity, ep_count, groups_of[0][0]
         )
         arrived = lax.all_to_all(outgoing, "ep", 0, 0, tiled=True)
 

time: 148 us -> 150 us (1.014)
  Pallas kernels: 18.6 us -> 20.7 us
    ppermute x4, starting transfers between devices: 18 us -> 14.8 us  [local(): group.append(lax.ppermute(weight, 'tp', partner))]
    ppermute x2, starting transfers between devices: 7.84 us -> 10.1 us  [local(): group.append(lax.ppermute(group[0], 'tp', neighbour))]
    pallas_call x1, Pallas kernels: 2.58 us -> 4.73 us  [pack_rows(): kernel_call(body, (jax.ShapeDtypeStruct((expert_total, width // wide, cap...]
    unnamed x27 -> x23, local copies, waits for them, and re-layouts: 6.65 us -> 6.07 us
  transfers between devices with their start and end apart: 16 -> 16, of which waited for: 6 -> 5; matrix products, arithmetic and copies ran while one was open for 2% -> 2% of each run, Pallas kernels for 11% -> 12%
where the time goes in v10:
time: 150 us; the launch traced here: 149 us
  starting transfers between devices  73.7 us (49%)
  waiting for transfers between devices  23.9 us (16%)
  blocking collectives  21.3 us (14%)
  Pallas kernels  20.7 us (14%)
  local copies, waits for them, and re-layouts  7.13 us (5%)
    all_gather x1, blocking collectives, local(): lax.all_gather(sequenced(attended, summed), 'tp', axis=0, tiled=True)  21.3 us
    ppermute x4, starting transfers between devices, local(): group.append(lax.ppermute(weight, 'tp', partner))  14.8 us
    all_to_all x1, waiting for transfers between devices, local(): lax.all_to_all(own_keys, 'ep', 0, 0, tiled=True, axis_index_groups=z_groups)  13.6 us
    all_to_all x1, starting transfers between devices, local(): arrived = lax.all_to_all(outgoing, 'ep', 0, 0, tiled=True)  12.9 us
    ppermute x2, starting transfers between devices, local(): group.append(lax.ppermute(group[0], 'tp', neighbour))  10.1 us
    ppermute x3, starting transfers between devices, local(): query_all.append(lax.ppermute(query, 'ep', x_shifts[x_count - i]))  9.51 us
    ppermute x3, starting transfers between devices, local(): lax.ppermute(partial_all[i], 'ep', x_shifts[i])  9.17 us
    all_to_all x1, starting transfers between devices, local(): groups = lax.all_to_all(partial_out, 'tp', 0, 0, tiled=True)  7.6 us
  transfers between devices with their start and end apart: 16, of which 5 were waited for; matrix products, arithmetic and copies ran while one was open for 2% of the time, Pallas kernels for 12%

profile of v10, /device:TPU:1, one launch (start us, length us, event | category | flops | bytes accessed | tf_op | source)
XLA Modules:
  0.0 148.7 jit_solution(11561357837357581331)
XLA Ops:
  0.7 2.4 %constant_dynamic-update-slice_fusion.1 = bf16[2,2048,256]{2,1,0:T(8,128)(2,1)} fusion(bf16[1,2048,256]{2,1,0:T(8,128)(2,1)} %param.24), kind=kLoop, calls=%fused_computation.2 | loop fusion | bytes 2097152
  4.1 5.9 %collective-permute-start.6 = (bf16[2,2048,256]{2,1,0:T(8,128)(2,1)}, bf16[2,2048,256]{2,1,0:T(8,128)(2,1)S(1)}, u32[]{:S(2)}, u32[]{:S(2)}) collective-permute-start(bf16[2,2048,256]{2,1,0:T(8,128)(2,1)} %constant_dynamic-update-slice_fusion.refs_0_), channel_id=1, source_target_pairs={{0,2},{1,15},{2,0},{3,5},{4,6},{5,3},{6,4},{7,9},{8,10},{9,7},{10,... | collective-permute-start | bytes 6291464 | tf_op jit(solution)/shard_map/ppermute | solution.py:462
  10.9 4.7 %shard_map.152 = (bf16[32,4,24,128]{3,2,1,0:T(8,128)(2,1)}, s32[256,2]{1,0:T(8,128)}) custom-call(s32[1]{0:T(128)} %bitcast.2.index_ref, bf16[256,2048]{1,0:T(8,128)(2,1)} %input_ref.1, f32[1,2048]{1,0:T(1,128)} %bitcast.12, s32[256,2]{1,0:T(8,128)} %copy.18.routes_ref, bf16[2,2048,256]{2,1,0:T(8,128)(2,1)} %constant_dynamic-update-slice_fusion.refs_0_), custom_call_target="tpu_custom_call" | custom-call | flops 805306368 | tf_op jit(solution)/shard_map/pallas_call | solution.py:191
  15.6 12.9 %all-to-all-start.1 = ((bf16[32,4,24,128]{3,2,1,0:T(8,128)(2,1)}), bf16[32,4,24,128]{3,2,1,0:T(8,128)(2,1)S(1)}, u32[]{:S(2)}, u32[]{:S(2)}) async-start(bf16[32,4,24,128]{3,2,1,0:T(8,128)(2,1)} %get-tuple-element.16), calls=%async_computation.1 | async-start | bytes 1572864 | tf_op jit(solution)/shard_map/all_to_all | solution.py:467
  30.4 4.2 %collective-permute-start.9 = (bf16[256,2048]{1,0:T(8,128)(2,1)}, bf16[256,2048]{1,0:T(8,128)(2,1)}, u32[]{:S(2)}, u32[]{:S(2)}) collective-permute-start(bf16[256,2048]{1,0:T(8,128)(2,1)} %bitcast.8), channel_id=1, source_target_pairs={{0,2},{1,15},{2,0},{3,5},{4,6},{5,3},{6,4},{7,9},{8,10},{9,7},{10,... | collective-permute-start | bytes 3145736 | tf_op jit(solution)/shard_map/ppermute | solution.py:462
  34.7 6.3 %collective-permute-start.8 = (bf16[2,2048,256]{2,1,0:T(8,128)(2,1)S(1)}, bf16[2,2048,256]{2,1,0:T(8,128)(2,1)}, u32[]{:S(2)}, u32[]{:S(2)}) collective-permute-start(bf16[2,2048,256]{2,1,0:T(8,128)(2,1)S(1)} %collective-permute-done.6.refs_1_), channel_id=1, source_target_pairs={{0,1},{1,0},{2,3},{3,2},{4,5},{5,4},{6,7},{7,6},{8,9},{9,8},{10,11... | collective-permute-start | bytes 6291464 | tf_op jit(solution)/shard_map/ppermute | solution.py:471
  41.0 1.9 %collective-permute-start.10 = (bf16[256,2048]{1,0:T(8,128)(2,1)}, bf16[256,2048]{1,0:T(8,128)(2,1)}, u32[]{:S(2)}, u32[]{:S(2)}) collective-permute-start(bf16[256,2048]{1,0:T(8,128)(2,1)} %bitcast.9), channel_id=1, source_target_pairs={{0,1},{1,0},{2,3},{3,2},{4,5},{5,4},{6,7},{7,6},{8,9},{9,8},{10,11... | collective-permute-start | bytes 3145736 | tf_op jit(solution)/shard_map/ppermute | solution.py:471
  42.9 4.8 %collective-permute-done.9.refs_5_ = bf16[256,2048]{1,0:T(8,128)(2,1)} collective-permute-done((bf16[256,2048]{1,0:T(8,128)(2,1)}, bf16[256,2048]{1,0:T(8,128)(2,1)}, u32[]{:S(2)}, u32[]{:S(2)}) %collective-permute-start.9) | collective-permute-done | bytes 1048608 | tf_op jit(solution)/shard_map/ppermute | solution.py:462
  47.7 4.7 %collective-permute-start.11 = (bf16[256,2048]{1,0:T(8,128)(2,1)}, bf16[256,2048]{1,0:T(8,128)(2,1)}, u32[]{:S(2)}, u32[]{:S(2)}) collective-permute-start(bf16[256,2048]{1,0:T(8,128)(2,1)} %collective-permute-done.9.refs_5_), channel_id=1, source_target_pairs={{0,1},{1,0},{2,3},{3,2},{4,5},{5,4},{6,7},{7,6},{8,9},{9,8},{10,11... | collective-permute-start | bytes 3145736 | tf_op jit(solution)/shard_map/ppermute | solution.py:471
  53.8 2.5 %shard_map.149 = (bf16[256,128]{1,0:T(8,128)(2,1)}, bf16[8,160,256]{2,1,0:T(8,128)(2,1)}) custom-call(s32[1]{0:T(128)} %bitcast.index_ref, bf16[256,96]{1,0:T(8,128)(2,1)} %copy.16.query_ref, bf16[256,512]{1,0:T(8,128)(2,1)} %latent_ref.1, bf16[256,32]{1,0:T(8,128)(2,1)} %copy.17.rope_ref, f32[1,512]{1,0:T(1,128)} %bitcast.13, bf16[512,128]{1,0:T(8,128)(2,1)} %weight_ref.2, ...), custom_call_target="tpu_custom_call" | custom-call | flops 33554432 | tf_op jit(solution)/shard_map/pallas_call | solution.py:90
  56.3 4.8 %all-to-all-start = ((bf16[8,160,256]{2,1,0:T(8,128)(2,1)}), bf16[8,160,256]{2,1,0:T(8,128)(2,1)}, u32[]{:S(2)}, u32[]{:S(2)}) async-start(bf16[8,160,256]{2,1,0:T(8,128)(2,1)} %get-tuple-element.10), calls=%async_computation | async-start | bytes 1310720 | tf_op jit(solution)/shard_map/all_to_all | solution.py:487
  62.4 6.0 %shard_map.153 = bf16[16,192,128]{2,1,0:T(8,128)(2,1)} custom-call(bf16[32,4,24,128]{3,2,1,0:T(8,128)(2,1)S(1)} %all-to-all-done.1.rows_ref, bf16[2,2048,256]{2,1,0:T(8,128)(2,1)} %constant_dynamic-update-slice_fusion.refs_0_, bf16[2,2048,256]{2,1,0:T(8,128)(2,1)S(1)} %collective-permute-done.6.refs_1_, ...), custom_call_target="tpu_custom_call" | custom-call | flops 2415919104 | tf_op jit(solution)/shard_map/pallas_call | solution.py:379
  68.5 13.6 %all-to-all-done.key_ref = bf16[8,160,256]{2,1,0:T(8,128)(2,1)} async-done(((bf16[8,160,256]{2,1,0:T(8,128)(2,1)}), bf16[8,160,256]{2,1,0:T(8,128)(2,1)}, u32[]{:S(2)}, u32[]{:S(2)}) %all-to-all-start) | async-done | bytes 655392 | tf_op jit(solution)/shard_map/all_to_all | solution.py:487
  82.0 7.6 %all-to-all-start.2 = ((bf16[16,192,128]{2,1,0:T(8,128)(2,1)}), bf16[16,192,128]{2,1,0:T(8,128)(2,1)S(1)}, u32[]{:S(2)}, u32[]{:S(2)}) async-start(bf16[16,192,128]{2,1,0:T(8,128)(2,1)} %shard_map.153), calls=%async_computation.2 | async-start | bytes 1572864 | tf_op jit(solution)/shard_map/all_to_all | solution.py:492
  89.7 4.4 %collective-permute-start = (bf16[256,128]{1,0:T(8,128)(2,1)S(1)}, bf16[256,128]{1,0:T(8,128)(2,1)S(1)}, u32[]{:S(2)}, u32[]{:S(2)}) collective-permute-start(bf16[256,128]{1,0:T(8,128)(2,1)S(1)} %copy-done.3), channel_id=1, source_target_pairs={{0,48},{16,0},{32,16},{48,32},{64,112},{80,64},{96,80},{112,96},{1... | collective-permute-start | bytes 196616 | tf_op jit(solution)/shard_map/ppermute | solution.py:486
  94.1 2.4 %collective-permute-start.1 = (bf16[256,128]{1,0:T(8,128)(2,1)S(1)}, bf16[256,128]{1,0:T(8,128)(2,1)S(1)}, u32[]{:S(2)}, u32[]{:S(2)}) collective-permute-start(bf16[256,128]{1,0:T(8,128)(2,1)S(1)} %copy-done.3), channel_id=1, source_target_pairs={{0,32},{16,48},{32,0},{48,16},{64,96},{80,112},{96,64},{112,80},{1... | collective-permute-start | bytes 196616 | tf_op jit(solution)/shard_map/ppermute | solution.py:486
  96.5 2.7 %collective-permute-start.2 = (bf16[256,128]{1,0:T(8,128)(2,1)S(1)}, bf16[256,128]{1,0:T(8,128)(2,1)S(1)}, u32[]{:S(2)}, u32[]{:S(2)}) collective-permute-start(bf16[256,128]{1,0:T(8,128)(2,1)S(1)} %copy-done.3), channel_id=1, source_target_pairs={{0,16},{16,32},{32,48},{48,0},{64,80},{80,96},{96,112},{112,64},{1... | collective-permute-start | bytes 196616 | tf_op jit(solution)/shard_map/ppermute | solution.py:486
  100.9 2.1 %collective-permute-done.2.refs_3_ = bf16[256,128]{1,0:T(8,128)(2,1)S(1)} collective-permute-done((bf16[256,128]{1,0:T(8,128)(2,1)S(1)}, bf16[256,128]{1,0:T(8,128)(2,1)S(1)}, u32[]{:S(2)}, u32[]{:S(2)}) %collective-permute-start.2) | collective-permute-done | bytes 65568 | tf_op jit(solution)/shard_map/ppermute | solution.py:486
  103.0 4.5 %shard_map.150 = (bf16[256,128]{1,0:T(8,128)(2,1)S(1)}, bf16[256,128]{1,0:T(8,128)(2,1)S(1)}, bf16[256,128]{1,0:T(8,128)(2,1)S(1)}, bf16[256,128]{1,0:T(8,128)(2,1)S(1)}) custom-call(bf16[8,160,256]{2,1,0:T(8,128)(2,1)} %all-to-all-done.key_ref, bf16[256,128]{1,0:T(8,128)(2,1)S(1)} %copy-done.3, bf16[256,128]{1,0:T(8,128)(2,1)S(1)} %collective-permute-done.refs_1_, ...), custom_call_target="tpu_custom_call" | custom-call | flops 2147483648 | tf_op jit(solution)/shard_map/pallas_call | solution.py:274
  107.5 2.1 %collective-permute-start.3 = (bf16[256,128]{1,0:T(8,128)(2,1)S(1)}, bf16[256,128]{1,0:T(8,128)(2,1)S(1)}, u32[]{:S(2)}, u32[]{:S(2)}) collective-permute-start(bf16[256,128]{1,0:T(8,128)(2,1)S(1)} %get-tuple-element.13), channel_id=1, source_target_pairs={{0,16},{16,32},{32,48},{48,0},{64,80},{80,96},{96,112},{112,64},{1... | collective-permute-start | bytes 196616 | tf_op jit(solution)/shard_map/ppermute | solution.py:496
  109.6 3.1 %collective-permute-start.4 = (bf16[256,128]{1,0:T(8,128)(2,1)S(1)}, bf16[256,128]{1,0:T(8,128)(2,1)S(1)}, u32[]{:S(2)}, u32[]{:S(2)}) collective-permute-start(bf16[256,128]{1,0:T(8,128)(2,1)S(1)} %get-tuple-element.14), channel_id=1, source_target_pairs={{0,32},{16,48},{32,0},{48,16},{64,96},{80,112},{96,64},{112,80},{1... | collective-permute-start | bytes 196616 | tf_op jit(solution)/shard_map/ppermute | solution.py:496
  112.7 4.0 %collective-permute-start.5 = (bf16[256,128]{1,0:T(8,128)(2,1)S(1)}, bf16[256,128]{1,0:T(8,128)(2,1)S(1)}, u32[]{:S(2)}, u32[]{:S(2)}) collective-permute-start(bf16[256,128]{1,0:T(8,128)(2,1)S(1)} %get-tuple-element.15), channel_id=1, source_target_pairs={{0,48},{16,0},{32,16},{48,32},{64,112},{80,64},{96,80},{112,96},{1... | collective-permute-start | bytes 196616 | tf_op jit(solution)/shard_map/ppermute | solution.py:496
  120.5 4.7 %all-to-all-start.3 = ((bf16[32,24,128]{2,1,0:T(8,128)(2,1)}), bf16[32,24,128]{2,1,0:T(8,128)(2,1)S(1)}, u32[]{:S(2)}, u32[]{:S(2)}) async-start(bf16[32,24,128]{2,1,0:T(8,128)(2,1)} %shard_map.154.refs_0_), calls=%async_computation.3 | async-start | bytes 393216 | tf_op jit(solution)/shard_map/all_to_all | solution.py:505
  125.3 21.3 %all_gather.3 = bf16[1024,256]{1,0:T(8,128)(2,1)S(1)} all-gather(bf16[64,256]{1,0:T(8,128)(2,1)S(1)} %shard_map.155), channel_id=1, replica_groups=mesh['ep'=32,'tp'=16] {'tp'}, dimensions={0}, use_global_device_ids=true | all-gather | bytes 557056 | tf_op jit(solution)/shard_map/all_gather | solution.py:500
  (42 shorter events, 14.0 us)
Async XLA Ops:
  0.6 146.0 %copy-start = (bf16[1024,128]{1,0:T(8,128)(2,1)S(1)}, bf16[1024,128]{1,0:T(8,128)(2,1)}, u32[]{:S(2)}) copy-start(bf16[1024,128]{1,0:T(8,128)(2,1)} %param.19) | copy-start | bytes 786436
  0.6 2.4 %copy-start.4 = (bf16[1,2048,256]{2,1,0:T(8,128)(2,1)S(1)}, bf16[1,2048,256]{2,1,0:T(8,128)(2,1)}, u32[]{:S(2)}) copy-start(bf16[1,2048,256]{2,1,0:T(8,128)(2,1)} %param.25) | copy-start | bytes 3145732
  0.7 9.4 %copy-start.7 = (s32[256,2]{0,1:T(2,128)S(1)}, s32[256,2]{0,1:T(2,128)}, u32[]{:S(2)}) copy-start(s32[256,2]{0,1:T(2,128)} %param.22) | copy-start | bytes 6148
  4.1 30.5 %collective-permute-start.6 = (bf16[2,2048,256]{2,1,0:T(8,128)(2,1)}, bf16[2,2048,256]{2,1,0:T(8,128)(2,1)S(1)}, u32[]{:S(2)}, u32[]{:S(2)}) collective-permute-start(bf16[2,2048,256]{2,1,0:T(8,128)(2,1)} %constant_dynamic-update-slice_fusion.refs_0_), channel_id=1, source_target_pairs={{0,2},{1,15},{2,0},{3,5},{4,6},{5,3},{6,4},{7,9},{8,10},{9,7},{10,... | collective-permute-start | bytes 6291464 | tf_op jit(solution)/shard_map/ppermute | solution.py:462
  10.9 41.5 %copy-start.5 = (bf16[256,96]{0,1:T(8,128)(2,1)S(1)}, bf16[256,96]{0,1:T(8,128)(2,1)}, u32[]{:S(2)}) copy-start(bf16[256,96]{0,1:T(8,128)(2,1)} %param.14) | copy-start | bytes 147460
  10.9 42.2 %copy-start.6 = (bf16[256,32]{0,1:T(8,128)(2,1)S(1)}, bf16[256,32]{0,1:T(8,128)(2,1)}, u32[]{:S(2)}) copy-start(bf16[256,32]{0,1:T(8,128)(2,1)} %param.16) | copy-start | bytes 49156
  15.6 40.7 %all-to-all-start.1 = ((bf16[32,4,24,128]{3,2,1,0:T(8,128)(2,1)}), bf16[32,4,24,128]{3,2,1,0:T(8,128)(2,1)S(1)}, u32[]{:S(2)}, u32[]{:S(2)}) async-start(bf16[32,4,24,128]{3,2,1,0:T(8,128)(2,1)} %get-tuple-element.16), calls=%async_computation.1 | async-start | bytes 1572864 | tf_op jit(solution)/shard_map/all_to_all | solution.py:467
  28.5 32.7 %collective-permute-start.7 = (bf16[2,2048,256]{2,1,0:T(8,128)(2,1)}, bf16[2,2048,256]{2,1,0:T(8,128)(2,1)}, u32[]{:S(2)}, u32[]{:S(2)}) collective-permute-start(bf16[2,2048,256]{2,1,0:T(8,128)(2,1)} %constant_dynamic-update-slice_fusion.refs_0_), channel_id=1, source_target_pairs={{0,1},{1,0},{2,3},{3,2},{4,5},{5,4},{6,7},{7,6},{8,9},{9,8},{10,11... | collective-permute-start | bytes 6291464 | tf_op jit(solution)/shard_map/ppermute | solution.py:471
  30.4 17.3 %collective-permute-start.9 = (bf16[256,2048]{1,0:T(8,128)(2,1)}, bf16[256,2048]{1,0:T(8,128)(2,1)}, u32[]{:S(2)}, u32[]{:S(2)}) collective-permute-start(bf16[256,2048]{1,0:T(8,128)(2,1)} %bitcast.8), channel_id=1, source_target_pairs={{0,2},{1,15},{2,0},{3,5},{4,6},{5,3},{6,4},{7,9},{8,10},{9,7},{10,... | collective-permute-start | bytes 3145736 | tf_op jit(solution)/shard_map/ppermute | solution.py:462
  34.7 26.6 %collective-permute-start.8 = (bf16[2,2048,256]{2,1,0:T(8,128)(2,1)S(1)}, bf16[2,2048,256]{2,1,0:T(8,128)(2,1)}, u32[]{:S(2)}, u32[]{:S(2)}) collective-permute-start(bf16[2,2048,256]{2,1,0:T(8,128)(2,1)S(1)} %collective-permute-done.6.refs_1_), channel_id=1, source_target_pairs={{0,1},{1,0},{2,3},{3,2},{4,5},{5,4},{6,7},{7,6},{8,9},{9,8},{10,11... | collective-permute-start | bytes 6291464 | tf_op jit(solution)/shard_map/ppermute | solution.py:471
  41.0 20.2 %collective-permute-start.10 = (bf16[256,2048]{1,0:T(8,128)(2,1)}, bf16[256,2048]{1,0:T(8,128)(2,1)}, u32[]{:S(2)}, u32[]{:S(2)}) collective-permute-start(bf16[256,2048]{1,0:T(8,128)(2,1)} %bitcast.9), channel_id=1, source_target_pairs={{0,1},{1,0},{2,3},{3,2},{4,5},{5,4},{6,7},{7,6},{8,9},{9,8},{10,11... | collective-permute-start | bytes 3145736 | tf_op jit(solution)/shard_map/ppermute | solution.py:471
  47.7 13.5 %collective-permute-start.11 = (bf16[256,2048]{1,0:T(8,128)(2,1)}, bf16[256,2048]{1,0:T(8,128)(2,1)}, u32[]{:S(2)}, u32[]{:S(2)}) collective-permute-start(bf16[256,2048]{1,0:T(8,128)(2,1)} %collective-permute-done.9.refs_5_), channel_id=1, source_target_pairs={{0,1},{1,0},{2,3},{3,2},{4,5},{5,4},{6,7},{7,6},{8,9},{9,8},{10,11... | collective-permute-start | bytes 3145736 | tf_op jit(solution)/shard_map/ppermute | solution.py:471
  56.3 33.3 %copy-start.3 = (bf16[256,128]{1,0:T(8,128)(2,1)S(1)}, bf16[256,128]{1,0:T(8,128)(2,1)}, u32[]{:S(2)}) copy-start(bf16[256,128]{1,0:T(8,128)(2,1)} %get-tuple-element.11.refs_0_) | copy-start | bytes 196612
  56.3 25.7 %all-to-all-start = ((bf16[8,160,256]{2,1,0:T(8,128)(2,1)}), bf16[8,160,256]{2,1,0:T(8,128)(2,1)}, u32[]{:S(2)}, u32[]{:S(2)}) async-start(bf16[8,160,256]{2,1,0:T(8,128)(2,1)} %get-tuple-element.10), calls=%async_computation | async-start | bytes 1310720 | tf_op jit(solution)/shard_map/all_to_all | solution.py:487
  82.0 37.2 %all-to-all-start.2 = ((bf16[16,192,128]{2,1,0:T(8,128)(2,1)}), bf16[16,192,128]{2,1,0:T(8,128)(2,1)S(1)}, u32[]{:S(2)}, u32[]{:S(2)}) async-start(bf16[16,192,128]{2,1,0:T(8,128)(2,1)} %shard_map.153), calls=%async_computation.2 | async-start | bytes 1572864 | tf_op jit(solution)/shard_map/all_to_all | solution.py:492
  89.7 27.1 %copy-start.8 = (f32[256,2]{0,1:T(2,128)S(1)}, f32[256,2]{0,1:T(2,128)}, u32[]{:S(2)}) copy-start(f32[256,2]{0,1:T(2,128)} %param.23) | copy-start | bytes 6148
  89.7 9.5 %collective-permute-start = (bf16[256,128]{1,0:T(8,128)(2,1)S(1)}, bf16[256,128]{1,0:T(8,128)(2,1)S(1)}, u32[]{:S(2)}, u32[]{:S(2)}) collective-permute-start(bf16[256,128]{1,0:T(8,128)(2,1)S(1)} %copy-done.3), channel_id=1, source_target_pairs={{0,48},{16,0},{32,16},{48,32},{64,112},{80,64},{96,80},{112,96},{1... | collective-permute-start | bytes 196616 | tf_op jit(solution)/shard_map/ppermute | solution.py:486
  94.1 6.8 %collective-permute-start.1 = (bf16[256,128]{1,0:T(8,128)(2,1)S(1)}, bf16[256,128]{1,0:T(8,128)(2,1)S(1)}, u32[]{:S(2)}, u32[]{:S(2)}) collective-permute-start(bf16[256,128]{1,0:T(8,128)(2,1)S(1)} %copy-done.3), channel_id=1, source_target_pairs={{0,32},{16,48},{32,0},{48,16},{64,96},{80,112},{96,64},{112,80},{1... | collective-permute-start | bytes 196616 | tf_op jit(solution)/shard_map/ppermute | solution.py:486
  96.5 6.5 %collective-permute-start.2 = (bf16[256,128]{1,0:T(8,128)(2,1)S(1)}, bf16[256,128]{1,0:T(8,128)(2,1)S(1)}, u32[]{:S(2)}, u32[]{:S(2)}) collective-permute-start(bf16[256,128]{1,0:T(8,128)(2,1)S(1)} %copy-done.3), channel_id=1, source_target_pairs={{0,16},{16,32},{32,48},{48,0},{64,80},{80,96},{96,112},{112,64},{1... | collective-permute-start | bytes 196616 | tf_op jit(solution)/shard_map/ppermute | solution.py:486
  107.5 40.1 %copy-start.2 = (s32[256,2]{1,0:T(8,128)S(1)}, s32[256,2]{1,0:T(8,128)}, u32[]{:S(2)}) copy-start(s32[256,2]{1,0:T(8,128)} %get-tuple-element.17.place_ref) | copy-start | bytes 6148
  107.5 9.3 %collective-permute-start.3 = (bf16[256,128]{1,0:T(8,128)(2,1)S(1)}, bf16[256,128]{1,0:T(8,128)(2,1)S(1)}, u32[]{:S(2)}, u32[]{:S(2)}) collective-permute-start(bf16[256,128]{1,0:T(8,128)(2,1)S(1)} %get-tuple-element.13), channel_id=1, source_target_pairs={{0,16},{16,32},{32,48},{48,0},{64,80},{80,96},{96,112},{112,64},{1... | collective-permute-start | bytes 196616 | tf_op jit(solution)/shard_map/ppermute | solution.py:496
  109.6 7.3 %collective-permute-start.4 = (bf16[256,128]{1,0:T(8,128)(2,1)S(1)}, bf16[256,128]{1,0:T(8,128)(2,1)S(1)}, u32[]{:S(2)}, u32[]{:S(2)}) collective-permute-start(bf16[256,128]{1,0:T(8,128)(2,1)S(1)} %get-tuple-element.14), channel_id=1, source_target_pairs={{0,32},{16,48},{32,0},{48,16},{64,96},{80,112},{96,64},{112,80},{1... | collective-permute-start | bytes 196616 | tf_op jit(solution)/shard_map/ppermute | solution.py:496
  112.7 5.9 %collective-permute-start.5 = (bf16[256,128]{1,0:T(8,128)(2,1)S(1)}, bf16[256,128]{1,0:T(8,128)(2,1)S(1)}, u32[]{:S(2)}, u32[]{:S(2)}) collective-permute-start(bf16[256,128]{1,0:T(8,128)(2,1)S(1)} %get-tuple-element.15), channel_id=1, source_target_pairs={{0,48},{16,0},{32,16},{48,32},{64,112},{80,64},{96,80},{112,96},{1... | collective-permute-start | bytes 196616 | tf_op jit(solution)/shard_map/ppermute | solution.py:496
  120.5 27.1 %all-to-all-start.3 = ((bf16[32,24,128]{2,1,0:T(8,128)(2,1)}), bf16[32,24,128]{2,1,0:T(8,128)(2,1)S(1)}, u32[]{:S(2)}, u32[]{:S(2)}) async-start(bf16[32,24,128]{2,1,0:T(8,128)(2,1)} %shard_map.154.refs_0_), calls=%async_computation.3 | async-start | bytes 393216 | tf_op jit(solution)/shard_map/all_to_all | solution.py:505
  (1 other events, 1.2 us)
